TPU v7x, 512 devices: a whole 4x8x8 slice. The times are simulated.
512 devices in a mesh: ep: 128 (over z, y, core), tp: 4 (over x).
Axes of the slice: x: 4, y: 8, z: 8, core: 2. Of those that a mesh axis runs over, the one named last changes fastest.
Arguments:
- tokens: bfloat16 [2304, 1024], P('ep'), may hold values from -16 to 16
- delta_state: float32 [2304, 4, 128, 128], P('ep', 'tp'), may hold values from -1.8 to 1.8
- mixer_gain: float32 [1024], replicated, may hold values from 0.1 to 1.9
- query_weight: bfloat16 [1024, 512], P(None, 'tp'), may hold values from -0.1875 to 0.1875
- key_weight: bfloat16 [1024, 512], P(None, 'tp'), may hold values from -0.1875 to 0.1875
- value_weight: bfloat16 [1024, 512], P(None, 'tp'), may hold values from -0.1875 to 0.1875
- write_weight: bfloat16 [1024, 4], P(None, 'tp'), may hold values from -0.1875 to 0.1875
- decay_weight: bfloat16 [1024, 4], P(None, 'tp'), may hold values from -0.1875 to 0.1875
- decay_rate: float32 [4], P('tp'), may hold values from 0.05 to 4
- decay_bias: float32 [4], P('tp'), may hold values from -2 to 1
- head_gain: float32 [128], replicated, may hold values from 0.1 to 1.9
- out_weight: bfloat16 [512, 1024], P('tp'), may hold values from -0.25 to 0.25
- channel_gain: float32 [1024], replicated, may hold values from 0.1 to 1.9
- routes: int32 [2304, 6], P('ep'), may hold values from 0 to 127, all different within a row; in each aligned block of 18 rows (0 to 17, 18 to 35, ...) at most 2 rows name the same one
- route_weights: float32 [2304, 6], P('ep'), may hold values from 0.1 to 1
- expert_gate: bfloat16 [128, 1024, 512], P('ep', None, 'tp'), may hold values from -0.1875 to 0.1875
- expert_up: bfloat16 [128, 1024, 512], P('ep', None, 'tp'), may hold values from -0.1875 to 0.1875
- expert_down: bfloat16 [128, 512, 1024], P('ep', 'tp'), may hold values from -0.25 to 0.25
- shared_gate: bfloat16 [1024, 512], P(None, 'tp'), may hold values from -0.1875 to 0.1875
- shared_up: bfloat16 [1024, 512], P(None, 'tp'), may hold values from -0.1875 to 0.1875
- shared_down: bfloat16 [512, 1024], P('tp'), may hold values from -0.25 to 0.25
Outputs:
- layer_out: bfloat16 [2304, 1024], P('ep', 'tp')
- next_state: float32 [2304, 4, 128, 128], P('ep', 'tp')
Inputs may be any that keep to these rules, and one draw needn't show every extreme that they name: `routes`: each row names 6 different experts. In each aligned block of 18 rows (the rows of one ep index) no expert is named by more than 2 rows, a bound that some block reaches.
All inputs are finite; a program needn't handle non-finite values.
Results may differ from a plain program's by a relative error of at most 0.015.
Values may be sent and summed in bfloat16 or wider, within the bound.
No kernel may reach another device: no remote copies, remote signals or barrier semaphores. Data moves between devices by JAX's collectives and lax.ppermute only.
A program may use at most 64 MiB of HBM per device.

v0:
```python
import jax
import jax.numpy as jnp
from jax import lax
from jax.sharding import PartitionSpec as P

EPS = 1e-06
ROUTED_SCALE = 2.5


def sent_to_all(array, axis):
    copies = jnp.broadcast_to(array, (lax.axis_size(axis), *array.shape))
    return lax.all_to_all(copies, axis, split_axis=0, concat_axis=0, tiled=True)


def over_copies(array, axis):
    return sent_to_all(array, axis).astype(jnp.float32).sum(axis=0)


def in_blocks(array, dim, length):
    shape = array.shape
    tiles = array.reshape(*shape[:dim], length, shape[dim] // length, *shape[dim + 1 :])
    return jnp.moveaxis(tiles, dim, 0)


def sent_and_summed(array, axis, dim):
    length = lax.axis_size(axis)
    tiles = lax.all_to_all(in_blocks(array, dim, length), axis, 0, 0, tiled=True)
    return jnp.sum(tiles.astype(jnp.float32), axis=0)


def side_by_side(arrays, axis, dim, along):
    ends, at = ([], 0)
    for a in arrays[:-1]:
        at += a.shape[along]
        ends.append(at)
    both = jnp.concatenate(arrays, axis=along)
    return tuple(jnp.split(sent_and_summed(both, axis, dim), ends, axis=along))


def rms_rows(values, gain_vec):
    mean_square = jnp.mean(values * values, axis=-1, keepdims=True)
    return values * lax.rsqrt(mean_square + EPS) * gain_vec


def unit_heads(raw, heads, head_dim):
    shaped = raw.astype(jnp.float32).reshape(raw.shape[0], heads, head_dim)
    return shaped * lax.rsqrt(jnp.sum(shaped * shaped, axis=-1, keepdims=True) + EPS)


def per_device(
    tokens,
    delta_state,
    mixer_gain,
    query_weight,
    key_weight,
    value_weight,
    write_weight,
    decay_weight,
    decay_rate,
    decay_bias,
    head_gain,
    out_weight,
    channel_gain,
    routes,
    route_weights,
    expert_gate,
    expert_up,
    expert_down,
    shared_gate,
    shared_up,
    shared_down,
):
    seq_rows, model_width = tokens.shape
    heads, head_dim = (delta_state.shape[1], delta_state.shape[2])
    top_k = routes.shape[1]
    tp_count = lax.axis_size("tp")
    ep_count = lax.axis_size("ep")
    share_width = model_width // tp_count
    share_start = lax.axis_index("tp") * share_width
    exp_local = expert_gate.shape[0]
    expert_total = exp_local * ep_count
    capacity = max(2, min(seq_rows, 2 * seq_rows * top_k // expert_total))
    pair_count = seq_rows * top_k
    normed = rms_rows(tokens.astype(jnp.float32), mixer_gain).astype(jnp.bfloat16)
    query_raw = jnp.dot(normed, query_weight, preferred_element_type=jnp.float32).astype(
        jnp.bfloat16
    )
    key_raw = jnp.dot(normed, key_weight, preferred_element_type=jnp.float32).astype(jnp.bfloat16)
    value_raw = jnp.dot(normed, value_weight, preferred_element_type=jnp.float32).astype(
        jnp.bfloat16
    )
    write_rate = jax.nn.sigmoid(jnp.dot(normed, write_weight, preferred_element_type=jnp.float32))
    decay_keep = jnp.exp(
        -decay_rate
        * jax.nn.softplus(
            jnp.dot(normed, decay_weight, preferred_element_type=jnp.float32) + decay_bias
        )
    )
    query_unit = unit_heads(query_raw, heads, head_dim) * head_dim ** (-0.5)
    key_unit = unit_heads(key_raw, heads, head_dim)
    value_vec = value_raw.astype(jnp.float32).reshape(seq_rows, heads, head_dim)
    held_state = decay_keep[:, :, None, None] * delta_state
    correction = value_vec - jnp.einsum(
        "rhkv,rhk->rhv", held_state, key_unit, precision=lax.Precision.HIGHEST
    )
    next_state = (
        held_state
        + write_rate[:, :, None, None] * key_unit[:, :, :, None] * correction[:, :, None, :]
    )
    readout = jnp.einsum("rhkv,rhk->rhv", next_state, query_unit, precision=lax.Precision.HIGHEST)
    head_out = rms_rows(readout, head_gain).astype(jnp.bfloat16).reshape(seq_rows, heads * head_dim)
    head_partial = jnp.dot(head_out, out_weight, preferred_element_type=jnp.float32)
    head_partial = head_partial.astype(jnp.bfloat16).astype(jnp.float32)
    mixer_out = (
        over_copies(head_partial.astype(jnp.bfloat16), "tp")
        .astype(jnp.float32)
        .astype(jnp.bfloat16)
    )
    residual = (tokens.astype(jnp.float32) + mixer_out.astype(jnp.float32)).astype(jnp.bfloat16)
    expert_input = rms_rows(residual.astype(jnp.float32), channel_gain).astype(jnp.bfloat16)
    residual_share = lax.dynamic_slice_in_dim(residual, share_start, share_width, 1)
    weight_norm = route_weights / jnp.sum(route_weights, axis=1, keepdims=True) * ROUTED_SCALE
    shared_act = (
        jax.nn.silu(jnp.dot(expert_input, shared_gate, preferred_element_type=jnp.float32))
        * jnp.dot(expert_input, shared_up, preferred_element_type=jnp.float32)
    ).astype(jnp.bfloat16)
    shared_partial = jnp.dot(shared_act, shared_down, preferred_element_type=jnp.float32)
    shared_partial = shared_partial.astype(jnp.bfloat16).astype(jnp.float32)
    order_pos = jnp.arange(pair_count, dtype=jnp.int32)
    pair_ids = routes.reshape(pair_count)
    earlier = (pair_ids[:, None] == pair_ids[None, :]) & (order_pos[:, None] > order_pos[None, :])
    slot_index = jnp.sum(earlier.astype(jnp.int32), axis=1)
    slot_flat = pair_ids * capacity + slot_index
    slot_total = expert_total * capacity
    slot_iota = jnp.arange(slot_total, dtype=jnp.int32)
    hit_table = (slot_iota[:, None] == slot_flat[None, :]).astype(jnp.float32)
    dispatch = jnp.sum(hit_table.reshape(slot_total, seq_rows, top_k), axis=2).astype(jnp.bfloat16)
    combine_mat = jnp.sum(
        (hit_table * weight_norm.reshape(1, pair_count)).reshape(slot_total, seq_rows, top_k),
        axis=2,
    )
    outgoing = jnp.dot(dispatch, expert_input, preferred_element_type=jnp.float32).astype(
        jnp.bfloat16
    )
    outgoing = outgoing.reshape(ep_count, exp_local * capacity, model_width)
    received = lax.all_to_all(outgoing, "ep", split_axis=0, concat_axis=0, tiled=True)
    expert_rows = received.reshape(ep_count, exp_local, capacity, model_width).transpose(1, 0, 2, 3)
    expert_rows = expert_rows.reshape(exp_local, ep_count * capacity, model_width)
    gate_val = jnp.einsum(
        "lrd,ldf->lrf", expert_rows, expert_gate, preferred_element_type=jnp.float32
    )
    up_val = jnp.einsum("lrd,ldf->lrf", expert_rows, expert_up, preferred_element_type=jnp.float32)
    hidden_act = (jax.nn.silu(gate_val) * up_val).astype(jnp.bfloat16)
    down_part = jnp.einsum(
        "lrf,lfd->lrd", hidden_act, expert_down, preferred_element_type=jnp.float32
    )
    down_part = down_part.astype(jnp.bfloat16).astype(jnp.float32).reshape(-1, model_width)
    summed, shared_sum = side_by_side(
        (down_part.astype(jnp.bfloat16), shared_partial.astype(jnp.bfloat16)), "tp", 1, 0
    )
    expert_share = summed.astype(jnp.bfloat16).reshape(exp_local, ep_count, capacity, share_width)
    shared_out = shared_sum.astype(jnp.bfloat16)
    homeward = expert_share.transpose(1, 0, 2, 3).reshape(
        ep_count, exp_local * capacity, share_width
    )
    returned = lax.all_to_all(homeward, "ep", split_axis=0, concat_axis=0, tiled=True)
    routed = jnp.einsum(
        "ts,td->sd",
        combine_mat,
        returned.reshape(slot_total, share_width).astype(jnp.float32),
        precision=lax.Precision.HIGHEST,
    )
    layer_out = (
        residual_share.astype(jnp.float32) + routed + shared_out.astype(jnp.float32)
    ).astype(jnp.bfloat16)
    return (layer_out, next_state)


def solution(mesh):
    return jax.shard_map(
        per_device,
        mesh=mesh,
        in_specs=(
            P("ep", None),
            P("ep", "tp", None, None),
            P(),
            P(None, "tp"),
            P(None, "tp"),
            P(None, "tp"),
            P(None, "tp"),
            P(None, "tp"),
            P("tp"),
            P("tp"),
            P(),
            P("tp", None),
            P(),
            P("ep", None),
            P("ep", None),
            P("ep", None, "tp"),
            P("ep", None, "tp"),
            P("ep", "tp", None),
            P(None, "tp"),
            P(None, "tp"),
            P("tp", None),
        ),
        out_specs=(P("ep", "tp"), P("ep", "tp", None, None)),
        check_vma=False,
    )
```

profile of v0, /device:TPU:1, one launch (start us, length us, event | category | flops | bytes accessed | tf_op | source)
XLA Modules:
  0.0 99.0 jit_solution(15603639640548451283)
XLA Ops:
  0.7 1.0 fusion.32
  1.7 1.4 %multiply_reduce_fusion.1 = (f32[18]{0:T(128)S(1)}, f32[18,128]{1,0:T(8,128)S(1)}) fusion(bf16[1024,128]{1,0:T(8,128)(2,1)} %param.25, bf16[18,1024]{1,0:T(8,128)(2,1)} %param.21, f32[1024]{0:T(1024)} %param.23, f32[18]{0:T(128)S(1)} %add_rsqrt_fusion.4), kind=kOutput, calls=%fused_computation.76 | convolution fusion | flops 4801518 | bytes 312464 | tf_op jit(solution)/shard_map/dot_general | solution.py:88
  3.1 1.0 %fusion.16 = f32[18]{0:T(128)S(1)} fusion(bf16[1024,1]{0,1:T(2,128)(2,1)} %param.27, bf16[18,1024]{1,0:T(8,128)(2,1)} %param.21, f32[1024]{0:T(1024)} %param.23, f32[18]{0:T(128)S(1)} %add_rsqrt_fusion.4), kind=kOutput, calls=%fused_computation.28 | convolution fusion | flops 110646 | bytes 43152 | tf_op jit(solution)/shard_map/dot_general | solution.py:92
  5.4 1.3 %multiply_reduce_fusion = (f32[18]{0:T(128)S(1)}, f32[18,128]{1,0:T(8,128)S(1)}) fusion(bf16[1024,128]{1,0:T(8,128)(2,1)} %param.24, bf16[18,1024]{1,0:T(8,128)(2,1)} %param.21, f32[1024]{0:T(1024)} %param.23, f32[18]{0:T(128)S(1)} %add_rsqrt_fusion.4), kind=kOutput, calls=%fused_computation.75 | convolution fusion | flops 4801518 | bytes 312464 | tf_op jit(solution)/shard_map/dot_general | solution.py:85
  6.8 1.0 %fusion.54 = f32[18]{0:T(128)S(1)} fusion(bf16[1024,1]{0,1:T(2,128)(2,1)} %param.28, f32[]{:T(128)} %bitcast.69, f32[]{:T(128)} %bitcast, bf16[18,1024]{1,0:T(8,128)(2,1)} %param.21, f32[1024]{0:T(1024)} %param.23, f32[18]{0:T(128)S(1)} %add_rsqrt_fusion.4), kind=kOutput, calls=%fused_computation.91 | convolution fusion | flops 110736 | bytes 43160 | tf_op jit(solution)/shard_map/dot_general | solution.py:96
  7.9 2.5 %fusion.2 = f32[18,1,128]{2,1,0:T(1,128)S(1)} fusion(f32[18,1,128,128]{3,2,1,0:T(8,128)} %param.22, f32[18]{0:T(128)S(1)} %fusion.54, f32[18,128,1]{1,0,2:T(8,128)S(1)} %get-tuple-element.7), kind=kOutput, calls=%fused_computation.4 | convolution fusion | flops 3833856 | bytes 1198152 | tf_op jit(solution)/shard_map/rhkv,rhk->rhv/dot_general | solution.py:103
  10.6 0.4 multiply_add_fusion
  11.2 1.1 %fusion = f32[18,1,128]{2,1,0:T(1,128)S(1)} fusion(f32[18,1,128,128]{3,2,1,0:T(8,128)S(1)} %multiply_add_fusion, f32[18,128,1]{1,0,2:T(8,128)S(1)} %multiply_bitcast_fusion), kind=kOutput, calls=%fused_computation.2 | convolution fusion | flops 3538944 | bytes 1198080 | tf_op jit(solution)/shard_map/rhkv,rhk->rhv/dot_general | solution.py:110
  12.6 0.7 broadcast_in_dim.2
  13.3 4.8 %all-to-all-start = ((bf16[4,18,1024]{2,1,0:T(8,128)(2,1)}), bf16[4,18,1024]{2,1,0:T(8,128)(2,1)S(1)}, u32[]{:S(2)}, u32[]{:S(2)}) async-start(bf16[4,18,1024]{2,1,0:T(8,128)(2,1)} %broadcast_in_dim.2), calls=%async_computation | async-start | bytes 393216 | tf_op jit(solution)/shard_map/all_to_all | solution.py:12
  19.0 4.4 %all-to-all-done = bf16[4,18,1024]{2,1,0:T(8,128)(2,1)S(1)} async-done(((bf16[4,18,1024]{2,1,0:T(8,128)(2,1)}), bf16[4,18,1024]{2,1,0:T(8,128)(2,1)S(1)}, u32[]{:S(2)}, u32[]{:S(2)}) %all-to-all-start) | async-done | bytes 147488 | tf_op jit(solution)/shard_map/all_to_all | solution.py:12
  23.5 0.3 convolution_convert_fusion.1
  23.9 1.0 reshape.227
  24.9 19.0 %all-to-all-start.1 = ((bf16[128,2,1024]{2,1,0:T(2,128)(2,1)}), bf16[128,2,1024]{2,1,0:T(2,128)(2,1)S(1)}, u32[]{:S(2)}, u32[]{:S(2)}) async-start(bf16[128,2,1024]{2,1,0:T(2,128)(2,1)} %reshape.227), calls=%async_computation.1 | async-start | bytes 1048576 | tf_op jit(solution)/shard_map/all_to_all | solution.py:146
  44.2 0.3 convolution_convert_fusion.2
  44.5 20.0 %all-to-all-done.1 = bf16[128,2,1024]{2,1,0:T(2,128)(2,1)S(1)} async-done(((bf16[128,2,1024]{2,1,0:T(2,128)(2,1)}), bf16[128,2,1024]{2,1,0:T(2,128)(2,1)S(1)}, u32[]{:S(2)}, u32[]{:S(2)}) %all-to-all-start.1) | async-done | bytes 524320 | tf_op jit(solution)/shard_map/all_to_all | solution.py:146
  64.7 0.3 fusion.22
  65.0 0.5 convolution_convert_fusion
  65.6 0.3 reshape.232
  66.0 12.6 %all_to_all.20 = bf16[4,274,256]{2,1,0:T(8,128)(2,1)S(1)} all-to-all(bf16[4,274,256]{2,1,0:T(8,128)(2,1)S(1)} %bitcast.70), channel_id=1, replica_groups=mesh['ep'=128,'tp'=4] {'tp'}, dimensions={0} | all-to-all | bytes 1122304 | tf_op jit(solution)/shard_map/all_to_all | solution.py:27
  78.7 0.7 reshape_transpose_reshape.4
  79.4 5.9 %all-to-all-start.3 = ((bf16[128,2,256]{2,1,0:T(2,128)(2,1)}), bf16[128,2,256]{2,1,0:T(2,128)(2,1)S(1)}, u32[]{:S(2)}, u32[]{:S(2)}) async-start(bf16[128,2,256]{2,1,0:T(2,128)(2,1)} %reshape_transpose_reshape.4), calls=%async_computation.3 | async-start | bytes 262144 | tf_op jit(solution)/shard_map/all_to_all | solution.py:166
  85.3 12.8 %all-to-all-done.3 = bf16[128,2,256]{2,1,0:T(2,128)(2,1)S(1)} async-done(((bf16[128,2,256]{2,1,0:T(2,128)(2,1)}), bf16[128,2,256]{2,1,0:T(2,128)(2,1)S(1)}, u32[]{:S(2)}, u32[]{:S(2)}) %all-to-all-start.3) | async-done | bytes 131104 | tf_op jit(solution)/shard_map/all_to_all | solution.py:166
  98.2 0.8 fusion.6
  (60 shorter events, 2.4 us)
Async XLA Ops:
  0.6 64.4 %copy-start = (bf16[1,128,1024]{2,1,0:T(8,128)(2,1)S(1)}, bf16[1,128,1024]{2,1,0:T(8,128)(2,1)}, u32[]{:S(2)}) copy-start(bf16[1,128,1024]{2,1,0:T(8,128)(2,1)} %param.38) | copy-start | bytes 786436
  0.6 9.7 %copy-start.3 = (bf16[18,1024]{1,0:T(8,128)(2,1)S(1)}, bf16[18,1024]{1,0:T(8,128)(2,1)}, u32[]{:S(2)}) copy-start(bf16[18,1024]{1,0:T(8,128)(2,1)} %param.21) | copy-start | bytes 110596
  0.7 9.7 %copy-start.11 = (f32[1024]{0:T(1024)S(1)}, f32[1024]{0:T(1024)}, u32[]{:S(2)}) copy-start(f32[1024]{0:T(1024)} %param.23) | copy-start | bytes 12292
  0.7 9.7 %copy-start.7 = (bf16[1024,128]{1,0:T(8,128)(2,1)S(1)}, bf16[1024,128]{1,0:T(8,128)(2,1)}, u32[]{:S(2)}) copy-start(bf16[1024,128]{1,0:T(8,128)(2,1)} %param.26) | copy-start | bytes 786436
  1.7 8.9 %copy-start.1 = (f32[18,1,128,128]{3,2,1,0:T(8,128)S(1)}, f32[18,1,128,128]{3,2,1,0:T(8,128)}, u32[]{:S(2)}) copy-start(f32[18,1,128,128]{3,2,1,0:T(8,128)} %param.22) | copy-start | bytes 3538948
  11.0 7.9 %copy-start.2 = (f32[18,1,128,128]{3,2,1,0:T(8,128)}, f32[18,1,128,128]{3,2,1,0:T(8,128)S(1)}, u32[]{:S(2)}) copy-start(f32[18,1,128,128]{3,2,1,0:T(8,128)S(1)} %multiply_add_fusion) | copy-start | bytes 3538948
  11.1 1.4 %copy-start.5 = (bf16[128,1024]{1,0:T(8,128)(2,1)S(1)}, bf16[128,1024]{1,0:T(8,128)(2,1)}, u32[]{:S(2)}) copy-start(bf16[128,1024]{1,0:T(8,128)(2,1)} %param.32) | copy-start | bytes 786436
  11.1 1.4 %copy-start.15 = (f32[128]{0:T(128)S(1)}, f32[128]{0:T(128)}, u32[]{:S(2)}) copy-start(f32[128]{0:T(128)} %param.31) | copy-start | bytes 1540
  11.1 7.1 %copy-start.14 = (s32[18,6]{0,1:T(8,128)S(1)}, s32[18,6]{0,1:T(8,128)}, u32[]{:S(2)}) copy-start(s32[18,6]{0,1:T(8,128)} %param.34) | copy-start | bytes 1300
  11.1 7.6 %copy-start.13 = (f32[18,6]{0,1:T(8,128)S(1)}, f32[18,6]{0,1:T(8,128)}, u32[]{:S(2)}) copy-start(f32[18,6]{0,1:T(8,128)} %param.35) | copy-start | bytes 1300
  11.2 12.4 %copy-start.12 = (f32[1024]{0:T(1024)S(1)}, f32[1024]{0:T(1024)}, u32[]{:S(2)}) copy-start(f32[1024]{0:T(1024)} %param.33) | copy-start | bytes 12292
  13.3 10.0 %all-to-all-start = ((bf16[4,18,1024]{2,1,0:T(8,128)(2,1)}), bf16[4,18,1024]{2,1,0:T(8,128)(2,1)S(1)}, u32[]{:S(2)}, u32[]{:S(2)}) async-start(bf16[4,18,1024]{2,1,0:T(8,128)(2,1)} %broadcast_in_dim.2), calls=%async_computation | async-start | bytes 393216 | tf_op jit(solution)/shard_map/all_to_all | solution.py:12
  23.9 20.0 %copy-start.6 = (bf16[1024,128]{1,0:T(8,128)(2,1)S(1)}, bf16[1024,128]{1,0:T(8,128)(2,1)}, u32[]{:S(2)}) copy-start(bf16[1024,128]{1,0:T(8,128)(2,1)} %param.39) | copy-start | bytes 786436
  23.9 20.3 %copy-start.8 = (bf16[128,1024]{1,0:T(8,128)(2,1)S(1)}, bf16[128,1024]{1,0:T(8,128)(2,1)}, u32[]{:S(2)}) copy-start(bf16[128,1024]{1,0:T(8,128)(2,1)} %param.41) | copy-start | bytes 786436
  23.9 20.3 %copy-start.9 = (bf16[1024,128]{1,0:T(8,128)(2,1)S(1)}, bf16[1024,128]{1,0:T(8,128)(2,1)}, u32[]{:S(2)}) copy-start(bf16[1024,128]{1,0:T(8,128)(2,1)} %param.40) | copy-start | bytes 786436
  24.9 39.6 %all-to-all-start.1 = ((bf16[128,2,1024]{2,1,0:T(2,128)(2,1)}), bf16[128,2,1024]{2,1,0:T(2,128)(2,1)S(1)}, u32[]{:S(2)}, u32[]{:S(2)}) async-start(bf16[128,2,1024]{2,1,0:T(2,128)(2,1)} %reshape.227), calls=%async_computation.1 | async-start | bytes 1048576 | tf_op jit(solution)/shard_map/all_to_all | solution.py:146
  44.0 20.8 %copy-start.4 = (bf16[1,1024,128]{2,1,0:T(8,128)(2,1)S(1)}, bf16[1,1024,128]{2,1,0:T(8,128)(2,1)}, u32[]{:S(2)}) copy-start(bf16[1,1024,128]{2,1,0:T(8,128)(2,1)} %param.36) | copy-start | bytes 786436
  44.2 20.8 %copy-start.10 = (bf16[1,1024,128]{2,1,0:T(8,128)(2,1)S(1)}, bf16[1,1024,128]{2,1,0:T(8,128)(2,1)}, u32[]{:S(2)}) copy-start(bf16[1,1024,128]{2,1,0:T(8,128)(2,1)} %param.37) | copy-start | bytes 786436
  79.4 18.7 %all-to-all-start.3 = ((bf16[128,2,256]{2,1,0:T(2,128)(2,1)}), bf16[128,2,256]{2,1,0:T(2,128)(2,1)S(1)}, u32[]{:S(2)}, u32[]{:S(2)}) async-start(bf16[128,2,256]{2,1,0:T(2,128)(2,1)} %reshape_transpose_reshape.4), calls=%async_computation.3 | async-start | bytes 262144 | tf_op jit(solution)/shard_map/all_to_all | solution.py:166
where the time goes:
time: 99.5 us; the launch traced here: 99 us
  waiting for transfers between devices  37.1 us (37%)
  starting transfers between devices  29.7 us (30%)
  blocking collectives  12.6 us (13%)
  matrix products  11.3 us (11%)
  local copies, waits for them, and re-layouts  3.48 us (3%)
  other arithmetic  2.38 us (2%)
  between operations  2.34 us (2%)
    all_to_all x1, waiting for transfers between devices, per_device(): lax.all_to_all(outgoing, 'ep', split_axis=0, concat_axis=0, tiled=True)  20 us
    all_to_all x1, starting transfers between devices, per_device(): lax.all_to_all(outgoing, 'ep', split_axis=0, concat_axis=0, tiled=True)  19 us
    all_to_all x1, waiting for transfers between devices, per_device(): lax.all_to_all(homeward, 'ep', split_axis=0, concat_axis=0, tiled=True)  12.8 us
    all_to_all x1, blocking collectives, sent_and_summed(): lax.all_to_all(in_blocks(array, dim, length), axis, 0, 0, tiled=True)  12.6 us
    all_to_all x1, starting transfers between devices, per_device(): lax.all_to_all(homeward, 'ep', split_axis=0, concat_axis=0, tiled=True)  5.88 us
    all_to_all x1, starting transfers between devices, sent_to_all(): return lax.all_to_all(copies, axis, split_axis=0, concat_axis=0, tiled=True)  4.83 us
    all_to_all x1, waiting for transfers between devices, sent_to_all(): return lax.all_to_all(copies, axis, split_axis=0, concat_axis=0, tiled=True)  4.37 us
    dot_general x1, matrix products, per_device(): jnp.einsum('rhkv,rhk->rhv', held_state, key_unit, precision=lax.Precision...  2.48 us
  transfers between devices with their start and end apart: 3, of which 3 were waited for; matrix products, arithmetic and copies ran while one was open for 1% of the time, Pallas kernels for 0%

commit v1 on v0

--- a/solution.py
+++ b/solution.py
@@ -79,8 +79,9 @@
     share_start = lax.axis_index("tp") * share_width
     exp_local = expert_gate.shape[0]
     expert_total = exp_local * ep_count
-    capacity = max(2, min(seq_rows, 2 * seq_rows * top_k // expert_total))
     pair_count = seq_rows * top_k
+    parity = lax.axis_index("tp") % 2
+    partner = [(i, i ^ 1) for i in range(tp_count)]
     normed = rms_rows(tokens.astype(jnp.float32), mixer_gain).astype(jnp.bfloat16)
     query_raw = jnp.dot(normed, query_weight, preferred_element_type=jnp.float32).astype(
         jnp.bfloat16
@@ -111,11 +112,11 @@
     head_out = rms_rows(readout, head_gain).astype(jnp.bfloat16).reshape(seq_rows, heads * head_dim)
     head_partial = jnp.dot(head_out, out_weight, preferred_element_type=jnp.float32)
     head_partial = head_partial.astype(jnp.bfloat16).astype(jnp.float32)
-    mixer_out = (
-        over_copies(head_partial.astype(jnp.bfloat16), "tp")
-        .astype(jnp.float32)
-        .astype(jnp.bfloat16)
-    )
+    mixer_out = over_copies(head_partial.astype(jnp.bfloat16), "tp").astype(jnp.bfloat16)
+    gate_own, up_own, down_own = (expert_gate[0], expert_up[0], expert_down[0])
+    gate_other = lax.ppermute(gate_own, "tp", partner)
+    up_other = lax.ppermute(up_own, "tp", partner)
+    down_other = lax.ppermute(down_own, "tp", partner)
     residual = (tokens.astype(jnp.float32) + mixer_out.astype(jnp.float32)).astype(jnp.bfloat16)
     expert_input = rms_rows(residual.astype(jnp.float32), channel_gain).astype(jnp.bfloat16)
     residual_share = lax.dynamic_slice_in_dim(residual, share_start, share_width, 1)
@@ -130,49 +131,43 @@
     pair_ids = routes.reshape(pair_count)
     earlier = (pair_ids[:, None] == pair_ids[None, :]) & (order_pos[:, None] > order_pos[None, :])
     slot_index = jnp.sum(earlier.astype(jnp.int32), axis=1)
-    slot_flat = pair_ids * capacity + slot_index
-    slot_total = expert_total * capacity
-    slot_iota = jnp.arange(slot_total, dtype=jnp.int32)
-    hit_table = (slot_iota[:, None] == slot_flat[None, :]).astype(jnp.float32)
-    dispatch = jnp.sum(hit_table.reshape(slot_total, seq_rows, top_k), axis=2).astype(jnp.bfloat16)
+    expert_iota = jnp.arange(expert_total, dtype=jnp.int32)
+    hit_table = (
+        (expert_iota[:, None] == pair_ids[None, :]) & (slot_index[None, :] == parity)
+    ).astype(jnp.float32)
+    dispatch = jnp.sum(hit_table.reshape(expert_total, seq_rows, top_k), axis=2).astype(
+        jnp.bfloat16
+    )
     combine_mat = jnp.sum(
-        (hit_table * weight_norm.reshape(1, pair_count)).reshape(slot_total, seq_rows, top_k),
+        (hit_table * weight_norm.reshape(1, pair_count)).reshape(expert_total, seq_rows, top_k),
         axis=2,
     )
     outgoing = jnp.dot(dispatch, expert_input, preferred_element_type=jnp.float32).astype(
         jnp.bfloat16
     )
-    outgoing = outgoing.reshape(ep_count, exp_local * capacity, model_width)
-    received = lax.all_to_all(outgoing, "ep", split_axis=0, concat_axis=0, tiled=True)
-    expert_rows = received.reshape(ep_count, exp_local, capacity, model_width).transpose(1, 0, 2, 3)
-    expert_rows = expert_rows.reshape(exp_local, ep_count * capacity, model_width)
-    gate_val = jnp.einsum(
-        "lrd,ldf->lrf", expert_rows, expert_gate, preferred_element_type=jnp.float32
-    )
-    up_val = jnp.einsum("lrd,ldf->lrf", expert_rows, expert_up, preferred_element_type=jnp.float32)
-    hidden_act = (jax.nn.silu(gate_val) * up_val).astype(jnp.bfloat16)
-    down_part = jnp.einsum(
-        "lrf,lfd->lrd", hidden_act, expert_down, preferred_element_type=jnp.float32
-    )
-    down_part = down_part.astype(jnp.bfloat16).astype(jnp.float32).reshape(-1, model_width)
-    summed, shared_sum = side_by_side(
-        (down_part.astype(jnp.bfloat16), shared_partial.astype(jnp.bfloat16)), "tp", 1, 0
-    )
-    expert_share = summed.astype(jnp.bfloat16).reshape(exp_local, ep_count, capacity, share_width)
-    shared_out = shared_sum.astype(jnp.bfloat16)
-    homeward = expert_share.transpose(1, 0, 2, 3).reshape(
-        ep_count, exp_local * capacity, share_width
-    )
+    received = lax.all_to_all(
+        outgoing.reshape(ep_count, 1, model_width), "ep", split_axis=0, concat_axis=0, tiled=True
+    )
+    rows = received.reshape(ep_count, model_width)
+    down_part = jnp.zeros((ep_count, model_width), jnp.float32)
+    for gate, up, down in (
+        (gate_own, up_own, down_own),
+        (gate_other, up_other, down_other),
+    ):
+        gate_val = jnp.dot(rows, gate, preferred_element_type=jnp.float32)
+        up_val = jnp.dot(rows, up, preferred_element_type=jnp.float32)
+        hidden_act = (jax.nn.silu(gate_val) * up_val).astype(jnp.bfloat16)
+        down_part = down_part + jnp.dot(hidden_act, down, preferred_element_type=jnp.float32)
+    homeward = down_part.astype(jnp.bfloat16).reshape(ep_count, 1, model_width)
     returned = lax.all_to_all(homeward, "ep", split_axis=0, concat_axis=0, tiled=True)
     routed = jnp.einsum(
         "ts,td->sd",
         combine_mat,
-        returned.reshape(slot_total, share_width).astype(jnp.float32),
+        returned.reshape(ep_count, model_width).astype(jnp.float32),
         precision=lax.Precision.HIGHEST,
     )
-    layer_out = (
-        residual_share.astype(jnp.float32) + routed + shared_out.astype(jnp.float32)
-    ).astype(jnp.bfloat16)
+    share_sum = sent_and_summed((routed + shared_partial).astype(jnp.bfloat16), "tp", 1)
+    layer_out = (residual_share.astype(jnp.float32) + share_sum).astype(jnp.bfloat16)
     return (layer_out, next_state)
 
 

time: 99.5 us -> 108 us (1.085)
  starting transfers between devices: 29.7 us -> 49.7 us
  blocking collectives: 12.6 us -> 0 us
  waiting for transfers between devices: 37.1 us -> 34.8 us
  other arithmetic: 2.38 us -> 4.48 us
  local copies, waits for them, and re-layouts: 3.48 us -> 4.6 us
    all_to_all x1 -> x0, blocking collectives: 12.6 us -> none  [sent_and_summed(): lax.all_to_all(in_blocks(array, dim, length), axis, 0, 0, tiled=True)]
    all_to_all x1, starting transfers between devices: 5.88 us -> 15.1 us  [per_device(): lax.all_to_all(homeward, 'ep', split_axis=0, concat_axis=0, tiled=True)]
    all_to_all x1 -> x2, waiting for transfers between devices: 20 us -> 12 us  [the longest x1 7.7 us: per_device(): lax.all_to_all(outgoing.reshape(ep_count, 1, model_width), 'ep', split_ax...]
    ppermute x0 -> x3, starting transfers between devices: none -> 7.48 us  [the longest x1 3.08 us: per_device(): gate_other = lax.ppermute(gate_own, 'tp', partner)]
    ppermute x0 -> x3, waiting for transfers between devices: none -> 3.72 us  [the longest x1 3.71 us: per_device(): down_other = lax.ppermute(down_own, 'tp', partner)]
    all_to_all x1 -> x2, starting transfers between devices: 19 us -> 22.3 us  [the longest x1 19 us: per_device(): lax.all_to_all(outgoing.reshape(ep_count, 1, model_width), 'ep', split_ax...]
    unnamed x33 -> x38, local copies, waits for them, and re-layouts: 0.2 us -> 2.46 us
    all_to_all x1, waiting for transfers between devices: 12.8 us -> 14.7 us  [per_device(): lax.all_to_all(homeward, 'ep', split_axis=0, concat_axis=0, tiled=True)]
  transfers between devices with their start and end apart: 3 -> 7, of which waited for: 3 -> 5; matrix products, arithmetic and copies ran while one was open for 1% -> 2% of each run, Pallas kernels for 0% -> 0%
where the time goes in v1:
time: 108 us; the launch traced here: 107 us
  starting transfers between devices  49.7 us (46%)
  waiting for transfers between devices  34.8 us (32%)
  matrix products  11.1 us (10%)
  local copies, waits for them, and re-layouts  4.6 us (4%)
  other arithmetic  4.48 us (4%)
  between operations  2.39 us (2%)
    all_to_all x1, starting transfers between devices, per_device(): lax.all_to_all(outgoing.reshape(ep_count, 1, model_width), 'ep', split_ax...  19 us
    all_to_all x1, starting transfers between devices, per_device(): lax.all_to_all(homeward, 'ep', split_axis=0, concat_axis=0, tiled=True)  15.1 us
    all_to_all x1, waiting for transfers between devices, per_device(): lax.all_to_all(homeward, 'ep', split_axis=0, concat_axis=0, tiled=True)  14.7 us
    all_to_all x1, waiting for transfers between devices, per_device(): lax.all_to_all(outgoing.reshape(ep_count, 1, model_width), 'ep', split_ax...  7.7 us
    all_to_all x1, starting transfers between devices, sent_to_all(): return lax.all_to_all(copies, axis, split_axis=0, concat_axis=0, tiled=True)  4.83 us
    all_to_all x1, waiting for transfers between devices, sent_to_all(): return lax.all_to_all(copies, axis, split_axis=0, concat_axis=0, tiled=True)  4.37 us
    all_to_all x1, waiting for transfers between devices, sent_and_summed(): lax.all_to_all(in_blocks(array, dim, length), axis, 0, 0, tiled=True)  4.35 us
    ppermute x1, waiting for transfers between devices, per_device(): down_other = lax.ppermute(down_own, 'tp', partner)  3.71 us
  transfers between devices with their start and end apart: 7, of which 5 were waited for; matrix products, arithmetic and copies ran while one was open for 2% of the time, Pallas kernels for 0%

profile of v1, /device:TPU:1, one launch (start us, length us, event | category | flops | bytes accessed | tf_op | source)
XLA Modules:
  0.0 107.0 jit_solution(5398676059387860522)
XLA Ops:
  0.7 1.0 fusion.36
  1.7 1.4 %multiply_reduce_fusion.1 = (f32[18]{0:T(128)S(1)}, f32[18,128]{1,0:T(8,128)S(1)}) fusion(bf16[1024,128]{1,0:T(8,128)(2,1)} %param.25, bf16[18,1024]{1,0:T(8,128)(2,1)} %param.21, f32[1024]{0:T(1024)} %param.23, f32[18]{0:T(128)S(1)} %add_rsqrt_fusion.4), kind=kOutput, calls=%fused_computation.87 | convolution fusion | flops 4801518 | bytes 312464 | tf_op jit(solution)/shard_map/dot_general | solution.py:89
  3.1 1.0 fusion.20
  5.4 1.3 %multiply_reduce_fusion = (f32[18]{0:T(128)S(1)}, f32[18,128]{1,0:T(8,128)S(1)}) fusion(bf16[1024,128]{1,0:T(8,128)(2,1)} %param.24, bf16[18,1024]{1,0:T(8,128)(2,1)} %param.21, f32[1024]{0:T(1024)} %param.23, f32[18]{0:T(128)S(1)} %add_rsqrt_fusion.4), kind=kOutput, calls=%fused_computation.86 | convolution fusion | flops 4801518 | bytes 312464 | tf_op jit(solution)/shard_map/dot_general | solution.py:86
  6.8 1.0 fusion.69
  7.9 2.5 %fusion.3 = f32[18,1,128]{2,1,0:T(1,128)S(1)} fusion(f32[18,1,128,128]{3,2,1,0:T(8,128)} %param.22, f32[18]{0:T(128)S(1)} %fusion.69, f32[18,128,1]{1,0,2:T(8,128)S(1)} %get-tuple-element.7), kind=kOutput, calls=%fused_computation.5 | convolution fusion | flops 3833856 | bytes 1198152 | tf_op jit(solution)/shard_map/rhkv,rhk->rhv/dot_general | solution.py:104
  11.2 1.1 %fusion.1 = f32[18,1,128]{2,1,0:T(1,128)S(1)} fusion(f32[18,1,128,128]{3,2,1,0:T(8,128)S(1)} %multiply_add_fusion, f32[18,128,1]{1,0,2:T(8,128)S(1)} %multiply_bitcast_fusion), kind=kOutput, calls=%fused_computation.3 | convolution fusion | flops 3538944 | bytes 1198080 | tf_op jit(solution)/shard_map/rhkv,rhk->rhv/dot_general | solution.py:111
  12.6 0.7 broadcast_in_dim.2
  13.3 4.8 %all-to-all-start = ((bf16[4,18,1024]{2,1,0:T(8,128)(2,1)}), bf16[4,18,1024]{2,1,0:T(8,128)(2,1)S(1)}, u32[]{:S(2)}, u32[]{:S(2)}) async-start(bf16[4,18,1024]{2,1,0:T(8,128)(2,1)} %broadcast_in_dim.2), calls=%async_computation | async-start | bytes 393216 | tf_op jit(solution)/shard_map/all_to_all | solution.py:12
  19.0 4.4 %all-to-all-done = bf16[4,18,1024]{2,1,0:T(8,128)(2,1)S(1)} async-done(((bf16[4,18,1024]{2,1,0:T(8,128)(2,1)}), bf16[4,18,1024]{2,1,0:T(8,128)(2,1)S(1)}, u32[]{:S(2)}, u32[]{:S(2)}) %all-to-all-start) | async-done | bytes 147488 | tf_op jit(solution)/shard_map/all_to_all | solution.py:12
  24.3 0.8 reduce.7
  25.1 0.9 reshape.225
  26.0 19.0 %all-to-all-start.1 = ((bf16[128,2,512]{2,1,0:T(2,128)(2,1)}), bf16[128,2,512]{2,1,0:T(2,128)(2,1)S(1)}, u32[]{:S(2)}, u32[]{:S(2)}) async-start(bf16[128,2,512]{2,1,0:T(2,128)(2,1)} %reshape.225), calls=%async_computation.1 | async-start | bytes 524288 | tf_op jit(solution)/shard_map/all_to_all | solution.py:148
  45.0 2.2 %collective-permute-start.1 = (bf16[1024,128]{1,0:T(8,128)(2,1)S(1)}, bf16[1024,128]{1,0:T(8,128)(2,1)S(1)}, u32[]{:S(2)}, u32[]{:S(2)}) collective-permute-start(bf16[1024,128]{1,0:T(8,128)(2,1)S(1)} %bitcast.92), channel_id=1, source_target_pairs={{0,1},{1,0},{2,3},{3,2},{4,5},{5,4},{6,7},{7,6},{8,9},{9,8},{10,11... | collective-permute-start | bytes 786440 | tf_op jit(solution)/shard_map/ppermute | solution.py:118
  47.3 3.1 %collective-permute-start = (bf16[1024,128]{1,0:T(8,128)(2,1)S(1)}, bf16[1024,128]{1,0:T(8,128)(2,1)S(1)}, u32[]{:S(2)}, u32[]{:S(2)}) collective-permute-start(bf16[1024,128]{1,0:T(8,128)(2,1)S(1)} %bitcast.91), channel_id=1, source_target_pairs={{0,1},{1,0},{2,3},{3,2},{4,5},{5,4},{6,7},{7,6},{8,9},{9,8},{10,11... | collective-permute-start | bytes 786440 | tf_op jit(solution)/shard_map/ppermute | solution.py:117
  50.4 2.2 %collective-permute-start.2 = (bf16[128,1024]{1,0:T(8,128)(2,1)S(1)}, bf16[128,1024]{1,0:T(8,128)(2,1)S(1)}, u32[]{:S(2)}, u32[]{:S(2)}) collective-permute-start(bf16[128,1024]{1,0:T(8,128)(2,1)S(1)} %bitcast.93), channel_id=1, source_target_pairs={{0,1},{1,0},{2,3},{3,2},{4,5},{5,4},{6,7},{7,6},{8,9},{9,8},{10,11... | collective-permute-start | bytes 786440 | tf_op jit(solution)/shard_map/ppermute | solution.py:119
  52.6 7.7 %all-to-all-done.1 = bf16[128,2,512]{2,1,0:T(2,128)(2,1)S(1)} async-done(((bf16[128,2,512]{2,1,0:T(2,128)(2,1)}), bf16[128,2,512]{2,1,0:T(2,128)(2,1)S(1)}, u32[]{:S(2)}, u32[]{:S(2)}) %all-to-all-start.1) | async-done | bytes 262176 | tf_op jit(solution)/shard_map/all_to_all | solution.py:148
  61.4 3.7 %collective-permute-done.2 = bf16[128,1024]{1,0:T(8,128)(2,1)S(1)} collective-permute-done((bf16[128,1024]{1,0:T(8,128)(2,1)S(1)}, bf16[128,1024]{1,0:T(8,128)(2,1)S(1)}, u32[]{:S(2)}, u32[]{:S(2)}) %collective-permute-start.2) | collective-permute-done | bytes 262176 | tf_op jit(solution)/shard_map/ppermute | solution.py:119
  65.6 0.9 reduce.8
  66.4 0.9 reshape.227
  67.3 15.1 %all-to-all-start.2 = ((bf16[128,2,512]{2,1,0:T(2,128)(2,1)}), bf16[128,2,512]{2,1,0:T(2,128)(2,1)S(1)}, u32[]{:S(2)}, u32[]{:S(2)}) async-start(bf16[128,2,512]{2,1,0:T(2,128)(2,1)} %reshape.227), calls=%async_computation.2 | async-start | bytes 524288 | tf_op jit(solution)/shard_map/all_to_all | solution.py:162
  83.0 14.7 %all-to-all-done.2 = bf16[128,2,512]{2,1,0:T(2,128)(2,1)S(1)} async-done(((bf16[128,2,512]{2,1,0:T(2,128)(2,1)}), bf16[128,2,512]{2,1,0:T(2,128)(2,1)S(1)}, u32[]{:S(2)}, u32[]{:S(2)}) %all-to-all-start.2) | async-done | bytes 262176 | tf_op jit(solution)/shard_map/all_to_all | solution.py:162
  98.8 3.3 %all-to-all-start.3 = ((bf16[4,18,256]{2,1,0:T(8,128)(2,1)}), bf16[4,18,256]{2,1,0:T(8,128)(2,1)S(1)}, u32[]{:S(2)}, u32[]{:S(2)}) async-start(bf16[4,18,256]{2,1,0:T(8,128)(2,1)} %bitcast.89), calls=%async_computation.3 | async-start | bytes 98304 | tf_op jit(solution)/shard_map/all_to_all | solution.py:27
  102.1 4.4 %all-to-all-done.3 = bf16[4,18,256]{2,1,0:T(8,128)(2,1)S(1)} async-done(((bf16[4,18,256]{2,1,0:T(8,128)(2,1)}), bf16[4,18,256]{2,1,0:T(8,128)(2,1)S(1)}, u32[]{:S(2)}, u32[]{:S(2)}) %all-to-all-start.3) | async-done | bytes 36896 | tf_op jit(solution)/shard_map/all_to_all | solution.py:27
  (72 shorter events, 6.7 us)
Async XLA Ops:
  0.6 11.8 %copy-start = (bf16[128,1024]{1,0:T(8,128)(2,1)S(1)}, bf16[128,1024]{1,0:T(8,128)(2,1)}, u32[]{:S(2)}) copy-start(bf16[128,1024]{1,0:T(8,128)(2,1)} %param.32) | copy-start | bytes 786436
  0.6 9.7 %copy-start.3 = (bf16[18,1024]{1,0:T(8,128)(2,1)S(1)}, bf16[18,1024]{1,0:T(8,128)(2,1)}, u32[]{:S(2)}) copy-start(bf16[18,1024]{1,0:T(8,128)(2,1)} %param.21) | copy-start | bytes 110596
  0.7 9.7 %copy-start.11 = (f32[1024]{0:T(1024)S(1)}, f32[1024]{0:T(1024)}, u32[]{:S(2)}) copy-start(f32[1024]{0:T(1024)} %param.23) | copy-start | bytes 12292
  0.7 9.7 %copy-start.5 = (bf16[1024,128]{1,0:T(8,128)(2,1)S(1)}, bf16[1024,128]{1,0:T(8,128)(2,1)}, u32[]{:S(2)}) copy-start(bf16[1024,128]{1,0:T(8,128)(2,1)} %param.26) | copy-start | bytes 786436
  1.7 8.9 %copy-start.1 = (f32[18,1,128,128]{3,2,1,0:T(8,128)S(1)}, f32[18,1,128,128]{3,2,1,0:T(8,128)}, u32[]{:S(2)}) copy-start(f32[18,1,128,128]{3,2,1,0:T(8,128)} %param.22) | copy-start | bytes 3538948
  11.0 12.3 %copy-start.2 = (f32[18,1,128,128]{3,2,1,0:T(8,128)}, f32[18,1,128,128]{3,2,1,0:T(8,128)S(1)}, u32[]{:S(2)}) copy-start(f32[18,1,128,128]{3,2,1,0:T(8,128)S(1)} %multiply_add_fusion) | copy-start | bytes 3538948
  11.1 1.4 %copy-start.15 = (f32[128]{0:T(128)S(1)}, f32[128]{0:T(128)}, u32[]{:S(2)}) copy-start(f32[128]{0:T(128)} %param.31) | copy-start | bytes 1540
  11.1 7.1 %copy-start.14 = (s32[18,6]{0,1:T(8,128)S(1)}, s32[18,6]{0,1:T(8,128)}, u32[]{:S(2)}) copy-start(s32[18,6]{0,1:T(8,128)} %param.34) | copy-start | bytes 1300
  11.1 7.6 %copy-start.13 = (f32[18,6]{0,1:T(8,128)S(1)}, f32[18,6]{0,1:T(8,128)}, u32[]{:S(2)}) copy-start(f32[18,6]{0,1:T(8,128)} %param.35) | copy-start | bytes 1300
  11.2 12.4 %copy-start.12 = (f32[1024]{0:T(1024)S(1)}, f32[1024]{0:T(1024)}, u32[]{:S(2)}) copy-start(f32[1024]{0:T(1024)} %param.33) | copy-start | bytes 12292
  13.3 10.0 %all-to-all-start = ((bf16[4,18,1024]{2,1,0:T(8,128)(2,1)}), bf16[4,18,1024]{2,1,0:T(8,128)(2,1)S(1)}, u32[]{:S(2)}, u32[]{:S(2)}) async-start(bf16[4,18,1024]{2,1,0:T(8,128)(2,1)} %broadcast_in_dim.2), calls=%async_computation | async-start | bytes 393216 | tf_op jit(solution)/shard_map/all_to_all | solution.py:12
  18.7 26.3 %copy-start.9 = (bf16[1,1024,128]{2,1,0:T(8,128)(2,1)S(1)}, bf16[1,1024,128]{2,1,0:T(8,128)(2,1)}, u32[]{:S(2)}) copy-start(bf16[1,1024,128]{2,1,0:T(8,128)(2,1)} %param.37) | copy-start | bytes 786436
  18.7 28.5 %copy-start.6 = (bf16[1,1024,128]{2,1,0:T(8,128)(2,1)S(1)}, bf16[1,1024,128]{2,1,0:T(8,128)(2,1)}, u32[]{:S(2)}) copy-start(bf16[1,1024,128]{2,1,0:T(8,128)(2,1)} %param.36) | copy-start | bytes 786436
  18.8 31.5 %copy-start.10 = (bf16[1,128,1024]{2,1,0:T(8,128)(2,1)S(1)}, bf16[1,128,1024]{2,1,0:T(8,128)(2,1)}, u32[]{:S(2)}) copy-start(bf16[1,128,1024]{2,1,0:T(8,128)(2,1)} %param.38) | copy-start | bytes 786436
  26.0 34.3 %all-to-all-start.1 = ((bf16[128,2,512]{2,1,0:T(2,128)(2,1)}), bf16[128,2,512]{2,1,0:T(2,128)(2,1)S(1)}, u32[]{:S(2)}, u32[]{:S(2)}) async-start(bf16[128,2,512]{2,1,0:T(2,128)(2,1)} %reshape.225), calls=%async_computation.1 | async-start | bytes 524288 | tf_op jit(solution)/shard_map/all_to_all | solution.py:148
  45.0 15.8 %collective-permute-start.1 = (bf16[1024,128]{1,0:T(8,128)(2,1)S(1)}, bf16[1024,128]{1,0:T(8,128)(2,1)S(1)}, u32[]{:S(2)}, u32[]{:S(2)}) collective-permute-start(bf16[1024,128]{1,0:T(8,128)(2,1)S(1)} %bitcast.92), channel_id=1, source_target_pairs={{0,1},{1,0},{2,3},{3,2},{4,5},{5,4},{6,7},{7,6},{8,9},{9,8},{10,11... | collective-permute-start | bytes 786440 | tf_op jit(solution)/shard_map/ppermute | solution.py:118
  47.3 14.2 %collective-permute-start = (bf16[1024,128]{1,0:T(8,128)(2,1)S(1)}, bf16[1024,128]{1,0:T(8,128)(2,1)S(1)}, u32[]{:S(2)}, u32[]{:S(2)}) collective-permute-start(bf16[1024,128]{1,0:T(8,128)(2,1)S(1)} %bitcast.91), channel_id=1, source_target_pairs={{0,1},{1,0},{2,3},{3,2},{4,5},{5,4},{6,7},{7,6},{8,9},{9,8},{10,11... | collective-permute-start | bytes 786440 | tf_op jit(solution)/shard_map/ppermute | solution.py:117
  50.4 14.8 %collective-permute-start.2 = (bf16[128,1024]{1,0:T(8,128)(2,1)S(1)}, bf16[128,1024]{1,0:T(8,128)(2,1)S(1)}, u32[]{:S(2)}, u32[]{:S(2)}) collective-permute-start(bf16[128,1024]{1,0:T(8,128)(2,1)S(1)} %bitcast.93), channel_id=1, source_target_pairs={{0,1},{1,0},{2,3},{3,2},{4,5},{5,4},{6,7},{7,6},{8,9},{9,8},{10,11... | collective-permute-start | bytes 786440 | tf_op jit(solution)/shard_map/ppermute | solution.py:119
  65.5 16.9 %copy-start.4 = (bf16[1024,128]{1,0:T(8,128)(2,1)S(1)}, bf16[1024,128]{1,0:T(8,128)(2,1)}, u32[]{:S(2)}) copy-start(bf16[1024,128]{1,0:T(8,128)(2,1)} %param.39) | copy-start | bytes 786436
  65.5 17.1 %copy-start.7 = (bf16[128,1024]{1,0:T(8,128)(2,1)S(1)}, bf16[128,1024]{1,0:T(8,128)(2,1)}, u32[]{:S(2)}) copy-start(bf16[128,1024]{1,0:T(8,128)(2,1)} %param.41) | copy-start | bytes 786436
  65.6 17.1 %copy-start.8 = (bf16[1024,128]{1,0:T(8,128)(2,1)S(1)}, bf16[1024,128]{1,0:T(8,128)(2,1)}, u32[]{:S(2)}) copy-start(bf16[1024,128]{1,0:T(8,128)(2,1)} %param.40) | copy-start | bytes 786436
  67.3 30.3 %all-to-all-start.2 = ((bf16[128,2,512]{2,1,0:T(2,128)(2,1)}), bf16[128,2,512]{2,1,0:T(2,128)(2,1)S(1)}, u32[]{:S(2)}, u32[]{:S(2)}) async-start(bf16[128,2,512]{2,1,0:T(2,128)(2,1)} %reshape.227), calls=%async_computation.2 | async-start | bytes 524288 | tf_op jit(solution)/shard_map/all_to_all | solution.py:162
  98.8 7.6 %all-to-all-start.3 = ((bf16[4,18,256]{2,1,0:T(8,128)(2,1)}), bf16[4,18,256]{2,1,0:T(8,128)(2,1)S(1)}, u32[]{:S(2)}, u32[]{:S(2)}) async-start(bf16[4,18,256]{2,1,0:T(8,128)(2,1)} %bitcast.89), calls=%async_computation.3 | async-start | bytes 98304 | tf_op jit(solution)/shard_map/all_to_all | solution.py:27

commit v2 on v1

v2 whole, which is shorter than its diff:
```python
import jax
import jax.numpy as jnp
from jax import lax
from jax.experimental import pallas as pl
from jax.experimental.pallas import tpu as pltpu
from jax.sharding import PartitionSpec as P

EPS = 1e-06
ROUTED_SCALE = 2.5


def rms_rows(values, gain_vec):
    mean_square = jnp.mean(values * values, axis=-1, keepdims=True)
    return values * lax.rsqrt(mean_square + EPS) * gain_vec


def unit_rows(raw):
    vals = raw.astype(jnp.bfloat16).astype(jnp.float32)
    return vals * lax.rsqrt(jnp.sum(vals * vals, axis=-1, keepdims=True) + EPS)


def columns_of(rows):
    pad = jnp.zeros((128 - rows.shape[0], rows.shape[1]), rows.dtype)
    return jnp.concatenate([rows, pad], axis=0).T


def mixer_kernel(
    tokens_ref,
    gain_ref,
    write_ref,
    decay_ref,
    head_gain_ref,
    rate_ref,
    bias_ref,
    query_hbm,
    key_hbm,
    value_hbm,
    state_hbm,
    out_weight_hbm,
    partial_ref,
    key_unit_ref,
    update_ref,
    keep_ref,
    query_v,
    key_v,
    value_v,
    state_v,
    out_weight_v,
    found_k,
    found_q,
    sems,
):
    seq_rows = tokens_ref.shape[0]
    half = seq_rows // 2
    copies = [
        pltpu.make_async_copy(query_hbm, query_v, sems.at[0]),
        pltpu.make_async_copy(key_hbm, key_v, sems.at[1]),
        pltpu.make_async_copy(value_hbm, value_v, sems.at[2]),
        pltpu.make_async_copy(
            state_hbm.at[pl.ds(0, half)], state_v.at[pl.ds(0, half)], sems.at[3]
        ),
        pltpu.make_async_copy(
            state_hbm.at[pl.ds(half, seq_rows - half)],
            state_v.at[pl.ds(half, seq_rows - half)],
            sems.at[4],
        ),
        pltpu.make_async_copy(out_weight_hbm, out_weight_v, sems.at[5]),
    ]
    for copy in copies:
        copy.start()
    normed = rms_rows(tokens_ref[...].astype(jnp.float32), gain_ref[...]).astype(jnp.bfloat16)
    wide = normed.astype(jnp.float32)
    write_logit = jnp.sum(wide * write_ref[...].astype(jnp.float32), axis=-1, keepdims=True)
    decay_logit = jnp.sum(wide * decay_ref[...].astype(jnp.float32), axis=-1, keepdims=True)
    write_rate = 1.0 / (1.0 + jnp.exp(-write_logit))
    biased = decay_logit + bias_ref[0]
    softplus = jnp.maximum(biased, 0.0) + jnp.log1p(jnp.exp(-jnp.abs(biased)))
    keep = jnp.exp(-rate_ref[0] * softplus)
    copies[0].wait()
    query_raw = jnp.dot(normed, query_v[...], preferred_element_type=jnp.float32)
    copies[1].wait()
    key_raw = jnp.dot(normed, key_v[...], preferred_element_type=jnp.float32)
    copies[2].wait()
    value_raw = jnp.dot(normed, value_v[...], preferred_element_type=jnp.float32)
    query_unit = unit_rows(query_raw) * query_raw.shape[1] ** (-0.5)
    key_unit = unit_rows(key_raw)
    value_vec = value_raw.astype(jnp.bfloat16).astype(jnp.float32)
    key_cols = columns_of(key_unit)
    query_cols = columns_of(query_unit)
    for row in range(seq_rows):
        if row == 0:
            copies[3].wait()
        if row == half:
            copies[4].wait()
        state = state_v[row]
        found_k[row : row + 1, :] = jnp.sum(
            state * key_cols[:, row : row + 1], axis=0, keepdims=True
        )
        found_q[row : row + 1, :] = jnp.sum(
            state * query_cols[:, row : row + 1], axis=0, keepdims=True
        )
    correction = value_vec - keep * found_k[...]
    overlap = jnp.sum(key_unit * query_unit, axis=-1, keepdims=True)
    update = write_rate * correction
    readout = keep * found_q[...] + overlap * update
    head_out = rms_rows(readout, head_gain_ref[...]).astype(jnp.bfloat16)
    copies[5].wait()
    partial = jnp.dot(head_out, out_weight_v[...], preferred_element_type=jnp.float32)
    partial = partial.astype(jnp.bfloat16)
    for copy_number in range(partial_ref.shape[0]):
        partial_ref[copy_number] = partial
    key_unit_ref[...] = key_unit
    update_ref[...] = update
    keep_ref[...] = jnp.broadcast_to(keep, keep_ref.shape)


def state_kernel(
    parity_ref,
    key_unit_ref,
    update_ref,
    keep_ref,
    routes_ref,
    weights_ref,
    state_hbm,
    gate_hbm,
    up_hbm,
    down_hbm,
    next_hbm,
    packed_hbm,
    dispatch_ref,
    combine_ref,
    state_v,
    next_v,
    sems,
):
    seq_rows = key_unit_ref.shape[0]
    width, hidden = gate_hbm.shape
    half = seq_rows // 2
    spans = [(0, half), (half, seq_rows - half)]
    loads = [
        pltpu.make_async_copy(
            state_hbm.at[pl.ds(at, size)], state_v.at[pl.ds(at, size)], sems.at[i]
        )
        for i, (at, size) in enumerate(spans)
    ]
    stores = [
        pltpu.make_async_copy(
            next_v.at[pl.ds(at, size)], next_hbm.at[pl.ds(at, size)], sems.at[2 + i]
        )
        for i, (at, size) in enumerate(spans)
    ]
    packs = [
        pltpu.make_async_copy(gate_hbm, packed_hbm.at[pl.ds(0, width)], sems.at[4]),
        pltpu.make_async_copy(up_hbm, packed_hbm.at[pl.ds(width, width)], sems.at[5]),
    ] + [
        pltpu.make_async_copy(
            down_hbm.at[:, pl.ds(j * hidden, hidden)],
            packed_hbm.at[pl.ds(2 * width + j * hidden, hidden)],
            sems.at[6 + j],
        )
        for j in range(width // hidden)
    ]
    for copy in loads + packs:
        copy.start()
    routes = routes_ref[...]
    weights = weights_ref[...]
    top_k = routes.shape[1]
    scale = weights / jnp.sum(weights, axis=1, keepdims=True) * ROUTED_SCALE
    expert_iota = lax.broadcasted_iota(jnp.int32, (seq_rows, 128), 1)
    named = jnp.zeros((seq_rows, 128), jnp.float32)
    mix = jnp.zeros((seq_rows, 128), jnp.float32)
    for route in range(top_k):
        hit = expert_iota == routes[:, route : route + 1]
        named = named + jnp.where(hit, 1.0, 0.0)
        mix = mix + jnp.where(hit, scale[:, route : route + 1], 0.0)
    row_a = lax.broadcasted_iota(jnp.int32, (seq_rows, seq_rows), 0)
    row_b = lax.broadcasted_iota(jnp.int32, (seq_rows, seq_rows), 1)
    below = jnp.where(row_b < row_a, 1.0, 0.0)
    earlier = jnp.dot(below, named, preferred_element_type=jnp.float32)
    slot = earlier.astype(jnp.int32)
    dispatch_ref[...] = jnp.where(slot == parity_ref[0], named, 0.0).astype(jnp.bfloat16)
    combine_ref[0] = jnp.where(slot == 0, mix, 0.0)
    combine_ref[1] = jnp.where(slot == 1, mix, 0.0)
    key_cols = columns_of(key_unit_ref[...])
    for part, (at, size) in enumerate(spans):
        loads[part].wait()
        for row in range(at, at + size):
            next_v[row] = (
                keep_ref[row : row + 1, :] * state_v[row]
                + key_cols[:, row : row + 1] * update_ref[row : row + 1, :]
            )
        stores[part].start()
    for copy in stores + packs:
        copy.wait()


def vmem():
    return pl.BlockSpec(memory_space=pltpu.VMEM)


def smem():
    return pl.BlockSpec(memory_space=pltpu.SMEM)


def anywhere():
    return pl.BlockSpec(memory_space=pl.ANY)


def per_device(
    tokens,
    delta_state,
    mixer_gain,
    query_weight,
    key_weight,
    value_weight,
    write_weight,
    decay_weight,
    decay_rate,
    decay_bias,
    head_gain,
    out_weight,
    channel_gain,
    routes,
    route_weights,
    expert_gate,
    expert_up,
    expert_down,
    shared_gate,
    shared_up,
    shared_down,
):
    seq_rows, model_width = tokens.shape
    head_dim = delta_state.shape[2]
    tp_count = lax.axis_size("tp")
    ep_count = lax.axis_size("ep")
    share_width = model_width // tp_count
    hidden = expert_gate.shape[2]
    tp_index = lax.axis_index("tp")
    parity = (tp_index % 2).astype(jnp.int32).reshape(1)
    f32, bf16 = jnp.float32, jnp.bfloat16
    state = delta_state.reshape(seq_rows, head_dim, head_dim)
    small = jax.ShapeDtypeStruct((seq_rows, head_dim), f32)
    partials, key_unit, update, keep = pl.pallas_call(
        mixer_kernel,
        out_shape=[
            jax.ShapeDtypeStruct((tp_count, seq_rows, model_width), bf16),
            small,
            small,
            small,
        ],
        in_specs=[vmem()] * 5 + [smem()] * 2 + [anywhere()] * 5,
        out_specs=[vmem()] * 4,
        scratch_shapes=[
            pltpu.VMEM((model_width, head_dim), bf16),
            pltpu.VMEM((model_width, head_dim), bf16),
            pltpu.VMEM((model_width, head_dim), bf16),
            pltpu.VMEM((seq_rows, head_dim, head_dim), f32),
            pltpu.VMEM((head_dim, model_width), bf16),
            pltpu.VMEM((seq_rows, head_dim), f32),
            pltpu.VMEM((seq_rows, head_dim), f32),
            pltpu.SemaphoreType.DMA((6,)),
        ],
    )(
        tokens,
        mixer_gain.reshape(1, model_width),
        write_weight.reshape(1, model_width),
        decay_weight.reshape(1, model_width),
        head_gain.reshape(1, head_dim),
        decay_rate,
        decay_bias,
        query_weight,
        key_weight,
        value_weight,
        state,
        out_weight,
    )
    gathered = lax.all_to_all(partials, "tp", 0, 0, tiled=True)
    next_state, packed, dispatch, combine = pl.pallas_call(
        state_kernel,
        out_shape=[
            jax.ShapeDtypeStruct((seq_rows, head_dim, head_dim), f32),
            jax.ShapeDtypeStruct((3 * model_width, hidden), bf16),
            jax.ShapeDtypeStruct((seq_rows, ep_count), bf16),
            jax.ShapeDtypeStruct((2, seq_rows, ep_count), f32),
        ],
        in_specs=[smem()] + [vmem()] * 5 + [anywhere()] * 4,
        out_specs=[anywhere()] * 2 + [vmem()] * 2,
        scratch_shapes=[
            pltpu.VMEM((seq_rows, head_dim, head_dim), f32),
            pltpu.VMEM((seq_rows, head_dim, head_dim), f32),
            pltpu.SemaphoreType.DMA((6 + model_width // hidden,)),
        ],
    )(
        parity,
        key_unit,
        update,
        keep,
        routes,
        route_weights,
        state,
        expert_gate[0],
        expert_up[0],
        expert_down[0],
    )
    other = lax.ppermute(packed, "tp", [(i, i ^ 1) for i in range(tp_count)])
    mixer_out = jnp.sum(gathered.astype(f32), axis=0).astype(bf16)
    residual = (tokens.astype(f32) + mixer_out.astype(f32)).astype(bf16)
    expert_input = rms_rows(residual.astype(f32), channel_gain).astype(bf16)
    outgoing = lax.dot_general(
        dispatch, expert_input, (((0,), (0,)), ((), ())), preferred_element_type=f32
    ).astype(bf16)
    received = lax.all_to_all(
        outgoing.reshape(ep_count, 2, model_width // 2), "ep", 0, 0, tiled=True
    )
    shared_act = (
        jax.nn.silu(jnp.dot(expert_input, shared_gate, preferred_element_type=f32))
        * jnp.dot(expert_input, shared_up, preferred_element_type=f32)
    ).astype(bf16)
    shared_partial = jnp.dot(shared_act, shared_down, preferred_element_type=f32).astype(bf16)
    rows = received.reshape(ep_count, model_width)
    down_part = jnp.zeros((ep_count, model_width), f32)
    for pack in (packed, other):
        gate_val = jnp.dot(rows, pack[:model_width], preferred_element_type=f32)
        up_val = jnp.dot(rows, pack[model_width : 2 * model_width], preferred_element_type=f32)
        hidden_act = (jax.nn.silu(gate_val) * up_val).astype(bf16)
        down = pack[2 * model_width :].reshape(model_width // hidden, hidden, hidden)
        down_part = down_part + jnp.einsum(
            "rf,jfd->rjd", hidden_act, down, preferred_element_type=f32
        ).reshape(ep_count, model_width)
    both = jnp.concatenate([down_part.astype(bf16), shared_partial], axis=0)
    blocks = both.reshape(ep_count + seq_rows, tp_count, share_width).transpose(1, 0, 2)
    parts = lax.all_to_all(blocks, "tp", 0, 0, tiled=True).astype(f32)
    expert_share = jnp.stack(
        [parts[0, :ep_count] + parts[2, :ep_count], parts[1, :ep_count] + parts[3, :ep_count]],
        axis=1,
    ).astype(bf16)
    shared_out = jnp.sum(parts[:, ep_count:], axis=0).astype(bf16)
    returned = lax.all_to_all(expert_share, "ep", 0, 0, tiled=True)
    routed = jnp.einsum(
        "cse,ecd->sd", combine, returned.astype(f32), precision=lax.Precision.HIGHEST
    )
    residual_share = lax.dynamic_slice_in_dim(residual, tp_index * share_width, share_width, 1)
    layer_out = (residual_share.astype(f32) + routed + shared_out.astype(f32)).astype(bf16)
    return (layer_out, next_state.reshape(delta_state.shape))


def solution(mesh):
    return jax.shard_map(
        per_device,
        mesh=mesh,
        in_specs=(
            P("ep", None),
            P("ep", "tp", None, None),
            P(),
            P(None, "tp"),
            P(None, "tp"),
            P(None, "tp"),
            P(None, "tp"),
            P(None, "tp"),
            P("tp"),
            P("tp"),
            P(),
            P("tp", None),
            P(),
            P("ep", None),
            P("ep", None),
            P("ep", None, "tp"),
            P("ep", None, "tp"),
            P("ep", "tp", None),
            P(None, "tp"),
            P(None, "tp"),
            P("tp", None),
        ),
        out_specs=(P("ep", "tp"), P("ep", "tp", None, None)),
        check_vma=False,
    )
```

time: 108 us -> 122 us (1.13)
  Pallas kernels: 0 us -> 30.6 us
  blocking collectives: 0 us -> 9.54 us
  matrix products: 11.1 us -> 3.57 us
  starting transfers between devices: 49.7 us -> 42.9 us
  waiting for transfers between devices: 34.8 us -> 28.2 us
  other arithmetic: 4.48 us -> 0.3 us
    pallas_call x0 -> x2, Pallas kernels: none -> 30.6 us  [the longest x1 26.4 us: per_device(): pl.pallas_call(state_kernel, out_shape=[jax.ShapeDtypeStruct((seq_rows, h...]
    all_to_all x0 -> x1, blocking collectives: none -> 9.54 us  [per_device(): parts = lax.all_to_all(blocks, 'tp', 0, 0, tiled=True).astype(f32)]
    all_to_all x4 -> x3, waiting for transfers between devices: 31.1 us -> 23.4 us  [the longest x1 12.6 us: per_device(): returned = lax.all_to_all(expert_share, 'ep', 0, 0, tiled=True)]
    dot_general x16 -> x8, matrix products: 11.1 us -> 3.57 us  [the longest x1 1.01 us: per_device(): lax.dot_general(dispatch, expert_input, (((0,), (0,)), ((), ())), preferr...]
    ppermute x3 -> x1, starting transfers between devices: 7.48 us -> 3.66 us  [per_device(): other = lax.ppermute(packed, 'tp', [(i, i ^ 1) for i in range(tp_count)])]
    all_to_all x4 -> x3, starting transfers between devices: 42.2 us -> 39.2 us  [the longest x1 17.9 us: per_device(): lax.all_to_all(outgoing.reshape(ep_count, 2, model_width // 2), 'ep', 0,...]
    reshape x2 -> x0, other arithmetic: 1.64 us -> none  [the longest x1 0.86 us: per_device(): homeward = down_part.astype(jnp.bfloat16).reshape(ep_count, 1, model_width)]
    ppermute x3 -> x1, waiting for transfers between devices: 3.72 us -> 4.81 us  [per_device(): other = lax.ppermute(packed, 'tp', [(i, i ^ 1) for i in range(tp_count)])]
  transfers between devices with their start and end apart: 7 -> 4, of which waited for: 5 -> 3; matrix products, arithmetic and copies ran while one was open for 2% -> 2% of each run, Pallas kernels for 0% -> 22%
where the time goes in v2:
time: 122 us; the launch traced here: 121 us
  starting transfers between devices  42.9 us (35%)
  Pallas kernels  30.6 us (25%)
  waiting for transfers between devices  28.2 us (23%)
  blocking collectives  9.54 us (8%)
  local copies, waits for them, and re-layouts  3.66 us (3%)
  matrix products  3.57 us (3%)
  between operations  2.25 us (2%)
    pallas_call x1, Pallas kernels, per_device(): pl.pallas_call(state_kernel, out_shape=[jax.ShapeDtypeStruct((seq_rows, h...  26.4 us
    all_to_all x1, starting transfers between devices, per_device(): lax.all_to_all(outgoing.reshape(ep_count, 2, model_width // 2), 'ep', 0,...  17.9 us
    all_to_all x1, starting transfers between devices, per_device(): returned = lax.all_to_all(expert_share, 'ep', 0, 0, tiled=True)  16.5 us
    all_to_all x1, waiting for transfers between devices, per_device(): returned = lax.all_to_all(expert_share, 'ep', 0, 0, tiled=True)  12.6 us
    all_to_all x1, waiting for transfers between devices, per_device(): lax.all_to_all(outgoing.reshape(ep_count, 2, model_width // 2), 'ep', 0,...  10.8 us
    all_to_all x1, blocking collectives, per_device(): parts = lax.all_to_all(blocks, 'tp', 0, 0, tiled=True).astype(f32)  9.54 us
    all_to_all x1, starting transfers between devices, per_device(): gathered = lax.all_to_all(partials, 'tp', 0, 0, tiled=True)  4.84 us
    ppermute x1, waiting for transfers between devices, per_device(): other = lax.ppermute(packed, 'tp', [(i, i ^ 1) for i in range(tp_count)])  4.81 us
  transfers between devices with their start and end apart: 4, of which 3 were waited for; matrix products, arithmetic and copies ran while one was open for 2% of the time, Pallas kernels for 22%

profile of v2, /device:TPU:1, one launch (start us, length us, event | category | flops | bytes accessed | tf_op | source)
XLA Modules:
  0.0 121.0 jit_solution(15332490840743184257)
XLA Ops:
  2.0 4.1 %shard_map.212 = (bf16[4,18,1024]{2,1,0:T(8,128)(2,1)}, f32[18,128]{1,0:T(8,128)}, f32[18,128]{1,0:T(8,128)}, f32[18,128]{1,0:T(8,128)}) custom-call(bf16[18,1024]{1,0:T(8,128)(2,1)} %tokens_ref.1, f32[1,1024]{1,0:T(1,128)} %bitcast.63, bf16[1,1024]{1,0:T(2,128)(2,1)} %bitcast.64, bf16[1,1024]{1,0:T(2,128)(2,1)} %bitcast.65, f32[1,128]{1,0:T(1,128)} %bitcast.66, ...), custom_call_target="tpu_custom_call" | custom-call | tf_op jit(solution)/shard_map/pallas_call | solution.py:243
  6.1 4.8 %all-to-all-start = ((bf16[4,18,1024]{2,1,0:T(8,128)(2,1)}), bf16[4,18,1024]{2,1,0:T(8,128)(2,1)S(1)}, u32[]{:S(2)}, u32[]{:S(2)}) async-start(bf16[4,18,1024]{2,1,0:T(8,128)(2,1)} %get-tuple-element.10), calls=%async_computation | async-start | bytes 393216 | tf_op jit(solution)/shard_map/all_to_all | solution.py:277
  11.0 0.7 copy.41.routes_ref
  11.7 0.7 copy.42.weights_ref
  12.4 26.4 %shard_map.213 = (f32[18,128,128]{2,1,0:T(8,128)}, bf16[3072,128]{1,0:T(8,128)(2,1)}, bf16[18,128]{1,0:T(8,128)(2,1)}, f32[2,18,128]{2,1,0:T(8,128)}) custom-call(s32[1]{0:T(128)} %bitcast.5.parity_ref, f32[18,128]{1,0:T(8,128)} %get-tuple-element.11.key_unit_ref, f32[18,128]{1,0:T(8,128)} %get-tuple-element.12.update_ref, ...), custom_call_target="tpu_custom_call" | custom-call | tf_op jit(solution)/shard_map/pallas_call | solution.py:278
  39.1 1.0 convolution_convert_fusion
  40.1 0.9 reshape.97
  41.0 17.9 %all-to-all-start.1 = ((bf16[128,2,512]{2,1,0:T(2,128)(2,1)}), bf16[128,2,512]{2,1,0:T(2,128)(2,1)S(1)}, u32[]{:S(2)}, u32[]{:S(2)}) async-start(bf16[128,2,512]{2,1,0:T(2,128)(2,1)} %reshape.97), calls=%async_computation.1 | async-start | bytes 524288 | tf_op jit(solution)/shard_map/all_to_all | solution.py:312
  58.9 3.7 %collective-permute-start = (bf16[3072,128]{1,0:T(8,128)(2,1)S(1)}, bf16[3072,128]{1,0:T(8,128)(2,1)S(1)}, u32[]{:S(2)}, u32[]{:S(2)}) collective-permute-start(bf16[3072,128]{1,0:T(8,128)(2,1)S(1)} %copy-done.1), channel_id=1, source_target_pairs={{0,1},{1,0},{2,3},{3,2},{4,5},{5,4},{6,7},{7,6},{8,9},{9,8},{10,11... | collective-permute-start | bytes 2359304 | tf_op jit(solution)/shard_map/ppermute | solution.py:305
  62.5 0.2 copy.43
  62.7 0.2 fusion.45
  63.0 0.3 convolution_convert_fusion.1
  63.3 10.8 %all-to-all-done.1 = bf16[128,2,512]{2,1,0:T(2,128)(2,1)S(1)} async-done(((bf16[128,2,512]{2,1,0:T(2,128)(2,1)}), bf16[128,2,512]{2,1,0:T(2,128)(2,1)S(1)}, u32[]{:S(2)}, u32[]{:S(2)}) %all-to-all-start.1) | async-done | bytes 262176 | tf_op jit(solution)/shard_map/all_to_all | solution.py:312
  74.1 0.2 fusion.13
  74.3 0.4 fusion.2
  74.7 4.8 %collective-permute-done = bf16[3072,128]{1,0:T(8,128)(2,1)S(1)} collective-permute-done((bf16[3072,128]{1,0:T(8,128)(2,1)S(1)}, bf16[3072,128]{1,0:T(8,128)(2,1)S(1)}, u32[]{:S(2)}, u32[]{:S(2)}) %collective-permute-start) | collective-permute-done | bytes 786464 | tf_op jit(solution)/shard_map/ppermute | solution.py:305
  79.5 0.2 copy.44
  79.7 0.2 fusion.7
  80.0 0.4 fusion
  80.6 9.5 %all_to_all.20 = bf16[4,146,256]{2,1,0:T(8,128)(2,1)S(1)} all-to-all(bf16[4,146,256]{2,1,0:T(8,128)(2,1)S(1)} %bitcast.54), channel_id=1, replica_groups=mesh['ep'=128,'tp'=4] {'tp'}, dimensions={0} | all-to-all | bytes 598016 | tf_op jit(solution)/shard_map/all_to_all | solution.py:332
  90.2 0.8 copy.46
  91.0 16.5 %all-to-all-start.3 = ((bf16[128,2,256]{2,1,0:T(2,128)(2,1)}), bf16[128,2,256]{2,1,0:T(2,128)(2,1)S(1)}, u32[]{:S(2)}, u32[]{:S(2)}) async-start(bf16[128,2,256]{2,1,0:T(2,128)(2,1)} %copy.46), calls=%async_computation.3 | async-start | bytes 262144 | tf_op jit(solution)/shard_map/all_to_all | solution.py:338
  107.6 12.6 %all-to-all-done.3 = bf16[128,2,256]{2,1,0:T(2,128)(2,1)S(1)} async-done(((bf16[128,2,256]{2,1,0:T(2,128)(2,1)}), bf16[128,2,256]{2,1,0:T(2,128)(2,1)S(1)}, u32[]{:S(2)}, u32[]{:S(2)}) %all-to-all-start.3) | async-done | bytes 131104 | tf_op jit(solution)/shard_map/all_to_all | solution.py:338
  120.2 0.8 fusion.5
  (32 shorter events, 0.6 us)
Async XLA Ops:
  0.6 62.3 %copy-start = (bf16[128,1024]{1,0:T(8,128)(2,1)S(1)}, bf16[128,1024]{1,0:T(8,128)(2,1)}, u32[]{:S(2)}) copy-start(bf16[128,1024]{1,0:T(8,128)(2,1)} %param.41) | copy-start | bytes 786436
  2.0 9.0 %copy-start.7 = (s32[18,6]{0,1:T(8,128)S(1)}, s32[18,6]{0,1:T(8,128)}, u32[]{:S(2)}) copy-start(s32[18,6]{0,1:T(8,128)} %param.34) | copy-start | bytes 1300
  2.0 9.7 %copy-start.8 = (f32[18,6]{0,1:T(8,128)S(1)}, f32[18,6]{0,1:T(8,128)}, u32[]{:S(2)}) copy-start(f32[18,6]{0,1:T(8,128)} %param.35) | copy-start | bytes 1300
  6.1 32.7 %all-to-all-start = ((bf16[4,18,1024]{2,1,0:T(8,128)(2,1)}), bf16[4,18,1024]{2,1,0:T(8,128)(2,1)S(1)}, u32[]{:S(2)}, u32[]{:S(2)}) async-start(bf16[4,18,1024]{2,1,0:T(8,128)(2,1)} %get-tuple-element.10), calls=%async_computation | async-start | bytes 393216 | tf_op jit(solution)/shard_map/all_to_all | solution.py:277
  11.0 27.9 %copy-start.4 = (bf16[18,1024]{1,0:T(8,128)(2,1)S(1)}, bf16[18,1024]{1,0:T(8,128)(2,1)}, u32[]{:S(2)}) copy-start(bf16[18,1024]{1,0:T(8,128)(2,1)} %tokens_ref.1) | copy-start | bytes 110596
  12.4 26.7 %copy-start.5 = (f32[1024]{0:T(1024)S(1)}, f32[1024]{0:T(1024)}, u32[]{:S(2)}) copy-start(f32[1024]{0:T(1024)} %param.33) | copy-start | bytes 12292
  38.8 20.0 %copy-start.1 = (bf16[3072,128]{1,0:T(8,128)(2,1)S(1)}, bf16[3072,128]{1,0:T(8,128)(2,1)}, u32[]{:S(2)}) copy-start(bf16[3072,128]{1,0:T(8,128)(2,1)} %get-tuple-element.16) | copy-start | bytes 2359300
  39.0 23.7 %copy-start.2 = (bf16[1024,128]{1,0:T(8,128)(2,1)S(1)}, bf16[1024,128]{1,0:T(8,128)(2,1)}, u32[]{:S(2)}) copy-start(bf16[1024,128]{1,0:T(8,128)(2,1)} %param.39) | copy-start | bytes 786436
  40.1 22.9 %copy-start.3 = (bf16[1024,128]{1,0:T(8,128)(2,1)S(1)}, bf16[1024,128]{1,0:T(8,128)(2,1)}, u32[]{:S(2)}) copy-start(bf16[1024,128]{1,0:T(8,128)(2,1)} %param.40) | copy-start | bytes 786436
  41.0 33.1 %all-to-all-start.1 = ((bf16[128,2,512]{2,1,0:T(2,128)(2,1)}), bf16[128,2,512]{2,1,0:T(2,128)(2,1)S(1)}, u32[]{:S(2)}, u32[]{:S(2)}) async-start(bf16[128,2,512]{2,1,0:T(2,128)(2,1)} %reshape.97), calls=%async_computation.1 | async-start | bytes 524288 | tf_op jit(solution)/shard_map/all_to_all | solution.py:312
  58.9 20.7 %collective-permute-start = (bf16[3072,128]{1,0:T(8,128)(2,1)S(1)}, bf16[3072,128]{1,0:T(8,128)(2,1)S(1)}, u32[]{:S(2)}, u32[]{:S(2)}) collective-permute-start(bf16[3072,128]{1,0:T(8,128)(2,1)S(1)} %copy-done.1), channel_id=1, source_target_pairs={{0,1},{1,0},{2,3},{3,2},{4,5},{5,4},{6,7},{7,6},{8,9},{9,8},{10,11... | collective-permute-start | bytes 2359304 | tf_op jit(solution)/shard_map/ppermute | solution.py:305
  90.1 30.1 %copy-start.6 = (f32[2,18,128]{2,1,0:T(8,128)S(1)}, f32[2,18,128]{2,1,0:T(8,128)}, u32[]{:S(2)}) copy-start(f32[2,18,128]{2,1,0:T(8,128)} %get-tuple-element.14) | copy-start | bytes 55300
  91.0 29.2 %all-to-all-start.3 = ((bf16[128,2,256]{2,1,0:T(2,128)(2,1)}), bf16[128,2,256]{2,1,0:T(2,128)(2,1)S(1)}, u32[]{:S(2)}, u32[]{:S(2)}) async-start(bf16[128,2,256]{2,1,0:T(2,128)(2,1)} %copy.46), calls=%async_computation.3 | async-start | bytes 262144 | tf_op jit(solution)/shard_map/all_to_all | solution.py:338

commit v3 on v2

--- a/solution.py
+++ b/solution.py
@@ -114,57 +114,36 @@
     keep_ref[...] = jnp.broadcast_to(keep, keep_ref.shape)
 
 
-def state_kernel(
+def tables_kernel(
     parity_ref,
-    key_unit_ref,
-    update_ref,
-    keep_ref,
     routes_ref,
     weights_ref,
-    state_hbm,
     gate_hbm,
     up_hbm,
     down_hbm,
-    next_hbm,
     packed_hbm,
     dispatch_ref,
     combine_ref,
-    state_v,
-    next_v,
+    packed_v,
     sems,
 ):
-    seq_rows = key_unit_ref.shape[0]
     width, hidden = gate_hbm.shape
-    half = seq_rows // 2
-    spans = [(0, half), (half, seq_rows - half)]
     loads = [
-        pltpu.make_async_copy(
-            state_hbm.at[pl.ds(at, size)], state_v.at[pl.ds(at, size)], sems.at[i]
-        )
-        for i, (at, size) in enumerate(spans)
-    ]
-    stores = [
-        pltpu.make_async_copy(
-            next_v.at[pl.ds(at, size)], next_hbm.at[pl.ds(at, size)], sems.at[2 + i]
-        )
-        for i, (at, size) in enumerate(spans)
-    ]
-    packs = [
-        pltpu.make_async_copy(gate_hbm, packed_hbm.at[pl.ds(0, width)], sems.at[4]),
-        pltpu.make_async_copy(up_hbm, packed_hbm.at[pl.ds(width, width)], sems.at[5]),
+        pltpu.make_async_copy(gate_hbm, packed_v.at[pl.ds(0, width)], sems.at[0]),
+        pltpu.make_async_copy(up_hbm, packed_v.at[pl.ds(width, width)], sems.at[1]),
     ] + [
         pltpu.make_async_copy(
             down_hbm.at[:, pl.ds(j * hidden, hidden)],
-            packed_hbm.at[pl.ds(2 * width + j * hidden, hidden)],
-            sems.at[6 + j],
+            packed_v.at[pl.ds(2 * width + j * hidden, hidden)],
+            sems.at[2 + j],
         )
         for j in range(width // hidden)
     ]
-    for copy in loads + packs:
+    for copy in loads:
         copy.start()
-    routes = routes_ref[...]
-    weights = weights_ref[...]
-    top_k = routes.shape[1]
+    top_k, seq_rows = routes_ref.shape
+    routes = columns_of(routes_ref[...].astype(jnp.float32))[:seq_rows].astype(jnp.int32)
+    weights = columns_of(weights_ref[...])[:seq_rows]
     scale = weights / jnp.sum(weights, axis=1, keepdims=True) * ROUTED_SCALE
     expert_iota = lax.broadcasted_iota(jnp.int32, (seq_rows, 128), 1)
     named = jnp.zeros((seq_rows, 128), jnp.float32)
@@ -181,6 +160,40 @@
     dispatch_ref[...] = jnp.where(slot == parity_ref[0], named, 0.0).astype(jnp.bfloat16)
     combine_ref[0] = jnp.where(slot == 0, mix, 0.0)
     combine_ref[1] = jnp.where(slot == 1, mix, 0.0)
+    for copy in loads:
+        copy.wait()
+    store = pltpu.make_async_copy(packed_v, packed_hbm, sems.at[0])
+    store.start()
+    store.wait()
+
+
+def state_kernel(
+    key_unit_ref,
+    update_ref,
+    keep_ref,
+    state_hbm,
+    next_hbm,
+    state_v,
+    next_v,
+    sems,
+):
+    seq_rows = key_unit_ref.shape[0]
+    half = seq_rows // 2
+    spans = [(0, half), (half, seq_rows - half)]
+    loads = [
+        pltpu.make_async_copy(
+            state_hbm.at[pl.ds(at, size)], state_v.at[pl.ds(at, size)], sems.at[i]
+        )
+        for i, (at, size) in enumerate(spans)
+    ]
+    stores = [
+        pltpu.make_async_copy(
+            next_v.at[pl.ds(at, size)], next_hbm.at[pl.ds(at, size)], sems.at[2 + i]
+        )
+        for i, (at, size) in enumerate(spans)
+    ]
+    for copy in loads:
+        copy.start()
     key_cols = columns_of(key_unit_ref[...])
     for part, (at, size) in enumerate(spans):
         loads[part].wait()
@@ -190,7 +203,7 @@
                 + key_cols[:, row : row + 1] * update_ref[row : row + 1, :]
             )
         stores[part].start()
-    for copy in stores + packs:
+    for copy in stores:
         copy.wait()
 
 
@@ -275,33 +288,38 @@
         out_weight,
     )
     gathered = lax.all_to_all(partials, "tp", 0, 0, tiled=True)
-    next_state, packed, dispatch, combine = pl.pallas_call(
-        state_kernel,
+    packed, dispatch, combine = pl.pallas_call(
+        tables_kernel,
         out_shape=[
-            jax.ShapeDtypeStruct((seq_rows, head_dim, head_dim), f32),
             jax.ShapeDtypeStruct((3 * model_width, hidden), bf16),
             jax.ShapeDtypeStruct((seq_rows, ep_count), bf16),
             jax.ShapeDtypeStruct((2, seq_rows, ep_count), f32),
         ],
-        in_specs=[smem()] + [vmem()] * 5 + [anywhere()] * 4,
-        out_specs=[anywhere()] * 2 + [vmem()] * 2,
+        in_specs=[smem()] + [vmem()] * 2 + [anywhere()] * 3,
+        out_specs=[anywhere()] + [vmem()] * 2,
+        scratch_shapes=[
+            pltpu.VMEM((3 * model_width, hidden), bf16),
+            pltpu.SemaphoreType.DMA((2 + model_width // hidden,)),
+        ],
+    )(
+        parity,
+        routes.T,
+        route_weights.T,
+        expert_gate[0],
+        expert_up[0],
+        expert_down[0],
+    )
+    next_state = pl.pallas_call(
+        state_kernel,
+        out_shape=jax.ShapeDtypeStruct((seq_rows, head_dim, head_dim), f32),
+        in_specs=[vmem()] * 3 + [anywhere()],
+        out_specs=anywhere(),
         scratch_shapes=[
             pltpu.VMEM((seq_rows, head_dim, head_dim), f32),
             pltpu.VMEM((seq_rows, head_dim, head_dim), f32),
-            pltpu.SemaphoreType.DMA((6 + model_width // hidden,)),
-        ],
-    )(
-        parity,
-        key_unit,
-        update,
-        keep,
-        routes,
-        route_weights,
-        state,
-        expert_gate[0],
-        expert_up[0],
-        expert_down[0],
-    )
+            pltpu.SemaphoreType.DMA((4,)),
+        ],
+    )(key_unit, update, keep, state)
     other = lax.ppermute(packed, "tp", [(i, i ^ 1) for i in range(tp_count)])
     mixer_out = jnp.sum(gathered.astype(f32), axis=0).astype(bf16)
     residual = (tokens.astype(f32) + mixer_out.astype(f32)).astype(bf16)

time: 122 us -> 98.1 us (0.80)
  Pallas kernels: 30.6 us -> 10.6 us
  blocking collectives: 9.54 us -> 8.16 us
  local copies, waits for them, and re-layouts: 3.66 us -> 2.3 us
    pallas_call x1 -> x2, Pallas kernels: 26.4 us -> 6.44 us  [the longest x1 3.32 us: per_device(): pl.pallas_call(tables_kernel, out_shape=[jax.ShapeDtypeStruct((3 * model_...]
    all_to_all x1, waiting for transfers between devices: 12.6 us -> 9.55 us  [per_device(): returned = lax.all_to_all(expert_share, 'ep', 0, 0, tiled=True)]
    all_to_all x1, waiting for transfers between devices: 0.01 us -> 1.84 us  [per_device(): gathered = lax.all_to_all(partials, 'tp', 0, 0, tiled=True)]
    ppermute x1, starting transfers between devices: 3.66 us -> 2.19 us  [per_device(): other = lax.ppermute(packed, 'tp', [(i, i ^ 1) for i in range(tp_count)])]
    all_to_all x1, waiting for transfers between devices: 10.8 us -> 12.2 us  [per_device(): lax.all_to_all(outgoing.reshape(ep_count, 2, model_width // 2), 'ep', 0,...]
    all_to_all x1, blocking collectives: 9.54 us -> 8.16 us  [per_device(): parts = lax.all_to_all(blocks, 'tp', 0, 0, tiled=True).astype(f32)]
    unnamed x21 -> x15, local copies, waits for them, and re-layouts: 1.45 us -> 0.07 us
  transfers between devices with their start and end apart: 4 -> 4, of which waited for: 3 -> 4; matrix products, arithmetic and copies ran while one was open for 2% -> 1% of each run, Pallas kernels for 22% -> 7%
where the time goes in v3:
time: 98.1 us; the launch traced here: 97.4 us
  starting transfers between devices  42.4 us (43%)
  waiting for transfers between devices  27.9 us (28%)
  Pallas kernels  10.6 us (11%)
  blocking collectives  8.16 us (8%)
  matrix products  3.56 us (4%)
  local copies, waits for them, and re-layouts  2.3 us (2%)
  between operations  2.25 us (2%)
    all_to_all x1, starting transfers between devices, per_device(): lax.all_to_all(outgoing.reshape(ep_count, 2, model_width // 2), 'ep', 0,...  19 us
    all_to_all x1, starting transfers between devices, per_device(): returned = lax.all_to_all(expert_share, 'ep', 0, 0, tiled=True)  16.2 us
    all_to_all x1, waiting for transfers between devices, per_device(): lax.all_to_all(outgoing.reshape(ep_count, 2, model_width // 2), 'ep', 0,...  12.2 us
    all_to_all x1, waiting for transfers between devices, per_device(): returned = lax.all_to_all(expert_share, 'ep', 0, 0, tiled=True)  9.55 us
    all_to_all x1, blocking collectives, per_device(): parts = lax.all_to_all(blocks, 'tp', 0, 0, tiled=True).astype(f32)  8.16 us
    all_to_all x1, starting transfers between devices, per_device(): gathered = lax.all_to_all(partials, 'tp', 0, 0, tiled=True)  4.97 us
    ppermute x1, waiting for transfers between devices, per_device(): other = lax.ppermute(packed, 'tp', [(i, i ^ 1) for i in range(tp_count)])  4.23 us
    pallas_call x1, Pallas kernels, per_device(): pl.pallas_call(mixer_kernel, out_shape=[jax.ShapeDtypeStruct((tp_count, s...  4.13 us
  transfers between devices with their start and end apart: 4, of which 4 were waited for; matrix products, arithmetic and copies ran while one was open for 1% of the time, Pallas kernels for 7%

profile of v3, /device:TPU:1, one launch (start us, length us, event | category | flops | bytes accessed | tf_op | source)
XLA Modules:
  0.0 97.4 jit_solution(15559062439469653159)
XLA Ops:
  2.0 4.1 %shard_map.212 = (bf16[4,18,1024]{2,1,0:T(8,128)(2,1)}, f32[18,128]{1,0:T(8,128)}, f32[18,128]{1,0:T(8,128)}, f32[18,128]{1,0:T(8,128)}) custom-call(bf16[18,1024]{1,0:T(8,128)(2,1)} %tokens_ref.1, f32[1,1024]{1,0:T(1,128)} %bitcast.66, bf16[1,1024]{1,0:T(2,128)(2,1)} %bitcast.67, bf16[1,1024]{1,0:T(2,128)(2,1)} %bitcast.68, f32[1,128]{1,0:T(1,128)} %bitcast.71, ...), custom_call_target="tpu_custom_call" | custom-call | tf_op jit(solution)/shard_map/pallas_call | solution.py:256
  6.1 5.0 %all-to-all-start = ((bf16[4,18,1024]{2,1,0:T(8,128)(2,1)}), bf16[4,18,1024]{2,1,0:T(8,128)(2,1)S(1)}, u32[]{:S(2)}, u32[]{:S(2)}) async-start(bf16[4,18,1024]{2,1,0:T(8,128)(2,1)} %get-tuple-element.9), calls=%async_computation | async-start | bytes 393216 | tf_op jit(solution)/shard_map/all_to_all | solution.py:290
  11.1 3.3 %shard_map.213 = (bf16[3072,128]{1,0:T(8,128)(2,1)}, bf16[18,128]{1,0:T(8,128)(2,1)}, f32[2,18,128]{2,1,0:T(8,128)}) custom-call(s32[1]{0:T(128)} %bitcast.5.parity_ref, s32[6,18]{1,0:T(8,128)} %bitcast.69, f32[6,18]{1,0:T(8,128)} %bitcast.70, bf16[1024,128]{1,0:T(8,128)(2,1)} %bitcast.63, bf16[1024,128]{1,0:T(8,128)(2,1)} %bitcast.64, ...), custom_call_target="tpu_custom_call" | custom-call | tf_op jit(solution)/shard_map/pallas_call | solution.py:291
  14.5 1.8 %all-to-all-done = bf16[4,18,1024]{2,1,0:T(8,128)(2,1)S(1)} async-done(((bf16[4,18,1024]{2,1,0:T(8,128)(2,1)}), bf16[4,18,1024]{2,1,0:T(8,128)(2,1)S(1)}, u32[]{:S(2)}, u32[]{:S(2)}) %all-to-all-start) | async-done | bytes 147488 | tf_op jit(solution)/shard_map/all_to_all | solution.py:290
  16.5 1.0 %convolution_convert_fusion = bf16[128,1024]{1,0:T(8,128)(2,1)S(1)} fusion(bf16[18,128]{1,0:T(8,128)(2,1)} %get-tuple-element.11, bf16[18,1024]{1,0:T(8,128)(2,1)S(1)} %get-tuple-element.25, f32[1024]{0:T(1024)S(1)} %copy-done.5, f32[18]{0:T(128)S(1)} %add_rsqrt_fusion), kind=kOutput, calls=%fused_computation.2 | convolution fusion | flops 4923392 | bytes 307784 | tf_op jit(solution)/shard_map/dot_general | solution.py:327
  17.5 0.9 reshape.97
  18.4 19.0 %all-to-all-start.1 = ((bf16[128,2,512]{2,1,0:T(2,128)(2,1)}), bf16[128,2,512]{2,1,0:T(2,128)(2,1)S(1)}, u32[]{:S(2)}, u32[]{:S(2)}) async-start(bf16[128,2,512]{2,1,0:T(2,128)(2,1)} %reshape.97), calls=%async_computation.1 | async-start | bytes 524288 | tf_op jit(solution)/shard_map/all_to_all | solution.py:330
  37.4 2.2 %collective-permute-start = (bf16[3072,128]{1,0:T(8,128)(2,1)S(1)}, bf16[3072,128]{1,0:T(8,128)(2,1)S(1)}, u32[]{:S(2)}, u32[]{:S(2)}) collective-permute-start(bf16[3072,128]{1,0:T(8,128)(2,1)S(1)} %copy-done.1), channel_id=1, source_target_pairs={{0,1},{1,0},{2,3},{3,2},{4,5},{5,4},{6,7},{7,6},{8,9},{9,8},{10,11... | collective-permute-start | bytes 2359304 | tf_op jit(solution)/shard_map/ppermute | solution.py:323
  39.7 0.2 copy.35
  39.9 0.2 fusion.45
  40.1 0.3 convolution_convert_fusion.1
  40.4 12.2 %all-to-all-done.1 = bf16[128,2,512]{2,1,0:T(2,128)(2,1)S(1)} async-done(((bf16[128,2,512]{2,1,0:T(2,128)(2,1)}), bf16[128,2,512]{2,1,0:T(2,128)(2,1)S(1)}, u32[]{:S(2)}, u32[]{:S(2)}) %all-to-all-start.1) | async-done | bytes 262176 | tf_op jit(solution)/shard_map/all_to_all | solution.py:330
  52.7 0.2 fusion.13
  52.9 0.4 fusion.2
  53.3 4.2 %collective-permute-done = bf16[3072,128]{1,0:T(8,128)(2,1)S(1)} collective-permute-done((bf16[3072,128]{1,0:T(8,128)(2,1)S(1)}, bf16[3072,128]{1,0:T(8,128)(2,1)S(1)}, u32[]{:S(2)}, u32[]{:S(2)}) %collective-permute-start) | collective-permute-done | bytes 786464 | tf_op jit(solution)/shard_map/ppermute | solution.py:323
  57.6 0.2 copy.36
  57.8 0.2 fusion.7
  58.0 0.4 fusion
  58.6 8.2 %all_to_all.20 = bf16[4,146,256]{2,1,0:T(8,128)(2,1)S(1)} all-to-all(bf16[4,146,256]{2,1,0:T(8,128)(2,1)S(1)} %bitcast.56), channel_id=1, replica_groups=mesh['ep'=128,'tp'=4] {'tp'}, dimensions={0} | all-to-all | bytes 598016 | tf_op jit(solution)/shard_map/all_to_all | solution.py:350
  66.9 0.8 copy.38
  67.7 16.2 %all-to-all-start.3 = ((bf16[128,2,256]{2,1,0:T(2,128)(2,1)}), bf16[128,2,256]{2,1,0:T(2,128)(2,1)S(1)}, u32[]{:S(2)}, u32[]{:S(2)}) async-start(bf16[128,2,256]{2,1,0:T(2,128)(2,1)} %copy.38), calls=%async_computation.3 | async-start | bytes 262144 | tf_op jit(solution)/shard_map/all_to_all | solution.py:356
  83.9 3.1 %shard_map.214 = f32[18,128,128]{2,1,0:T(8,128)} custom-call(f32[18,128]{1,0:T(8,128)} %get-tuple-element.13.key_unit_ref, f32[18,128]{1,0:T(8,128)} %get-tuple-element.14.update_ref, f32[18,128]{1,0:T(8,128)} %get-tuple-element.15.keep_ref, f32[18,128,128]{2,1,0:T(8,128)} %bitcast.55), custom_call_target="tpu_custom_call" | custom-call | tf_op jit(solution)/shard_map/pallas_call | solution.py:312
  87.1 9.5 %all-to-all-done.3 = bf16[128,2,256]{2,1,0:T(2,128)(2,1)S(1)} async-done(((bf16[128,2,256]{2,1,0:T(2,128)(2,1)}), bf16[128,2,256]{2,1,0:T(2,128)(2,1)S(1)}, u32[]{:S(2)}, u32[]{:S(2)}) %all-to-all-start.3) | async-done | bytes 131104 | tf_op jit(solution)/shard_map/all_to_all | solution.py:356
  96.6 0.8 fusion.5
  (27 shorter events, 0.6 us)
Async XLA Ops:
  0.6 39.4 %copy-start = (bf16[128,1024]{1,0:T(8,128)(2,1)S(1)}, bf16[128,1024]{1,0:T(8,128)(2,1)}, u32[]{:S(2)}) copy-start(bf16[128,1024]{1,0:T(8,128)(2,1)} %param.41) | copy-start | bytes 786436
  6.1 10.2 %copy-start.4 = (bf16[18,1024]{1,0:T(8,128)(2,1)S(1)}, bf16[18,1024]{1,0:T(8,128)(2,1)}, u32[]{:S(2)}) copy-start(bf16[18,1024]{1,0:T(8,128)(2,1)} %tokens_ref.1) | copy-start | bytes 110596
  6.1 10.4 %copy-start.5 = (f32[1024]{0:T(1024)S(1)}, f32[1024]{0:T(1024)}, u32[]{:S(2)}) copy-start(f32[1024]{0:T(1024)} %param.33) | copy-start | bytes 12292
  6.1 10.2 %all-to-all-start = ((bf16[4,18,1024]{2,1,0:T(8,128)(2,1)}), bf16[4,18,1024]{2,1,0:T(8,128)(2,1)S(1)}, u32[]{:S(2)}, u32[]{:S(2)}) async-start(bf16[4,18,1024]{2,1,0:T(8,128)(2,1)} %get-tuple-element.9), calls=%async_computation | async-start | bytes 393216 | tf_op jit(solution)/shard_map/all_to_all | solution.py:290
  14.4 23.0 %copy-start.1 = (bf16[3072,128]{1,0:T(8,128)(2,1)S(1)}, bf16[3072,128]{1,0:T(8,128)(2,1)}, u32[]{:S(2)}) copy-start(bf16[3072,128]{1,0:T(8,128)(2,1)} %get-tuple-element.12) | copy-start | bytes 2359300
  16.5 23.4 %copy-start.2 = (bf16[1024,128]{1,0:T(8,128)(2,1)S(1)}, bf16[1024,128]{1,0:T(8,128)(2,1)}, u32[]{:S(2)}) copy-start(bf16[1024,128]{1,0:T(8,128)(2,1)} %param.39) | copy-start | bytes 786436
  17.5 22.6 %copy-start.3 = (bf16[1024,128]{1,0:T(8,128)(2,1)S(1)}, bf16[1024,128]{1,0:T(8,128)(2,1)}, u32[]{:S(2)}) copy-start(bf16[1024,128]{1,0:T(8,128)(2,1)} %param.40) | copy-start | bytes 786436
  18.4 34.3 %all-to-all-start.1 = ((bf16[128,2,512]{2,1,0:T(2,128)(2,1)}), bf16[128,2,512]{2,1,0:T(2,128)(2,1)S(1)}, u32[]{:S(2)}, u32[]{:S(2)}) async-start(bf16[128,2,512]{2,1,0:T(2,128)(2,1)} %reshape.97), calls=%async_computation.1 | async-start | bytes 524288 | tf_op jit(solution)/shard_map/all_to_all | solution.py:330
  37.4 20.1 %collective-permute-start = (bf16[3072,128]{1,0:T(8,128)(2,1)S(1)}, bf16[3072,128]{1,0:T(8,128)(2,1)S(1)}, u32[]{:S(2)}, u32[]{:S(2)}) collective-permute-start(bf16[3072,128]{1,0:T(8,128)(2,1)S(1)} %copy-done.1), channel_id=1, source_target_pairs={{0,1},{1,0},{2,3},{3,2},{4,5},{5,4},{6,7},{7,6},{8,9},{9,8},{10,11... | collective-permute-start | bytes 2359304 | tf_op jit(solution)/shard_map/ppermute | solution.py:323
  67.7 29.0 %all-to-all-start.3 = ((bf16[128,2,256]{2,1,0:T(2,128)(2,1)}), bf16[128,2,256]{2,1,0:T(2,128)(2,1)S(1)}, u32[]{:S(2)}, u32[]{:S(2)}) async-start(bf16[128,2,256]{2,1,0:T(2,128)(2,1)} %copy.38), calls=%async_computation.3 | async-start | bytes 262144 | tf_op jit(solution)/shard_map/all_to_all | solution.py:356
  83.9 12.7 %copy-start.6 = (f32[2,18,128]{2,1,0:T(8,128)S(1)}, f32[2,18,128]{2,1,0:T(8,128)}, u32[]{:S(2)}) copy-start(f32[2,18,128]{2,1,0:T(8,128)} %get-tuple-element.10) | copy-start | bytes 55300

commit v4 on v3

v4 whole, which is shorter than its diff:
```python
import jax
import jax.numpy as jnp
from jax import lax
from jax.experimental import pallas as pl
from jax.experimental.pallas import tpu as pltpu
from jax.sharding import PartitionSpec as P

EPS = 1e-06
ROUTED_SCALE = 2.5


def rms_rows(values, gain_vec):
    mean_square = jnp.mean(values * values, axis=-1, keepdims=True)
    return values * lax.rsqrt(mean_square + EPS) * gain_vec


def unit_rows(raw):
    vals = raw.astype(jnp.bfloat16).astype(jnp.float32)
    return vals * lax.rsqrt(jnp.sum(vals * vals, axis=-1, keepdims=True) + EPS)


def columns_of(rows):
    pad = jnp.zeros((128 - rows.shape[0], rows.shape[1]), rows.dtype)
    return jnp.concatenate([rows, pad], axis=0).T


def mixer_kernel(
    parity_ref,
    tokens_hbm,
    gain_hbm,
    write_hbm,
    decay_hbm,
    head_gain_hbm,
    rate_hbm,
    bias_hbm,
    routes_hbm,
    weights_hbm,
    query_hbm,
    key_hbm,
    value_hbm,
    state_hbm,
    out_weight_hbm,
    gate_hbm,
    up_hbm,
    down_hbm,
    partial_ref,
    key_unit_ref,
    update_ref,
    keep_ref,
    dispatch_ref,
    combine_ref,
    packed_hbm,
    tokens_v,
    gain_v,
    write_v,
    decay_v,
    head_gain_v,
    rate_v,
    bias_v,
    routes_v,
    weights_v,
    query_v,
    key_v,
    value_v,
    state_v,
    out_weight_v,
    packed_v,
    found_k,
    found_q,
    sems,
):
    seq_rows = tokens_hbm.shape[0]
    width, hidden = gate_hbm.shape
    half = seq_rows // 2
    pairs = [
        (tokens_hbm, tokens_v),
        (gain_hbm, gain_v),
        (write_hbm, write_v),
        (decay_hbm, decay_v),
        (rate_hbm, rate_v),
        (bias_hbm, bias_v),
        (query_hbm, query_v),
        (key_hbm, key_v),
        (value_hbm, value_v),
        (state_hbm.at[pl.ds(0, half)], state_v.at[pl.ds(0, half)]),
        (
            state_hbm.at[pl.ds(half, seq_rows - half)],
            state_v.at[pl.ds(half, seq_rows - half)],
        ),
        (routes_hbm, routes_v),
        (weights_hbm, weights_v),
        (head_gain_hbm, head_gain_v),
        (out_weight_hbm, out_weight_v),
        (gate_hbm, packed_v.at[pl.ds(0, width)]),
        (up_hbm, packed_v.at[pl.ds(width, width)]),
    ] + [
        (
            down_hbm.at[:, pl.ds(j * hidden, hidden)],
            packed_v.at[pl.ds(2 * width + j * hidden, hidden)],
        )
        for j in range(width // hidden)
    ]
    loads = [pltpu.make_async_copy(src, dst, sems.at[i]) for i, (src, dst) in enumerate(pairs)]
    for copy in loads:
        copy.start()
    for copy in loads[:6]:
        copy.wait()
    normed = rms_rows(tokens_v[...].astype(jnp.float32), gain_v[...]).astype(jnp.bfloat16)
    wide = normed.astype(jnp.float32)
    write_logit = jnp.sum(wide * write_v[...].astype(jnp.float32), axis=-1, keepdims=True)
    decay_logit = jnp.sum(wide * decay_v[...].astype(jnp.float32), axis=-1, keepdims=True)
    write_rate = 1.0 / (1.0 + jnp.exp(-write_logit))
    biased = decay_logit + bias_v[0]
    softplus = jnp.maximum(biased, 0.0) + jnp.log1p(jnp.exp(-jnp.abs(biased)))
    keep = jnp.exp(-rate_v[0] * softplus)
    loads[6].wait()
    query_raw = jnp.dot(normed, query_v[...], preferred_element_type=jnp.float32)
    loads[7].wait()
    key_raw = jnp.dot(normed, key_v[...], preferred_element_type=jnp.float32)
    loads[8].wait()
    value_raw = jnp.dot(normed, value_v[...], preferred_element_type=jnp.float32)
    query_unit = unit_rows(query_raw) * query_raw.shape[1] ** (-0.5)
    key_unit = unit_rows(key_raw)
    value_vec = value_raw.astype(jnp.bfloat16).astype(jnp.float32)
    key_cols = columns_of(key_unit)
    query_cols = columns_of(query_unit)
    for row in range(seq_rows):
        if row == 0:
            loads[9].wait()
        if row == half:
            loads[10].wait()
        state = state_v[row]
        found_k[row : row + 1, :] = jnp.sum(
            state * key_cols[:, row : row + 1], axis=0, keepdims=True
        )
        found_q[row : row + 1, :] = jnp.sum(
            state * query_cols[:, row : row + 1], axis=0, keepdims=True
        )
    for copy in loads[11:14]:
        copy.wait()
    correction = value_vec - keep * found_k[...]
    overlap = jnp.sum(key_unit * query_unit, axis=-1, keepdims=True)
    update = write_rate * correction
    readout = keep * found_q[...] + overlap * update
    head_out = rms_rows(readout, head_gain_v[...]).astype(jnp.bfloat16)
    loads[14].wait()
    partial = jnp.dot(head_out, out_weight_v[...], preferred_element_type=jnp.float32)
    partial = partial.astype(jnp.bfloat16)
    for copy_number in range(partial_ref.shape[0]):
        partial_ref[copy_number] = partial
    for copy in loads[15:]:
        copy.wait()
    store = pltpu.make_async_copy(packed_v, packed_hbm, sems.at[0])
    store.start()
    key_unit_ref[...] = key_unit
    update_ref[...] = update
    keep_ref[...] = jnp.broadcast_to(keep, keep_ref.shape)
    routes = columns_of(routes_v[...].astype(jnp.float32))[:seq_rows].astype(jnp.int32)
    weights = columns_of(weights_v[...])[:seq_rows]
    scale = weights / jnp.sum(weights, axis=1, keepdims=True) * ROUTED_SCALE
    expert_iota = lax.broadcasted_iota(jnp.int32, (seq_rows, 128), 1)
    named = jnp.zeros((seq_rows, 128), jnp.float32)
    mix = jnp.zeros((seq_rows, 128), jnp.float32)
    for route in range(routes_hbm.shape[0]):
        hit = expert_iota == routes[:, route : route + 1]
        named = named + jnp.where(hit, 1.0, 0.0)
        mix = mix + jnp.where(hit, scale[:, route : route + 1], 0.0)
    row_a = lax.broadcasted_iota(jnp.int32, (seq_rows, seq_rows), 0)
    row_b = lax.broadcasted_iota(jnp.int32, (seq_rows, seq_rows), 1)
    below = jnp.where(row_b < row_a, 1.0, 0.0)
    earlier = jnp.dot(below, named, preferred_element_type=jnp.float32)
    slot = earlier.astype(jnp.int32)
    dispatch_ref[...] = jnp.where(slot == parity_ref[0], named, 0.0).astype(jnp.bfloat16)
    combine_ref[0] = jnp.where(slot == 0, mix, 0.0)
    combine_ref[1] = jnp.where(slot == 1, mix, 0.0)
    store.wait()


def rows_kernel(
    gathered_ref,
    tokens_ref,
    gain_ref,
    dispatch_ref,
    residual_ref,
    input_ref,
    rows_ref,
    wide_v,
):
    mixed = jnp.sum(gathered_ref[...].astype(jnp.float32), axis=0)
    mixed = mixed.astype(jnp.bfloat16).astype(jnp.float32)
    residual = (tokens_ref[...].astype(jnp.float32) + mixed).astype(jnp.bfloat16)
    inputs = rms_rows(residual.astype(jnp.float32), gain_ref[...]).astype(jnp.bfloat16)
    residual_ref[...] = residual
    input_ref[...] = inputs
    experts = dispatch_ref.shape[1]
    picked = lax.dot_general(
        dispatch_ref[...], inputs, (((0,), (0,)), ((), ())), preferred_element_type=jnp.float32
    )
    lanes = inputs.shape[1] // 128
    for lane in range(lanes):
        wide_v[pl.ds(lane, experts, stride=lanes), :] = picked[:, lane * 128 : (lane + 1) * 128]
    rows_ref[...] = wide_v[...].astype(jnp.bfloat16)


def expert_kernel(
    rows_ref,
    own_ref,
    other_ref,
    shared_ref,
    blocks_ref,
    wide_v,
    rows_v,
):
    lanes = 8
    experts = rows_ref.shape[0] // lanes
    width = lanes * 128
    wide_v[...] = rows_ref[...].astype(jnp.float32)
    for lane in range(lanes):
        rows_v[:, lane * 128 : (lane + 1) * 128] = wide_v[
            pl.ds(lane, experts, stride=lanes), :
        ].astype(jnp.bfloat16)
    rows = rows_v[...]
    acts = []
    for pack_ref in (own_ref, other_ref):
        gate = jnp.dot(rows, pack_ref[:width], preferred_element_type=jnp.float32)
        up = jnp.dot(rows, pack_ref[width : 2 * width], preferred_element_type=jnp.float32)
        acts.append((gate / (1.0 + jnp.exp(-gate)) * up).astype(jnp.bfloat16))
    parts = blocks_ref.shape[0]
    share = width // parts
    for j in range(lanes):
        at = 2 * width + j * 128
        down = jnp.dot(acts[0], own_ref[at : at + 128], preferred_element_type=jnp.float32)
        down += jnp.dot(acts[1], other_ref[at : at + 128], preferred_element_type=jnp.float32)
        col = j * 128 % share
        blocks_ref[j * 128 // share, :experts, col : col + 128] = down.astype(jnp.bfloat16)
    for part in range(parts):
        blocks_ref[part, experts:, :] = shared_ref[:, part * share : (part + 1) * share]


def share_kernel(parts_ref, rows_ref, shared_ref, wide_v):
    share = parts_ref.shape[2]
    seq_rows = shared_ref.shape[0]
    experts = parts_ref.shape[1] - seq_rows
    quads = rows_ref.shape[0] // experts
    chunks = share // 128
    for slot in range(2):
        total = parts_ref[slot, :experts, :].astype(jnp.float32)
        total += parts_ref[slot + 2, :experts, :].astype(jnp.float32)
        for chunk in range(chunks):
            wide_v[pl.ds(slot * chunks + chunk, experts, stride=quads), :] = total[
                :, chunk * 128 : (chunk + 1) * 128
            ]
    rows_ref[...] = wide_v[...].astype(jnp.bfloat16)
    shared = jnp.sum(parts_ref[:, experts:, :].astype(jnp.float32), axis=0)
    shared_ref[...] = shared.astype(jnp.bfloat16).astype(jnp.float32)


def final_kernel(
    index_ref, rows_ref, combine_ref, residual_ref, shared_ref, out_ref, wide_v
):
    share = out_ref.shape[1]
    chunks = share // 128
    experts = combine_ref.shape[2]
    quads = rows_ref.shape[0] // experts
    wide_v[...] = rows_ref[...].astype(jnp.float32)
    at = pl.multiple_of(index_ref[0] * share, share)
    base = residual_ref[:, pl.ds(at, share)].astype(jnp.float32) + shared_ref[...]
    for chunk in range(chunks):
        routed = base[:, chunk * 128 : (chunk + 1) * 128]
        for slot in range(2):
            rows = wide_v[pl.ds(slot * chunks + chunk, experts, stride=quads), :]
            routed += jnp.dot(
                combine_ref[slot],
                rows,
                preferred_element_type=jnp.float32,
                precision=lax.Precision.HIGHEST,
            )
        out_ref[:, chunk * 128 : (chunk + 1) * 128] = routed.astype(jnp.bfloat16)


def state_kernel(
    key_unit_ref,
    update_ref,
    keep_ref,
    state_hbm,
    next_hbm,
    state_v,
    next_v,
    sems,
):
    seq_rows = key_unit_ref.shape[0]
    half = seq_rows // 2
    spans = [(0, half), (half, seq_rows - half)]
    loads = [
        pltpu.make_async_copy(
            state_hbm.at[pl.ds(at, size)], state_v.at[pl.ds(at, size)], sems.at[i]
        )
        for i, (at, size) in enumerate(spans)
    ]
    stores = [
        pltpu.make_async_copy(
            next_v.at[pl.ds(at, size)], next_hbm.at[pl.ds(at, size)], sems.at[2 + i]
        )
        for i, (at, size) in enumerate(spans)
    ]
    for copy in loads:
        copy.start()
    key_cols = columns_of(key_unit_ref[...])
    for part, (at, size) in enumerate(spans):
        loads[part].wait()
        for row in range(at, at + size):
            next_v[row] = (
                keep_ref[row : row + 1, :] * state_v[row]
                + key_cols[:, row : row + 1] * update_ref[row : row + 1, :]
            )
        stores[part].start()
    for copy in stores:
        copy.wait()


def vmem():
    return pl.BlockSpec(memory_space=pltpu.VMEM)


def smem():
    return pl.BlockSpec(memory_space=pltpu.SMEM)


def anywhere():
    return pl.BlockSpec(memory_space=pl.ANY)


def in_vmem(array):
    return pltpu.with_memory_space_constraint(array, pltpu.VMEM)


def per_device(
    tokens,
    delta_state,
    mixer_gain,
    query_weight,
    key_weight,
    value_weight,
    write_weight,
    decay_weight,
    decay_rate,
    decay_bias,
    head_gain,
    out_weight,
    channel_gain,
    routes,
    route_weights,
    expert_gate,
    expert_up,
    expert_down,
    shared_gate,
    shared_up,
    shared_down,
):
    seq_rows, model_width = tokens.shape
    head_dim = delta_state.shape[2]
    tp_count = lax.axis_size("tp")
    ep_count = lax.axis_size("ep")
    share_width = model_width // tp_count
    hidden = expert_gate.shape[2]
    tp_index = lax.axis_index("tp")
    parity = (tp_index % 2).astype(jnp.int32).reshape(1)
    f32, bf16 = jnp.float32, jnp.bfloat16
    state = delta_state.reshape(seq_rows, head_dim, head_dim)
    small = pltpu.VMEM((seq_rows, head_dim), f32)
    partials, key_unit, update, keep, dispatch, combine, packed = pl.pallas_call(
        mixer_kernel,
        out_shape=[
            jax.ShapeDtypeStruct((tp_count, seq_rows, model_width), bf16),
            small,
            small,
            small,
            pltpu.VMEM((seq_rows, ep_count), bf16),
            pltpu.VMEM((2, seq_rows, ep_count), f32),
            jax.ShapeDtypeStruct((3 * model_width, hidden), bf16),
        ],
        in_specs=[smem()] + [anywhere()] * 17,
        out_specs=[vmem()] * 6 + [anywhere()],
        scratch_shapes=[
            pltpu.VMEM((seq_rows, model_width), bf16),
            pltpu.VMEM((1, model_width), f32),
            pltpu.VMEM((1, model_width), bf16),
            pltpu.VMEM((1, model_width), bf16),
            pltpu.VMEM((1, head_dim), f32),
            pltpu.SMEM((1,), f32),
            pltpu.SMEM((1,), f32),
            pltpu.VMEM(routes.T.shape, jnp.int32),
            pltpu.VMEM(routes.T.shape, f32),
            pltpu.VMEM((model_width, head_dim), bf16),
            pltpu.VMEM((model_width, head_dim), bf16),
            pltpu.VMEM((model_width, head_dim), bf16),
            pltpu.VMEM((seq_rows, head_dim, head_dim), f32),
            pltpu.VMEM((head_dim, model_width), bf16),
            pltpu.VMEM((3 * model_width, hidden), bf16),
            pltpu.VMEM((seq_rows, head_dim), f32),
            pltpu.VMEM((seq_rows, head_dim), f32),
            pltpu.SemaphoreType.DMA((17 + model_width // hidden,)),
        ],
    )(
        parity,
        tokens,
        mixer_gain.reshape(1, model_width),
        write_weight.reshape(1, model_width),
        decay_weight.reshape(1, model_width),
        head_gain.reshape(1, head_dim),
        decay_rate,
        decay_bias,
        routes.T,
        route_weights.T,
        query_weight,
        key_weight,
        value_weight,
        state,
        out_weight,
        expert_gate[0],
        expert_up[0],
        expert_down[0],
    )
    gathered = lax.all_to_all(partials, "tp", 0, 0, tiled=True)
    next_state = pl.pallas_call(
        state_kernel,
        out_shape=jax.ShapeDtypeStruct((seq_rows, head_dim, head_dim), f32),
        in_specs=[vmem()] * 3 + [anywhere()],
        out_specs=anywhere(),
        scratch_shapes=[
            pltpu.VMEM((seq_rows, head_dim, head_dim), f32),
            pltpu.VMEM((seq_rows, head_dim, head_dim), f32),
            pltpu.SemaphoreType.DMA((4,)),
        ],
    )(in_vmem(key_unit), in_vmem(update), in_vmem(keep), state)
    other = lax.ppermute(packed, "tp", [(i, i ^ 1) for i in range(tp_count)])
    lanes = model_width // 128
    residual, expert_input, outgoing = pl.pallas_call(
        rows_kernel,
        out_shape=[
            pltpu.VMEM((seq_rows, model_width), bf16),
            pltpu.VMEM((seq_rows, model_width), bf16),
            jax.ShapeDtypeStruct((ep_count * lanes, 128), bf16),
        ],
        in_specs=[vmem()] * 4,
        out_specs=[vmem()] * 3,
        scratch_shapes=[pltpu.VMEM((ep_count * lanes, 128), f32)],
    )(
        in_vmem(gathered),
        in_vmem(tokens),
        in_vmem(channel_gain.reshape(1, model_width)),
        in_vmem(dispatch),
    )
    received = lax.all_to_all(outgoing.reshape(ep_count, lanes, 128), "ep", 0, 0, tiled=True)
    shared_act = (
        jax.nn.silu(jnp.dot(expert_input, shared_gate, preferred_element_type=f32))
        * jnp.dot(expert_input, shared_up, preferred_element_type=f32)
    ).astype(bf16)
    shared_partial = jnp.dot(shared_act, shared_down, preferred_element_type=f32).astype(bf16)
    blocks = pl.pallas_call(
        expert_kernel,
        out_shape=pltpu.VMEM((tp_count, ep_count + seq_rows, share_width), bf16),
        in_specs=[vmem()] * 4,
        out_specs=vmem(),
        scratch_shapes=[
            pltpu.VMEM((ep_count * lanes, 128), f32),
            pltpu.VMEM((ep_count, model_width), bf16),
        ],
    )(
        in_vmem(received.reshape(ep_count * lanes, 128)),
        in_vmem(packed),
        in_vmem(other),
        in_vmem(shared_partial),
    )
    parts = lax.all_to_all(blocks, "tp", 0, 0, tiled=True)
    quads = 2 * (share_width // 128)
    expert_share, shared_out = pl.pallas_call(
        share_kernel,
        out_shape=[
            pltpu.VMEM((ep_count * quads, 128), bf16),
            pltpu.VMEM((seq_rows, share_width), f32),
        ],
        in_specs=[vmem()],
        out_specs=[vmem()] * 2,
        scratch_shapes=[pltpu.VMEM((ep_count * quads, 128), f32)],
    )(in_vmem(parts))
    returned = lax.all_to_all(expert_share.reshape(ep_count, quads, 128), "ep", 0, 0, tiled=True)
    layer_out = pl.pallas_call(
        final_kernel,
        out_shape=jax.ShapeDtypeStruct((seq_rows, share_width), bf16),
        in_specs=[smem()] + [vmem()] * 4,
        out_specs=vmem(),
        scratch_shapes=[pltpu.VMEM((ep_count * quads, 128), f32)],
    )(
        tp_index.astype(jnp.int32).reshape(1),
        in_vmem(returned.reshape(ep_count * quads, 128)),
        in_vmem(combine),
        in_vmem(residual),
        in_vmem(shared_out),
    )
    return (layer_out, next_state.reshape(delta_state.shape))


def solution(mesh):
    return jax.shard_map(
        per_device,
        mesh=mesh,
        in_specs=(
            P("ep", None),
            P("ep", "tp", None, None),
            P(),
            P(None, "tp"),
            P(None, "tp"),
            P(None, "tp"),
            P(None, "tp"),
            P(None, "tp"),
            P("tp"),
            P("tp"),
            P(),
            P("tp", None),
            P(),
            P("ep", None),
            P("ep", None),
            P("ep", None, "tp"),
            P("ep", None, "tp"),
            P("ep", "tp", None),
            P(None, "tp"),
            P(None, "tp"),
            P("tp", None),
        ),
        out_specs=(P("ep", "tp"), P("ep", "tp", None, None)),
        check_vma=False,
    )
```

time: 98.1 us -> 98.5 us (level)
  blocking collectives: 8.16 us -> 30.4 us
  starting transfers between devices: 42.4 us -> 29.4 us
  matrix products: 3.56 us -> 0.44 us
  waiting for transfers between devices: 27.9 us -> 25.2 us
  local copies, waits for them, and re-layouts: 2.3 us -> 0.04 us
    all_to_all x1 -> x2, blocking collectives: 8.16 us -> 30.4 us  [the longest x1 21.4 us: per_device(): gathered = lax.all_to_all(partials, 'tp', 0, 0, tiled=True)]
    all_to_all x3 -> x2, starting transfers between devices: 40.2 us -> 25.3 us  [the longest x1 18.7 us: per_device(): lax.all_to_all(outgoing.reshape(ep_count, lanes, 128), 'ep', 0, 0, tiled=...]
    ppermute x1, waiting for transfers between devices: 4.23 us -> 0.01 us  [per_device(): other = lax.ppermute(packed, 'tp', [(i, i ^ 1) for i in range(tp_count)])]
    dot_general x6 -> x0, matrix products: 3.02 us -> none  [the longest x1 1.01 us: per_device(): lax.dot_general(dispatch, expert_input, (((0,), (0,)), ((), ())), preferr...]
    ppermute x1, starting transfers between devices: 2.19 us -> 4.07 us  [per_device(): other = lax.ppermute(packed, 'tp', [(i, i ^ 1) for i in range(tp_count)])]
    all_to_all x3 -> x2, waiting for transfers between devices: 23.6 us -> 25.2 us  [the longest x1 14.8 us: per_device(): lax.all_to_all(outgoing.reshape(ep_count, lanes, 128), 'ep', 0, 0, tiled=...]
    reshape x5 -> x0, local copies, waits for them, and re-layouts: 1.41 us -> none  [the longest x1 0.88 us: per_device(): outgoing.reshape(ep_count, 2, model_width // 2)]
    pallas_call x1 -> x4, Pallas kernels: 3.32 us -> 3.53 us  [the longest x1 1.07 us: per_device(): pl.pallas_call(rows_kernel, out_shape=[pltpu.VMEM((seq_rows, model_width)...]
  transfers between devices with their start and end apart: 4 -> 3, of which waited for: 4 -> 2; matrix products, arithmetic and copies ran while one was open for 1% -> 0% of each run, Pallas kernels for 7% -> 4%
where the time goes in v4:
time: 98.5 us; the launch traced here: 98.1 us
  blocking collectives  30.4 us (31%)
  starting transfers between devices  29.4 us (30%)
  waiting for transfers between devices  25.2 us (26%)
  Pallas kernels  10.5 us (11%)
  between operations  2.11 us (2%)
    all_to_all x1, blocking collectives, per_device(): gathered = lax.all_to_all(partials, 'tp', 0, 0, tiled=True)  21.4 us
    all_to_all x1, starting transfers between devices, per_device(): lax.all_to_all(outgoing.reshape(ep_count, lanes, 128), 'ep', 0, 0, tiled=...  18.7 us
    all_to_all x1, waiting for transfers between devices, per_device(): lax.all_to_all(outgoing.reshape(ep_count, lanes, 128), 'ep', 0, 0, tiled=...  14.8 us
    all_to_all x1, waiting for transfers between devices, per_device(): lax.all_to_all(expert_share.reshape(ep_count, quads, 128), 'ep', 0, 0, ti...  10.4 us
    all_to_all x1, blocking collectives, per_device(): parts = lax.all_to_all(blocks, 'tp', 0, 0, tiled=True)  9.02 us
    all_to_all x1, starting transfers between devices, per_device(): lax.all_to_all(expert_share.reshape(ep_count, quads, 128), 'ep', 0, 0, ti...  6.61 us
    pallas_call x1, Pallas kernels, per_device(): pl.pallas_call(mixer_kernel, out_shape=[jax.ShapeDtypeStruct((tp_count, s...  4.55 us
    ppermute x1, starting transfers between devices, per_device(): other = lax.ppermute(packed, 'tp', [(i, i ^ 1) for i in range(tp_count)])  4.07 us
  transfers between devices with their start and end apart: 3, of which 2 were waited for; matrix products, arithmetic and copies ran while one was open for 0% of the time, Pallas kernels for 4%

profile of v4, /device:TPU:1, one launch (start us, length us, event | category | flops | bytes accessed | tf_op | source)
XLA Modules:
  0.0 98.1 jit_solution(11942266376245642250)
XLA Ops:
  0.6 0.0 copy-start
  2.0 0.0 copy-start.2
  2.0 0.0 copy-start.3
  2.0 4.5 %shard_map.212 = (bf16[4,18,1024]{2,1,0:T(8,128)(2,1)}, f32[18,128]{1,0:T(8,128)S(1)}, f32[18,128]{1,0:T(8,128)S(1)}, f32[18,128]{1,0:T(8,128)S(1)}, bf16[18,128...) custom-call(s32[1]{0:T(128)} %bitcast.1.parity_ref, bf16[18,1024]{1,0:T(8,128)(2,1)} %tokens_ref.1, ...), custom_call_target="tpu_custom_call" | custom-call | tf_op jit(solution)/shard_map/pallas_call | solution.py:371
  6.6 0.0 copy-start.4
  6.6 0.0 copy-start.5
  6.6 0.0 copy-start.1
  6.6 4.1 %collective-permute-start = (bf16[3072,128]{1,0:T(8,128)(2,1)}, bf16[3072,128]{1,0:T(8,128)(2,1)S(1)}, u32[]{:S(2)}, u32[]{:S(2)}) collective-permute-start(bf16[3072,128]{1,0:T(8,128)(2,1)} %get-tuple-element.17.own_ref), channel_id=1, source_target_pairs={{0,1},{1,0},{2,3},{3,2},{4,5},{5,4},{6,7},{7,6},{8,9},{9,8},{10,11... | collective-permute-start | bytes 2359304 | tf_op jit(solution)/shard_map/ppermute | solution.py:436
  10.7 21.4 %all_to_all.20.gathered_ref = bf16[4,18,1024]{2,1,0:T(8,128)(2,1)S(1)} all-to-all(bf16[4,18,1024]{2,1,0:T(8,128)(2,1)} %get-tuple-element.14), channel_id=1, replica_groups=mesh['ep'=128,'tp'=4] {'tp'}, dimensions={0} | all-to-all | bytes 294912 | tf_op jit(solution)/shard_map/all_to_all | solution.py:424
  32.1 0.0 copy-done.3
  32.1 1.1 %shard_map.213 = (bf16[18,1024]{1,0:T(8,128)(2,1)S(1)}, bf16[18,1024]{1,0:T(8,128)(2,1)S(1)}, bf16[1024,128]{1,0:T(8,128)(2,1)}) custom-call(bf16[4,18,1024]{2,1,0:T(8,128)(2,1)S(1)} %all_to_all.20.gathered_ref, bf16[18,1024]{1,0:T(8,128)(2,1)S(1)} %copy-done.2, f32[1,1024]{1,0:T(1,128)S(1)} %bitcast.27, bf16[18,128]{1,0:T(8,128)(2,1)S(1)} %get-tuple-element.15.dispatch_ref), custom_call_target="tpu_custom_call" | custom-call | tf_op jit(solution)/shard_map/pallas_call | solution.py:438
  33.2 18.7 %all-to-all-start.1 = ((bf16[128,8,128]{2,1,0:T(8,128)(2,1)}), bf16[128,8,128]{2,1,0:T(8,128)(2,1)S(1)}, u32[]{:S(2)}, u32[]{:S(2)}) async-start(bf16[128,8,128]{2,1,0:T(8,128)(2,1)} %bitcast.31), calls=%async_computation.1 | async-start | bytes 524288 | tf_op jit(solution)/shard_map/all_to_all | solution.py:454
  51.9 0.0 copy-done.4
  51.9 0.2 fusion.8
  52.1 0.3 convolution_convert_fusion.shared_ref
  52.4 14.8 %all-to-all-done.1 = bf16[128,8,128]{2,1,0:T(8,128)(2,1)S(1)} async-done(((bf16[128,8,128]{2,1,0:T(8,128)(2,1)}), bf16[128,8,128]{2,1,0:T(8,128)(2,1)S(1)}, u32[]{:S(2)}, u32[]{:S(2)}) %all-to-all-start.1) | async-done | bytes 262176 | tf_op jit(solution)/shard_map/all_to_all | solution.py:454
  67.2 0.0 collective-permute-done.other_ref
  67.2 0.8 shard_map.214
  68.0 9.0 %all_to_all.21.parts_ref = bf16[4,146,256]{2,1,0:T(8,128)(2,1)S(1)} all-to-all(bf16[4,146,256]{2,1,0:T(8,128)(2,1)S(1)} %shard_map.214), channel_id=1, replica_groups=mesh['ep'=128,'tp'=4] {'tp'}, dimensions={0} | all-to-all | bytes 598016 | tf_op jit(solution)/shard_map/all_to_all | solution.py:475
  77.0 0.7 shard_map.215
  77.7 6.6 %all-to-all-start.3 = ((bf16[128,4,128]{2,1,0:T(4,128)(2,1)}), bf16[128,4,128]{2,1,0:T(4,128)(2,1)S(1)}, u32[]{:S(2)}, u32[]{:S(2)}) async-start(bf16[128,4,128]{2,1,0:T(4,128)(2,1)} %bitcast.15), calls=%async_computation.3 | async-start | bytes 262144 | tf_op jit(solution)/shard_map/all_to_all | solution.py:487
  84.3 2.4 %shard_map.217 = f32[18,128,128]{2,1,0:T(8,128)} custom-call(f32[18,128]{1,0:T(8,128)S(1)} %get-tuple-element.23.key_unit_ref, f32[18,128]{1,0:T(8,128)S(1)} %get-tuple-element.24.update_ref, f32[18,128]{1,0:T(8,128)S(1)} %get-tuple-element.25.keep_ref, f32[18,128,128]{2,1,0:T(8,128)} %bitcast.29), custom_call_target="tpu_custom_call" | custom-call | tf_op jit(solution)/shard_map/pallas_call | solution.py:425
  86.7 10.4 %all-to-all-done.3 = bf16[128,4,128]{2,1,0:T(4,128)(2,1)S(1)} async-done(((bf16[128,4,128]{2,1,0:T(4,128)(2,1)}), bf16[128,4,128]{2,1,0:T(4,128)(2,1)S(1)}, u32[]{:S(2)}, u32[]{:S(2)}) %all-to-all-start.3) | async-done | bytes 131104 | tf_op jit(solution)/shard_map/all_to_all | solution.py:487
  97.1 0.9 shard_map.216
  (4 shorter events, 0.0 us)
Async XLA Ops:
  0.6 51.5 %copy-start = (bf16[128,1024]{1,0:T(8,128)(2,1)S(1)}, bf16[128,1024]{1,0:T(8,128)(2,1)}, u32[]{:S(2)}) copy-start(bf16[128,1024]{1,0:T(8,128)(2,1)} %param.41) | copy-start | bytes 786436
  2.0 30.1 %copy-start.2 = (bf16[18,1024]{1,0:T(8,128)(2,1)S(1)}, bf16[18,1024]{1,0:T(8,128)(2,1)}, u32[]{:S(2)}) copy-start(bf16[18,1024]{1,0:T(8,128)(2,1)} %tokens_ref.1) | copy-start | bytes 110596
  2.0 30.1 %copy-start.3 = (f32[1024]{0:T(1024)S(1)}, f32[1024]{0:T(1024)}, u32[]{:S(2)}) copy-start(f32[1024]{0:T(1024)} %param.33) | copy-start | bytes 12292
  6.6 45.4 %copy-start.4 = (bf16[1024,128]{1,0:T(8,128)(2,1)S(1)}, bf16[1024,128]{1,0:T(8,128)(2,1)}, u32[]{:S(2)}) copy-start(bf16[1024,128]{1,0:T(8,128)(2,1)} %param.39) | copy-start | bytes 786436
  6.6 45.5 %copy-start.5 = (bf16[1024,128]{1,0:T(8,128)(2,1)S(1)}, bf16[1024,128]{1,0:T(8,128)(2,1)}, u32[]{:S(2)}) copy-start(bf16[1024,128]{1,0:T(8,128)(2,1)} %param.40) | copy-start | bytes 786436
  6.6 60.6 %copy-start.1 = (bf16[3072,128]{1,0:T(8,128)(2,1)S(1)}, bf16[3072,128]{1,0:T(8,128)(2,1)}, u32[]{:S(2)}) copy-start(bf16[3072,128]{1,0:T(8,128)(2,1)} %get-tuple-element.17.own_ref) | copy-start | bytes 2359300
  6.6 60.5 %collective-permute-start = (bf16[3072,128]{1,0:T(8,128)(2,1)}, bf16[3072,128]{1,0:T(8,128)(2,1)S(1)}, u32[]{:S(2)}, u32[]{:S(2)}) collective-permute-start(bf16[3072,128]{1,0:T(8,128)(2,1)} %get-tuple-element.17.own_ref), channel_id=1, source_target_pairs={{0,1},{1,0},{2,3},{3,2},{4,5},{5,4},{6,7},{7,6},{8,9},{9,8},{10,11... | collective-permute-start | bytes 2359304 | tf_op jit(solution)/shard_map/ppermute | solution.py:436
  33.2 34.0 %all-to-all-start.1 = ((bf16[128,8,128]{2,1,0:T(8,128)(2,1)}), bf16[128,8,128]{2,1,0:T(8,128)(2,1)S(1)}, u32[]{:S(2)}, u32[]{:S(2)}) async-start(bf16[128,8,128]{2,1,0:T(8,128)(2,1)} %bitcast.31), calls=%async_computation.1 | async-start | bytes 524288 | tf_op jit(solution)/shard_map/all_to_all | solution.py:454
  77.7 19.4 %all-to-all-start.3 = ((bf16[128,4,128]{2,1,0:T(4,128)(2,1)}), bf16[128,4,128]{2,1,0:T(4,128)(2,1)S(1)}, u32[]{:S(2)}, u32[]{:S(2)}) async-start(bf16[128,4,128]{2,1,0:T(4,128)(2,1)} %bitcast.15), calls=%async_computation.3 | async-start | bytes 262144 | tf_op jit(solution)/shard_map/all_to_all | solution.py:487

commit v5 on v4

--- a/solution.py
+++ b/solution.py
@@ -25,7 +25,6 @@
 
 
 def mixer_kernel(
-    parity_ref,
     tokens_hbm,
     gain_hbm,
     write_hbm,
@@ -43,13 +42,13 @@
     gate_hbm,
     up_hbm,
     down_hbm,
-    partial_ref,
+    partial_hbm,
     key_unit_ref,
     update_ref,
     keep_ref,
     dispatch_ref,
     combine_ref,
-    packed_hbm,
+    packed_ref,
     tokens_v,
     gain_v,
     write_v,
@@ -64,7 +63,7 @@
     value_v,
     state_v,
     out_weight_v,
-    packed_v,
+    partial_v,
     found_k,
     found_q,
     sems,
@@ -72,6 +71,7 @@
     seq_rows = tokens_hbm.shape[0]
     width, hidden = gate_hbm.shape
     half = seq_rows // 2
+    wide_block = 2 * hidden
     pairs = [
         (tokens_hbm, tokens_v),
         (gain_hbm, gain_v),
@@ -79,6 +79,8 @@
         (decay_hbm, decay_v),
         (rate_hbm, rate_v),
         (bias_hbm, bias_v),
+        (routes_hbm, routes_v),
+        (weights_hbm, weights_v),
         (query_hbm, query_v),
         (key_hbm, key_v),
         (value_hbm, value_v),
@@ -87,23 +89,21 @@
             state_hbm.at[pl.ds(half, seq_rows - half)],
             state_v.at[pl.ds(half, seq_rows - half)],
         ),
-        (routes_hbm, routes_v),
-        (weights_hbm, weights_v),
         (head_gain_hbm, head_gain_v),
         (out_weight_hbm, out_weight_v),
-        (gate_hbm, packed_v.at[pl.ds(0, width)]),
-        (up_hbm, packed_v.at[pl.ds(width, width)]),
+        (gate_hbm, packed_ref.at[pl.ds(0, width), pl.ds(0, hidden)]),
+        (up_hbm, packed_ref.at[pl.ds(0, width), pl.ds(hidden, hidden)]),
     ] + [
         (
-            down_hbm.at[:, pl.ds(j * hidden, hidden)],
-            packed_v.at[pl.ds(2 * width + j * hidden, hidden)],
+            down_hbm.at[:, pl.ds(j * wide_block, wide_block)],
+            packed_ref.at[pl.ds(width + j * hidden, hidden)],
         )
-        for j in range(width // hidden)
+        for j in range(width // wide_block)
     ]
     loads = [pltpu.make_async_copy(src, dst, sems.at[i]) for i, (src, dst) in enumerate(pairs)]
     for copy in loads:
         copy.start()
-    for copy in loads[:6]:
+    for copy in loads[:8]:
         copy.wait()
     normed = rms_rows(tokens_v[...].astype(jnp.float32), gain_v[...]).astype(jnp.bfloat16)
     wide = normed.astype(jnp.float32)
@@ -113,48 +113,6 @@
     biased = decay_logit + bias_v[0]
     softplus = jnp.maximum(biased, 0.0) + jnp.log1p(jnp.exp(-jnp.abs(biased)))
     keep = jnp.exp(-rate_v[0] * softplus)
-    loads[6].wait()
-    query_raw = jnp.dot(normed, query_v[...], preferred_element_type=jnp.float32)
-    loads[7].wait()
-    key_raw = jnp.dot(normed, key_v[...], preferred_element_type=jnp.float32)
-    loads[8].wait()
-    value_raw = jnp.dot(normed, value_v[...], preferred_element_type=jnp.float32)
-    query_unit = unit_rows(query_raw) * query_raw.shape[1] ** (-0.5)
-    key_unit = unit_rows(key_raw)
-    value_vec = value_raw.astype(jnp.bfloat16).astype(jnp.float32)
-    key_cols = columns_of(key_unit)
-    query_cols = columns_of(query_unit)
-    for row in range(seq_rows):
-        if row == 0:
-            loads[9].wait()
-        if row == half:
-            loads[10].wait()
-        state = state_v[row]
-        found_k[row : row + 1, :] = jnp.sum(
-            state * key_cols[:, row : row + 1], axis=0, keepdims=True
-        )
-        found_q[row : row + 1, :] = jnp.sum(
-            state * query_cols[:, row : row + 1], axis=0, keepdims=True
-        )
-    for copy in loads[11:14]:
-        copy.wait()
-    correction = value_vec - keep * found_k[...]
-    overlap = jnp.sum(key_unit * query_unit, axis=-1, keepdims=True)
-    update = write_rate * correction
-    readout = keep * found_q[...] + overlap * update
-    head_out = rms_rows(readout, head_gain_v[...]).astype(jnp.bfloat16)
-    loads[14].wait()
-    partial = jnp.dot(head_out, out_weight_v[...], preferred_element_type=jnp.float32)
-    partial = partial.astype(jnp.bfloat16)
-    for copy_number in range(partial_ref.shape[0]):
-        partial_ref[copy_number] = partial
-    for copy in loads[15:]:
-        copy.wait()
-    store = pltpu.make_async_copy(packed_v, packed_hbm, sems.at[0])
-    store.start()
-    key_unit_ref[...] = key_unit
-    update_ref[...] = update
-    keep_ref[...] = jnp.broadcast_to(keep, keep_ref.shape)
     routes = columns_of(routes_v[...].astype(jnp.float32))[:seq_rows].astype(jnp.int32)
     weights = columns_of(weights_v[...])[:seq_rows]
     scale = weights / jnp.sum(weights, axis=1, keepdims=True) * ROUTED_SCALE
@@ -170,9 +128,50 @@
     below = jnp.where(row_b < row_a, 1.0, 0.0)
     earlier = jnp.dot(below, named, preferred_element_type=jnp.float32)
     slot = earlier.astype(jnp.int32)
-    dispatch_ref[...] = jnp.where(slot == parity_ref[0], named, 0.0).astype(jnp.bfloat16)
+    dispatch_ref[...] = jnp.where(slot == lax.axis_index("tp") % 2, named, 0.0).astype(jnp.bfloat16)
     combine_ref[0] = jnp.where(slot == 0, mix, 0.0)
     combine_ref[1] = jnp.where(slot == 1, mix, 0.0)
+    loads[8].wait()
+    query_raw = jnp.dot(normed, query_v[...], preferred_element_type=jnp.float32)
+    loads[9].wait()
+    key_raw = jnp.dot(normed, key_v[...], preferred_element_type=jnp.float32)
+    loads[10].wait()
+    value_raw = jnp.dot(normed, value_v[...], preferred_element_type=jnp.float32)
+    query_unit = unit_rows(query_raw) * query_raw.shape[1] ** (-0.5)
+    key_unit = unit_rows(key_raw)
+    value_vec = value_raw.astype(jnp.bfloat16).astype(jnp.float32)
+    key_cols = columns_of(key_unit)
+    query_cols = columns_of(query_unit)
+    for row in range(seq_rows):
+        if row == 0:
+            loads[11].wait()
+        if row == half:
+            loads[12].wait()
+        state = state_v[row]
+        found_k[row : row + 1, :] = jnp.sum(
+            state * key_cols[:, row : row + 1], axis=0, keepdims=True
+        )
+        found_q[row : row + 1, :] = jnp.sum(
+            state * query_cols[:, row : row + 1], axis=0, keepdims=True
+        )
+    loads[13].wait()
+    correction = value_vec - keep * found_k[...]
+    overlap = jnp.sum(key_unit * query_unit, axis=-1, keepdims=True)
+    update = write_rate * correction
+    readout = keep * found_q[...] + overlap * update
+    head_out = rms_rows(readout, head_gain_v[...]).astype(jnp.bfloat16)
+    loads[14].wait()
+    partial = jnp.dot(head_out, out_weight_v[...], preferred_element_type=jnp.float32)
+    partial = partial.astype(jnp.bfloat16)
+    for copy_number in range(partial_v.shape[0]):
+        partial_v[copy_number] = partial
+    store = pltpu.make_async_copy(partial_v, partial_hbm, sems.at[0])
+    store.start()
+    key_unit_ref[...] = key_unit
+    update_ref[...] = update
+    keep_ref[...] = jnp.broadcast_to(keep, keep_ref.shape)
+    for copy in loads[15:]:
+        copy.wait()
     store.wait()
 
 
@@ -222,18 +221,17 @@
     rows = rows_v[...]
     acts = []
     for pack_ref in (own_ref, other_ref):
-        gate = jnp.dot(rows, pack_ref[:width], preferred_element_type=jnp.float32)
-        up = jnp.dot(rows, pack_ref[width : 2 * width], preferred_element_type=jnp.float32)
+        both = jnp.dot(rows, pack_ref[:width], preferred_element_type=jnp.float32)
+        gate, up = both[:, :128], both[:, 128:]
         acts.append((gate / (1.0 + jnp.exp(-gate)) * up).astype(jnp.bfloat16))
+    act = jnp.concatenate(acts, axis=1)
     parts = blocks_ref.shape[0]
     share = width // parts
-    for j in range(lanes):
-        at = 2 * width + j * 128
-        down = jnp.dot(acts[0], own_ref[at : at + 128], preferred_element_type=jnp.float32)
-        down += jnp.dot(acts[1], other_ref[at : at + 128], preferred_element_type=jnp.float32)
-        col = j * 128 % share
-        blocks_ref[j * 128 // share, :experts, col : col + 128] = down.astype(jnp.bfloat16)
     for part in range(parts):
+        at = width + part * 128
+        down = jnp.concatenate([own_ref[at : at + 128], other_ref[at : at + 128]], axis=0)
+        total = jnp.dot(act, down, preferred_element_type=jnp.float32)
+        blocks_ref[part, :experts, :] = total.astype(jnp.bfloat16)
         blocks_ref[part, experts:, :] = shared_ref[:, part * share : (part + 1) * share]
 
 
@@ -255,35 +253,27 @@
     shared_ref[...] = shared.astype(jnp.bfloat16).astype(jnp.float32)
 
 
-def final_kernel(
-    index_ref, rows_ref, combine_ref, residual_ref, shared_ref, out_ref, wide_v
-):
-    share = out_ref.shape[1]
+def final_kernel(rows_ref, mix_ref, residual_ref, shared_ref, out_ref):
+    seq_rows, share = out_ref.shape
     chunks = share // 128
-    experts = combine_ref.shape[2]
-    quads = rows_ref.shape[0] // experts
-    wide_v[...] = rows_ref[...].astype(jnp.float32)
-    at = pl.multiple_of(index_ref[0] * share, share)
+    found = jnp.dot(mix_ref[...], rows_ref[...], preferred_element_type=jnp.float32)
+    at = pl.multiple_of(lax.axis_index("tp") * share, share)
     base = residual_ref[:, pl.ds(at, share)].astype(jnp.float32) + shared_ref[...]
     for chunk in range(chunks):
-        routed = base[:, chunk * 128 : (chunk + 1) * 128]
-        for slot in range(2):
-            rows = wide_v[pl.ds(slot * chunks + chunk, experts, stride=quads), :]
-            routed += jnp.dot(
-                combine_ref[slot],
-                rows,
-                preferred_element_type=jnp.float32,
-                precision=lax.Precision.HIGHEST,
-            )
-        out_ref[:, chunk * 128 : (chunk + 1) * 128] = routed.astype(jnp.bfloat16)
+        high = found[chunk * 32 : chunk * 32 + seq_rows]
+        low = found[(chunks + chunk) * 32 : (chunks + chunk) * 32 + seq_rows]
+        total = base[:, chunk * 128 : (chunk + 1) * 128] + (high + low)
+        out_ref[:, chunk * 128 : (chunk + 1) * 128] = total.astype(jnp.bfloat16)
 
 
 def state_kernel(
     key_unit_ref,
     update_ref,
     keep_ref,
+    combine_ref,
     state_hbm,
     next_hbm,
+    mix_ref,
     state_v,
     next_v,
     sems,
@@ -305,6 +295,24 @@
     ]
     for copy in loads:
         copy.start()
+    slots, _, experts = combine_ref.shape
+    chunks = mix_ref.shape[0] // 64
+    spread = slots * chunks * experts
+    lane = lax.broadcasted_iota(jnp.int32, (experts, spread), 1)
+    place = lax.broadcasted_iota(jnp.int32, (experts, spread), 0)
+    expand = jnp.where(lane // (slots * chunks) == place, 1.0, 0.0).astype(jnp.bfloat16)
+    member = lax.broadcasted_iota(jnp.int32, (seq_rows, spread), 1) % (slots * chunks)
+    mix_ref[...] = jnp.zeros(mix_ref.shape, mix_ref.dtype)
+    for slot in range(slots):
+        full = combine_ref[slot]
+        high = full.astype(jnp.bfloat16)
+        low = (full - high.astype(jnp.float32)).astype(jnp.bfloat16)
+        for part, term in enumerate((high, low)):
+            grown = jnp.dot(term, expand, preferred_element_type=jnp.float32)
+            for chunk in range(chunks):
+                at = (part * chunks + chunk) * 32
+                kept = jnp.where(member == slot * chunks + chunk, grown, 0.0)
+                mix_ref[at : at + seq_rows, :] += kept.astype(jnp.bfloat16)
     key_cols = columns_of(key_unit_ref[...])
     for part, (at, size) in enumerate(spans):
         loads[part].wait()
@@ -320,10 +328,6 @@
 
 def vmem():
     return pl.BlockSpec(memory_space=pltpu.VMEM)
-
-
-def smem():
-    return pl.BlockSpec(memory_space=pltpu.SMEM)
 
 
 def anywhere():
@@ -363,8 +367,7 @@
     ep_count = lax.axis_size("ep")
     share_width = model_width // tp_count
     hidden = expert_gate.shape[2]
-    tp_index = lax.axis_index("tp")
-    parity = (tp_index % 2).astype(jnp.int32).reshape(1)
+    quads = 2 * (share_width // 128)
     f32, bf16 = jnp.float32, jnp.bfloat16
     state = delta_state.reshape(seq_rows, head_dim, head_dim)
     small = pltpu.VMEM((seq_rows, head_dim), f32)
@@ -377,10 +380,10 @@
             small,
             pltpu.VMEM((seq_rows, ep_count), bf16),
             pltpu.VMEM((2, seq_rows, ep_count), f32),
-            jax.ShapeDtypeStruct((3 * model_width, hidden), bf16),
-        ],
-        in_specs=[smem()] + [anywhere()] * 17,
-        out_specs=[vmem()] * 6 + [anywhere()],
+            pltpu.VMEM((3 * model_width // 2, 2 * hidden), bf16),
+        ],
+        in_specs=[anywhere()] * 17,
+        out_specs=[anywhere()] + [vmem()] * 6,
         scratch_shapes=[
             pltpu.VMEM((seq_rows, model_width), bf16),
             pltpu.VMEM((1, model_width), f32),
@@ -396,13 +399,12 @@
             pltpu.VMEM((model_width, head_dim), bf16),
             pltpu.VMEM((seq_rows, head_dim, head_dim), f32),
             pltpu.VMEM((head_dim, model_width), bf16),
-            pltpu.VMEM((3 * model_width, hidden), bf16),
+            pltpu.VMEM((tp_count, seq_rows, model_width), bf16),
             pltpu.VMEM((seq_rows, head_dim), f32),
             pltpu.VMEM((seq_rows, head_dim), f32),
-            pltpu.SemaphoreType.DMA((17 + model_width // hidden,)),
+            pltpu.SemaphoreType.DMA((17 + model_width // (2 * hidden),)),
         ],
     )(
-        parity,
         tokens,
         mixer_gain.reshape(1, model_width),
         write_weight.reshape(1, model_width),
@@ -422,17 +424,22 @@
         expert_down[0],
     )
     gathered = lax.all_to_all(partials, "tp", 0, 0, tiled=True)
-    next_state = pl.pallas_call(
+    next_state, mix = pl.pallas_call(
         state_kernel,
-        out_shape=jax.ShapeDtypeStruct((seq_rows, head_dim, head_dim), f32),
-        in_specs=[vmem()] * 3 + [anywhere()],
-        out_specs=anywhere(),
+        out_shape=[
+            jax.ShapeDtypeStruct((seq_rows, head_dim, head_dim), f32),
+            pltpu.VMEM((64 * (share_width // 128), ep_count * quads), bf16),
+        ],
+        in_specs=[vmem()] * 4 + [anywhere()],
+        out_specs=[anywhere(), vmem()],
         scratch_shapes=[
             pltpu.VMEM((seq_rows, head_dim, head_dim), f32),
             pltpu.VMEM((seq_rows, head_dim, head_dim), f32),
             pltpu.SemaphoreType.DMA((4,)),
         ],
-    )(in_vmem(key_unit), in_vmem(update), in_vmem(keep), state)
+    )(
+        in_vmem(key_unit), in_vmem(update), in_vmem(keep), in_vmem(combine), state
+    )
     other = lax.ppermute(packed, "tp", [(i, i ^ 1) for i in range(tp_count)])
     lanes = model_width // 128
     residual, expert_input, outgoing = pl.pallas_call(
@@ -473,7 +480,6 @@
         in_vmem(shared_partial),
     )
     parts = lax.all_to_all(blocks, "tp", 0, 0, tiled=True)
-    quads = 2 * (share_width // 128)
     expert_share, shared_out = pl.pallas_call(
         share_kernel,
         out_shape=[
@@ -488,13 +494,11 @@
     layer_out = pl.pallas_call(
         final_kernel,
         out_shape=jax.ShapeDtypeStruct((seq_rows, share_width), bf16),
-        in_specs=[smem()] + [vmem()] * 4,
+        in_specs=[vmem()] * 4,
         out_specs=vmem(),
-        scratch_shapes=[pltpu.VMEM((ep_count * quads, 128), f32)],
     )(
-        tp_index.astype(jnp.int32).reshape(1),
         in_vmem(returned.reshape(ep_count * quads, 128)),
-        in_vmem(combine),
+        in_vmem(mix),
         in_vmem(residual),
         in_vmem(shared_out),
     )

time: 98.5 us -> 97.1 us (0.986)
  Pallas kernels: 10.5 us -> 9.28 us
where the time goes in v5:
time: 97.1 us; the launch traced here: 96.7 us
  blocking collectives  30.2 us (31%)
  starting transfers between devices  29.4 us (30%)
  waiting for transfers between devices  25.2 us (26%)
  Pallas kernels  9.28 us (10%)
  between operations  2.09 us (2%)
    all_to_all x1, blocking collectives, per_device(): gathered = lax.all_to_all(partials, 'tp', 0, 0, tiled=True)  21.2 us
    all_to_all x1, starting transfers between devices, per_device(): lax.all_to_all(outgoing.reshape(ep_count, lanes, 128), 'ep', 0, 0, tiled=...  18.7 us
    all_to_all x1, waiting for transfers between devices, per_device(): lax.all_to_all(outgoing.reshape(ep_count, lanes, 128), 'ep', 0, 0, tiled=...  14.8 us
    all_to_all x1, waiting for transfers between devices, per_device(): lax.all_to_all(expert_share.reshape(ep_count, quads, 128), 'ep', 0, 0, ti...  10.4 us
    all_to_all x1, blocking collectives, per_device(): parts = lax.all_to_all(blocks, 'tp', 0, 0, tiled=True)  9.02 us
    all_to_all x1, starting transfers between devices, per_device(): lax.all_to_all(expert_share.reshape(ep_count, quads, 128), 'ep', 0, 0, ti...  6.61 us
    ppermute x1, starting transfers between devices, per_device(): other = lax.ppermute(packed, 'tp', [(i, i ^ 1) for i in range(tp_count)])  4.07 us
    pallas_call x1, Pallas kernels, per_device(): pl.pallas_call(mixer_kernel, out_shape=[jax.ShapeDtypeStruct((tp_count, s...  3.78 us
  transfers between devices with their start and end apart: 3, of which 2 were waited for; matrix products, arithmetic and copies ran while one was open for 0% of the time, Pallas kernels for 4%

profile of v5, /device:TPU:1, one launch (start us, length us, event | category | flops | bytes accessed | tf_op | source)
XLA Modules:
  0.0 96.7 jit_solution(11768037874787311933)
XLA Ops:
  0.6 0.0 copy-start
  2.0 0.0 copy-start.1
  2.0 0.0 copy-start.2
  2.0 3.8 %shard_map.212 = (bf16[4,18,1024]{2,1,0:T(8,128)(2,1)}, f32[18,128]{1,0:T(8,128)S(1)}, f32[18,128]{1,0:T(8,128)S(1)}, f32[18,128]{1,0:T(8,128)S(1)}, bf16[18,128...) custom-call(bf16[18,1024]{1,0:T(8,128)(2,1)} %tokens_ref.1, f32[1,1024]{1,0:T(1,128)} %bitcast.32, ...), custom_call_target="tpu_custom_call" | custom-call | tf_op jit(solution)/shard_map/pallas_call | solution.py:374
  5.8 0.0 copy-start.3
  5.8 0.0 copy-start.4
  5.8 4.1 %collective-permute-start = (bf16[1536,256]{1,0:T(8,128)(2,1)S(1)}, bf16[1536,256]{1,0:T(8,128)(2,1)S(1)}, u32[]{:S(2)}, u32[]{:S(2)}) collective-permute-start(bf16[1536,256]{1,0:T(8,128)(2,1)S(1)} %get-tuple-element.19.own_ref), channel_id=1, source_target_pairs={{0,1},{1,0},{2,3},{3,2},{4,5},{5,4},{6,7},{7,6},{8,9},{9,8},{10,11... | collective-permute-start | bytes 2359304 | tf_op jit(solution)/shard_map/ppermute | solution.py:443
  9.9 21.2 %all_to_all.20.gathered_ref = bf16[4,18,1024]{2,1,0:T(8,128)(2,1)S(1)} all-to-all(bf16[4,18,1024]{2,1,0:T(8,128)(2,1)} %get-tuple-element.16), channel_id=1, replica_groups=mesh['ep'=128,'tp'=4] {'tp'}, dimensions={0} | all-to-all | bytes 294912 | tf_op jit(solution)/shard_map/all_to_all | solution.py:426
  31.1 0.0 copy-done.1
  31.1 0.0 copy-done.2
  31.1 1.1 %shard_map.213 = (bf16[18,1024]{1,0:T(8,128)(2,1)S(1)}, bf16[18,1024]{1,0:T(8,128)(2,1)S(1)}, bf16[1024,128]{1,0:T(8,128)(2,1)}) custom-call(bf16[4,18,1024]{2,1,0:T(8,128)(2,1)S(1)} %all_to_all.20.gathered_ref, bf16[18,1024]{1,0:T(8,128)(2,1)S(1)} %copy-done.1, f32[1,1024]{1,0:T(1,128)S(1)} %bitcast.25, bf16[18,128]{1,0:T(8,128)(2,1)S(1)} %get-tuple-element.17.dispatch_ref), custom_call_target="tpu_custom_call" | custom-call | tf_op jit(solution)/shard_map/pallas_call | solution.py:445
  32.2 18.7 %all-to-all-start.1 = ((bf16[128,8,128]{2,1,0:T(8,128)(2,1)}), bf16[128,8,128]{2,1,0:T(8,128)(2,1)S(1)}, u32[]{:S(2)}, u32[]{:S(2)}) async-start(bf16[128,8,128]{2,1,0:T(8,128)(2,1)} %bitcast.31), calls=%async_computation.1 | async-start | bytes 524288 | tf_op jit(solution)/shard_map/all_to_all | solution.py:461
  50.9 0.0 copy-done.3
  50.9 0.2 fusion.8
  51.1 0.3 convolution_convert_fusion.shared_ref
  51.4 14.8 %all-to-all-done.1 = bf16[128,8,128]{2,1,0:T(8,128)(2,1)S(1)} async-done(((bf16[128,8,128]{2,1,0:T(8,128)(2,1)}), bf16[128,8,128]{2,1,0:T(8,128)(2,1)S(1)}, u32[]{:S(2)}, u32[]{:S(2)}) %all-to-all-start.1) | async-done | bytes 262176 | tf_op jit(solution)/shard_map/all_to_all | solution.py:461
  66.2 0.0 collective-permute-done.other_ref
  66.2 0.6 shard_map.214
  66.7 9.0 %all_to_all.21.parts_ref = bf16[4,146,256]{2,1,0:T(8,128)(2,1)S(1)} all-to-all(bf16[4,146,256]{2,1,0:T(8,128)(2,1)S(1)} %shard_map.214), channel_id=1, replica_groups=mesh['ep'=128,'tp'=4] {'tp'}, dimensions={0} | all-to-all | bytes 598016 | tf_op jit(solution)/shard_map/all_to_all | solution.py:482
  75.8 0.7 shard_map.215
  76.5 6.6 %all-to-all-start.3 = ((bf16[128,4,128]{2,1,0:T(4,128)(2,1)}), bf16[128,4,128]{2,1,0:T(4,128)(2,1)S(1)}, u32[]{:S(2)}, u32[]{:S(2)}) async-start(bf16[128,4,128]{2,1,0:T(4,128)(2,1)} %bitcast.13), calls=%async_computation.3 | async-start | bytes 262144 | tf_op jit(solution)/shard_map/all_to_all | solution.py:493
  83.1 2.4 %shard_map.216 = (f32[18,128,128]{2,1,0:T(8,128)}, bf16[128,512]{1,0:T(8,128)(2,1)S(1)}) custom-call(f32[18,128]{1,0:T(8,128)S(1)} %get-tuple-element.22.key_unit_ref, f32[18,128]{1,0:T(8,128)S(1)} %get-tuple-element.23.update_ref, f32[18,128]{1,0:T(8,128)S(1)} %get-tuple-element.24.keep_ref, f32[2,18,128]{2,1,0:T(8,128)S(1)} %get-tuple-element.25.combine_ref, ...), custom_call_target="tpu_custom_call" | custom-call | tf_op jit(solution)/shard_map/pallas_call | solution.py:427
  85.5 10.4 %all-to-all-done.3 = bf16[128,4,128]{2,1,0:T(4,128)(2,1)S(1)} async-done(((bf16[128,4,128]{2,1,0:T(4,128)(2,1)}), bf16[128,4,128]{2,1,0:T(4,128)(2,1)S(1)}, u32[]{:S(2)}, u32[]{:S(2)}) %all-to-all-start.3) | async-done | bytes 131104 | tf_op jit(solution)/shard_map/all_to_all | solution.py:493
  95.9 0.8 shard_map.217
  (2 shorter events, 0.0 us)
Async XLA Ops:
  0.6 50.5 %copy-start = (bf16[128,1024]{1,0:T(8,128)(2,1)S(1)}, bf16[128,1024]{1,0:T(8,128)(2,1)}, u32[]{:S(2)}) copy-start(bf16[128,1024]{1,0:T(8,128)(2,1)} %param.41) | copy-start | bytes 786436
  2.0 29.1 %copy-start.1 = (bf16[18,1024]{1,0:T(8,128)(2,1)S(1)}, bf16[18,1024]{1,0:T(8,128)(2,1)}, u32[]{:S(2)}) copy-start(bf16[18,1024]{1,0:T(8,128)(2,1)} %tokens_ref.1) | copy-start | bytes 110596
  2.0 29.1 %copy-start.2 = (f32[1024]{0:T(1024)S(1)}, f32[1024]{0:T(1024)}, u32[]{:S(2)}) copy-start(f32[1024]{0:T(1024)} %param.33) | copy-start | bytes 12292
  5.8 45.1 %copy-start.3 = (bf16[1024,128]{1,0:T(8,128)(2,1)S(1)}, bf16[1024,128]{1,0:T(8,128)(2,1)}, u32[]{:S(2)}) copy-start(bf16[1024,128]{1,0:T(8,128)(2,1)} %param.39) | copy-start | bytes 786436
  5.8 45.3 %copy-start.4 = (bf16[1024,128]{1,0:T(8,128)(2,1)S(1)}, bf16[1024,128]{1,0:T(8,128)(2,1)}, u32[]{:S(2)}) copy-start(bf16[1024,128]{1,0:T(8,128)(2,1)} %param.40) | copy-start | bytes 786436
  5.8 60.3 %collective-permute-start = (bf16[1536,256]{1,0:T(8,128)(2,1)S(1)}, bf16[1536,256]{1,0:T(8,128)(2,1)S(1)}, u32[]{:S(2)}, u32[]{:S(2)}) collective-permute-start(bf16[1536,256]{1,0:T(8,128)(2,1)S(1)} %get-tuple-element.19.own_ref), channel_id=1, source_target_pairs={{0,1},{1,0},{2,3},{3,2},{4,5},{5,4},{6,7},{7,6},{8,9},{9,8},{10,11... | collective-permute-start | bytes 2359304 | tf_op jit(solution)/shard_map/ppermute | solution.py:443
  32.2 34.0 %all-to-all-start.1 = ((bf16[128,8,128]{2,1,0:T(8,128)(2,1)}), bf16[128,8,128]{2,1,0:T(8,128)(2,1)S(1)}, u32[]{:S(2)}, u32[]{:S(2)}) async-start(bf16[128,8,128]{2,1,0:T(8,128)(2,1)} %bitcast.31), calls=%async_computation.1 | async-start | bytes 524288 | tf_op jit(solution)/shard_map/all_to_all | solution.py:461
  76.5 19.4 %all-to-all-start.3 = ((bf16[128,4,128]{2,1,0:T(4,128)(2,1)}), bf16[128,4,128]{2,1,0:T(4,128)(2,1)S(1)}, u32[]{:S(2)}, u32[]{:S(2)}) async-start(bf16[128,4,128]{2,1,0:T(4,128)(2,1)} %bitcast.13), calls=%async_computation.3 | async-start | bytes 262144 | tf_op jit(solution)/shard_map/all_to_all | solution.py:493

commit v6 on v5

--- a/solution.py
+++ b/solution.py
@@ -43,11 +43,9 @@
     up_hbm,
     down_hbm,
     partial_hbm,
-    key_unit_ref,
-    update_ref,
-    keep_ref,
+    next_hbm,
     dispatch_ref,
-    combine_ref,
+    mix_ref,
     packed_ref,
     tokens_v,
     gain_v,
@@ -62,6 +60,7 @@
     key_v,
     value_v,
     state_v,
+    next_v,
     out_weight_v,
     partial_v,
     found_k,
@@ -127,10 +126,8 @@
     row_b = lax.broadcasted_iota(jnp.int32, (seq_rows, seq_rows), 1)
     below = jnp.where(row_b < row_a, 1.0, 0.0)
     earlier = jnp.dot(below, named, preferred_element_type=jnp.float32)
-    slot = earlier.astype(jnp.int32)
-    dispatch_ref[...] = jnp.where(slot == lax.axis_index("tp") % 2, named, 0.0).astype(jnp.bfloat16)
-    combine_ref[0] = jnp.where(slot == 0, mix, 0.0)
-    combine_ref[1] = jnp.where(slot == 1, mix, 0.0)
+    chosen = earlier.astype(jnp.int32)
+    dispatch_ref[...] = jnp.where(chosen == lax.axis_index("tp") % 2, named, 0.0).astype(jnp.bfloat16)
     loads[8].wait()
     query_raw = jnp.dot(normed, query_v[...], preferred_element_type=jnp.float32)
     loads[9].wait()
@@ -167,12 +164,42 @@
         partial_v[copy_number] = partial
     store = pltpu.make_async_copy(partial_v, partial_hbm, sems.at[0])
     store.start()
-    key_unit_ref[...] = key_unit
-    update_ref[...] = update
-    keep_ref[...] = jnp.broadcast_to(keep, keep_ref.shape)
+    keep_rows = jnp.broadcast_to(keep, update.shape)
+    stores = [store]
+    step = 3
+    for at in range(0, seq_rows, step):
+        for row in range(at, at + step):
+            next_v[row] = (
+                keep_rows[row : row + 1, :] * state_v[row]
+                + key_cols[:, row : row + 1] * update[row : row + 1, :]
+            )
+        store = pltpu.make_async_copy(
+            next_v.at[pl.ds(at, step)], next_hbm.at[pl.ds(at, step)], sems.at[1 + at // step]
+        )
+        store.start()
+        stores.append(store)
+    slots, experts = 2, dispatch_ref.shape[1]
+    chunks = mix_ref.shape[0] // 64
+    spread = slots * chunks * experts
+    lane = lax.broadcasted_iota(jnp.int32, (experts, spread), 1)
+    place = lax.broadcasted_iota(jnp.int32, (experts, spread), 0)
+    expand = jnp.where(lane // (slots * chunks) == place, 1.0, 0.0).astype(jnp.bfloat16)
+    member = lax.broadcasted_iota(jnp.int32, (seq_rows, spread), 1) % (slots * chunks)
+    mix_ref[...] = jnp.zeros(mix_ref.shape, mix_ref.dtype)
+    for slot in range(slots):
+        full = jnp.where(chosen == slot, mix, 0.0)
+        high = full.astype(jnp.bfloat16)
+        low = (full - high.astype(jnp.float32)).astype(jnp.bfloat16)
+        for part, term in enumerate((high, low)):
+            grown = jnp.dot(term, expand, preferred_element_type=jnp.float32)
+            for chunk in range(chunks):
+                at = (part * chunks + chunk) * 32
+                kept = jnp.where(member == slot * chunks + chunk, grown, 0.0)
+                mix_ref[at : at + seq_rows, :] += kept.astype(jnp.bfloat16)
     for copy in loads[15:]:
         copy.wait()
-    store.wait()
+    for copy in stores:
+        copy.wait()
 
 
 def rows_kernel(
@@ -266,66 +293,6 @@
         out_ref[:, chunk * 128 : (chunk + 1) * 128] = total.astype(jnp.bfloat16)
 
 
-def state_kernel(
-    key_unit_ref,
-    update_ref,
-    keep_ref,
-    combine_ref,
-    state_hbm,
-    next_hbm,
-    mix_ref,
-    state_v,
-    next_v,
-    sems,
-):
-    seq_rows = key_unit_ref.shape[0]
-    half = seq_rows // 2
-    spans = [(0, half), (half, seq_rows - half)]
-    loads = [
-        pltpu.make_async_copy(
-            state_hbm.at[pl.ds(at, size)], state_v.at[pl.ds(at, size)], sems.at[i]
-        )
-        for i, (at, size) in enumerate(spans)
-    ]
-    stores = [
-        pltpu.make_async_copy(
-            next_v.at[pl.ds(at, size)], next_hbm.at[pl.ds(at, size)], sems.at[2 + i]
-        )
-        for i, (at, size) in enumerate(spans)
-    ]
-    for copy in loads:
-        copy.start()
-    slots, _, experts = combine_ref.shape
-    chunks = mix_ref.shape[0] // 64
-    spread = slots * chunks * experts
-    lane = lax.broadcasted_iota(jnp.int32, (experts, spread), 1)
-    place = lax.broadcasted_iota(jnp.int32, (experts, spread), 0)
-    expand = jnp.where(lane // (slots * chunks) == place, 1.0, 0.0).astype(jnp.bfloat16)
-    member = lax.broadcasted_iota(jnp.int32, (seq_rows, spread), 1) % (slots * chunks)
-    mix_ref[...] = jnp.zeros(mix_ref.shape, mix_ref.dtype)
-    for slot in range(slots):
-        full = combine_ref[slot]
-        high = full.astype(jnp.bfloat16)
-        low = (full - high.astype(jnp.float32)).astype(jnp.bfloat16)
-        for part, term in enumerate((high, low)):
-            grown = jnp.dot(term, expand, preferred_element_type=jnp.float32)
-            for chunk in range(chunks):
-                at = (part * chunks + chunk) * 32
-                kept = jnp.where(member == slot * chunks + chunk, grown, 0.0)
-                mix_ref[at : at + seq_rows, :] += kept.astype(jnp.bfloat16)
-    key_cols = columns_of(key_unit_ref[...])
-    for part, (at, size) in enumerate(spans):
-        loads[part].wait()
-        for row in range(at, at + size):
-            next_v[row] = (
-                keep_ref[row : row + 1, :] * state_v[row]
-                + key_cols[:, row : row + 1] * update_ref[row : row + 1, :]
-            )
-        stores[part].start()
-    for copy in stores:
-        copy.wait()
-
-
 def vmem():
     return pl.BlockSpec(memory_space=pltpu.VMEM)
 
@@ -370,20 +337,17 @@
     quads = 2 * (share_width // 128)
     f32, bf16 = jnp.float32, jnp.bfloat16
     state = delta_state.reshape(seq_rows, head_dim, head_dim)
-    small = pltpu.VMEM((seq_rows, head_dim), f32)
-    partials, key_unit, update, keep, dispatch, combine, packed = pl.pallas_call(
+    partials, next_state, dispatch, mix, packed = pl.pallas_call(
         mixer_kernel,
         out_shape=[
             jax.ShapeDtypeStruct((tp_count, seq_rows, model_width), bf16),
-            small,
-            small,
-            small,
+            jax.ShapeDtypeStruct(state.shape, f32),
             pltpu.VMEM((seq_rows, ep_count), bf16),
-            pltpu.VMEM((2, seq_rows, ep_count), f32),
+            pltpu.VMEM((64 * (share_width // 128), ep_count * quads), bf16),
             pltpu.VMEM((3 * model_width // 2, 2 * hidden), bf16),
         ],
         in_specs=[anywhere()] * 17,
-        out_specs=[anywhere()] + [vmem()] * 6,
+        out_specs=[anywhere()] * 2 + [vmem()] * 3,
         scratch_shapes=[
             pltpu.VMEM((seq_rows, model_width), bf16),
             pltpu.VMEM((1, model_width), f32),
@@ -397,6 +361,7 @@
             pltpu.VMEM((model_width, head_dim), bf16),
             pltpu.VMEM((model_width, head_dim), bf16),
             pltpu.VMEM((model_width, head_dim), bf16),
+            pltpu.VMEM((seq_rows, head_dim, head_dim), f32),
             pltpu.VMEM((seq_rows, head_dim, head_dim), f32),
             pltpu.VMEM((head_dim, model_width), bf16),
             pltpu.VMEM((tp_count, seq_rows, model_width), bf16),
@@ -424,22 +389,6 @@
         expert_down[0],
     )
     gathered = lax.all_to_all(partials, "tp", 0, 0, tiled=True)
-    next_state, mix = pl.pallas_call(
-        state_kernel,
-        out_shape=[
-            jax.ShapeDtypeStruct((seq_rows, head_dim, head_dim), f32),
-            pltpu.VMEM((64 * (share_width // 128), ep_count * quads), bf16),
-        ],
-        in_specs=[vmem()] * 4 + [anywhere()],
-        out_specs=[anywhere(), vmem()],
-        scratch_shapes=[
-            pltpu.VMEM((seq_rows, head_dim, head_dim), f32),
-            pltpu.VMEM((seq_rows, head_dim, head_dim), f32),
-            pltpu.SemaphoreType.DMA((4,)),
-        ],
-    )(
-        in_vmem(key_unit), in_vmem(update), in_vmem(keep), in_vmem(combine), state
-    )
     other = lax.ppermute(packed, "tp", [(i, i ^ 1) for i in range(tp_count)])
     lanes = model_width // 128
     residual, expert_input, outgoing = pl.pallas_call(
@@ -447,7 +396,7 @@
         out_shape=[
             pltpu.VMEM((seq_rows, model_width), bf16),
             pltpu.VMEM((seq_rows, model_width), bf16),
-            jax.ShapeDtypeStruct((ep_count * lanes, 128), bf16),
+            pltpu.VMEM((ep_count * lanes, 128), bf16),
         ],
         in_specs=[vmem()] * 4,
         out_specs=[vmem()] * 3,
@@ -458,12 +407,13 @@
         in_vmem(channel_gain.reshape(1, model_width)),
         in_vmem(dispatch),
     )
-    received = lax.all_to_all(outgoing.reshape(ep_count, lanes, 128), "ep", 0, 0, tiled=True)
     shared_act = (
         jax.nn.silu(jnp.dot(expert_input, shared_gate, preferred_element_type=f32))
         * jnp.dot(expert_input, shared_up, preferred_element_type=f32)
     ).astype(bf16)
     shared_partial = jnp.dot(shared_act, shared_down, preferred_element_type=f32).astype(bf16)
+    outgoing, shared_partial = lax.optimization_barrier((outgoing, shared_partial))
+    received = lax.all_to_all(outgoing.reshape(ep_count, lanes, 128), "ep", 0, 0, tiled=True)
     blocks = pl.pallas_call(
         expert_kernel,
         out_shape=pltpu.VMEM((tp_count, ep_count + seq_rows, share_width), bf16),

time: 97.1 us -> 81.1 us (0.84)
  blocking collectives: 30.2 us -> 62.3 us
  waiting for transfers between devices: 25.2 us -> 1.81 us
  starting transfers between devices: 29.4 us -> 8.2 us
  Pallas kernels: 9.28 us -> 5.93 us
    all_to_all x1 -> x2, blocking collectives: 21.2 us -> 52.9 us  [the longest x1 34 us: per_device(): lax.all_to_all(outgoing.reshape(ep_count, lanes, 128), 'ep', 0, 0, tiled=...]
    all_to_all x2 -> x1, waiting for transfers between devices: 25.2 us -> 1.81 us  [per_device(): gathered = lax.all_to_all(partials, 'tp', 0, 0, tiled=True)]
    all_to_all x2 -> x1, starting transfers between devices: 25.3 us -> 4.84 us  [per_device(): gathered = lax.all_to_all(partials, 'tp', 0, 0, tiled=True)]
    pallas_call x1 -> x0, Pallas kernels: 2.39 us -> none  [per_device(): pl.pallas_call(state_kernel, out_shape=[jax.ShapeDtypeStruct((seq_rows, h...]
  transfers between devices with their start and end apart: 3 -> 2, of which waited for: 2 -> 1; matrix products, arithmetic and copies ran while one was open for 0% -> 1% of each run, Pallas kernels for 4% -> 0%
where the time goes in v6:
time: 81.1 us; the launch traced here: 80.8 us
  blocking collectives  62.3 us (77%)
  starting transfers between devices  8.2 us (10%)
  Pallas kernels  5.93 us (7%)
  between operations  2.08 us (3%)
  waiting for transfers between devices  1.81 us (2%)
    all_to_all x1, blocking collectives, per_device(): lax.all_to_all(outgoing.reshape(ep_count, lanes, 128), 'ep', 0, 0, tiled=...  34 us
    all_to_all x1, blocking collectives, per_device(): lax.all_to_all(expert_share.reshape(ep_count, quads, 128), 'ep', 0, 0, ti...  18.9 us
    all_to_all x1, blocking collectives, per_device(): parts = lax.all_to_all(blocks, 'tp', 0, 0, tiled=True)  9.37 us
    all_to_all x1, starting transfers between devices, per_device(): gathered = lax.all_to_all(partials, 'tp', 0, 0, tiled=True)  4.84 us
    pallas_call x1, Pallas kernels, per_device(): pl.pallas_call(mixer_kernel, out_shape=[jax.ShapeDtypeStruct((tp_count, s...  4.17 us
    ppermute x1, starting transfers between devices, per_device(): other = lax.ppermute(packed, 'tp', [(i, i ^ 1) for i in range(tp_count)])  3.36 us
    all_to_all x1, waiting for transfers between devices, per_device(): gathered = lax.all_to_all(partials, 'tp', 0, 0, tiled=True)  1.81 us
  transfers between devices with their start and end apart: 2, of which 1 were waited for; matrix products, arithmetic and copies ran while one was open for 1% of the time, Pallas kernels for 0%

profile of v6, /device:TPU:1, one launch (start us, length us, event | category | flops | bytes accessed | tf_op | source)
XLA Modules:
  0.0 80.8 jit_solution(4218607131805170527)
XLA Ops:
  0.6 0.0 copy-start
  2.0 0.0 copy-start.1
  2.0 0.0 copy-start.2
  2.0 0.0 copy-start.3
  2.0 0.0 copy-start.4
  2.0 4.2 %shard_map.212 = (bf16[4,18,1024]{2,1,0:T(8,128)(2,1)}, f32[18,128,128]{2,1,0:T(8,128)}, bf16[18,128]{1,0:T(8,128)(2,1)S(1)}, bf16[128,512]{1,0:T(8,128)(2,1)S(1)}, bf16[1536,256]{1,0:T(8,128)(2,1)S(1)}) custom-call(bf16[18,1024]{1,0:T(8,128)(2,1)} %tokens_ref.1, f32[1,1024]{1,0:T(1,128)} %bitcast.32, bf16[1,1024]{1,0:T(2,128)(2,1)} %bitcast.33, ...), custom_call_target="tpu_custom_call" | custom-call | tf_op jit(solution)/shard_map/pallas_call | solution.py:340
  6.2 4.8 %all-to-all-start = ((bf16[4,18,1024]{2,1,0:T(8,128)(2,1)}), bf16[4,18,1024]{2,1,0:T(8,128)(2,1)S(1)}, u32[]{:S(2)}, u32[]{:S(2)}) async-start(bf16[4,18,1024]{2,1,0:T(8,128)(2,1)} %get-tuple-element.14), calls=%async_computation | async-start | bytes 393216 | tf_op jit(solution)/shard_map/all_to_all | solution.py:391
  11.0 3.4 %collective-permute-start = (bf16[1536,256]{1,0:T(8,128)(2,1)S(1)}, bf16[1536,256]{1,0:T(8,128)(2,1)S(1)}, u32[]{:S(2)}, u32[]{:S(2)}) collective-permute-start(bf16[1536,256]{1,0:T(8,128)(2,1)S(1)} %get-tuple-element.19.own_ref), channel_id=1, source_target_pairs={{0,1},{1,0},{2,3},{3,2},{4,5},{5,4},{6,7},{7,6},{8,9},{9,8},{10,11... | collective-permute-start | bytes 2359304 | tf_op jit(solution)/shard_map/ppermute | solution.py:392
  14.4 1.8 %all-to-all-done.gathered_ref = bf16[4,18,1024]{2,1,0:T(8,128)(2,1)S(1)} async-done(((bf16[4,18,1024]{2,1,0:T(8,128)(2,1)}), bf16[4,18,1024]{2,1,0:T(8,128)(2,1)S(1)}, u32[]{:S(2)}, u32[]{:S(2)}) %all-to-all-start) | async-done | bytes 147488 | tf_op jit(solution)/shard_map/all_to_all | solution.py:391
  16.2 0.0 copy-done.1
  16.2 0.0 copy-done.2
  16.2 0.4 shard_map.213
  16.6 0.0 copy-done.3
  16.6 0.2 fusion.8
  16.8 0.0 copy-done
  16.8 0.0 copy-done.4
  16.8 0.3 convolution_convert_fusion.shared_ref
  17.1 34.0 %all_to_all.20 = bf16[128,8,128]{2,1,0:T(8,128)(2,1)S(1)} all-to-all(bf16[128,8,128]{2,1,0:T(8,128)(2,1)S(1)} %bitcast.25), channel_id=1, replica_groups=mesh['ep'=128,'tp'=4] {'ep'}, dimensions={0} | all-to-all | bytes 524288 | tf_op jit(solution)/shard_map/all_to_all | solution.py:416
  51.1 0.0 collective-permute-done.other_ref
  51.1 0.6 shard_map.214
  51.7 9.4 %all_to_all.21.parts_ref = bf16[4,146,256]{2,1,0:T(8,128)(2,1)S(1)} all-to-all(bf16[4,146,256]{2,1,0:T(8,128)(2,1)S(1)} %shard_map.214), channel_id=1, replica_groups=mesh['ep'=128,'tp'=4] {'tp'}, dimensions={0} | all-to-all | bytes 598016 | tf_op jit(solution)/shard_map/all_to_all | solution.py:432
  61.1 18.9 %all_to_all.22 = bf16[128,4,128]{2,1,0:T(4,128)(2,1)S(1)} all-to-all(bf16[128,4,128]{2,1,0:T(4,128)(2,1)S(1)} %bitcast.26), channel_id=1, replica_groups=mesh['ep'=128,'tp'=4] {'ep'}, dimensions={0} | all-to-all | bytes 262144 | tf_op jit(solution)/shard_map/all_to_all | solution.py:443
  80.0 0.8 shard_map.216
  (1 shorter events, 0.0 us)
Async XLA Ops:
  0.6 16.1 %copy-start = (bf16[128,1024]{1,0:T(8,128)(2,1)S(1)}, bf16[128,1024]{1,0:T(8,128)(2,1)}, u32[]{:S(2)}) copy-start(bf16[128,1024]{1,0:T(8,128)(2,1)} %param.41) | copy-start | bytes 786436
  2.0 14.2 %copy-start.1 = (bf16[18,1024]{1,0:T(8,128)(2,1)S(1)}, bf16[18,1024]{1,0:T(8,128)(2,1)}, u32[]{:S(2)}) copy-start(bf16[18,1024]{1,0:T(8,128)(2,1)} %tokens_ref.1) | copy-start | bytes 110596
  2.0 14.2 %copy-start.2 = (f32[1024]{0:T(1024)S(1)}, f32[1024]{0:T(1024)}, u32[]{:S(2)}) copy-start(f32[1024]{0:T(1024)} %param.33) | copy-start | bytes 12292
  2.0 14.6 %copy-start.3 = (bf16[1024,128]{1,0:T(8,128)(2,1)S(1)}, bf16[1024,128]{1,0:T(8,128)(2,1)}, u32[]{:S(2)}) copy-start(bf16[1024,128]{1,0:T(8,128)(2,1)} %param.39) | copy-start | bytes 786436
  2.0 14.8 %copy-start.4 = (bf16[1024,128]{1,0:T(8,128)(2,1)S(1)}, bf16[1024,128]{1,0:T(8,128)(2,1)}, u32[]{:S(2)}) copy-start(bf16[1024,128]{1,0:T(8,128)(2,1)} %param.40) | copy-start | bytes 786436
  6.2 10.0 %all-to-all-start = ((bf16[4,18,1024]{2,1,0:T(8,128)(2,1)}), bf16[4,18,1024]{2,1,0:T(8,128)(2,1)S(1)}, u32[]{:S(2)}, u32[]{:S(2)}) async-start(bf16[4,18,1024]{2,1,0:T(8,128)(2,1)} %get-tuple-element.14), calls=%async_computation | async-start | bytes 393216 | tf_op jit(solution)/shard_map/all_to_all | solution.py:391
  11.0 40.1 %collective-permute-start = (bf16[1536,256]{1,0:T(8,128)(2,1)S(1)}, bf16[1536,256]{1,0:T(8,128)(2,1)S(1)}, u32[]{:S(2)}, u32[]{:S(2)}) collective-permute-start(bf16[1536,256]{1,0:T(8,128)(2,1)S(1)} %get-tuple-element.19.own_ref), channel_id=1, source_target_pairs={{0,1},{1,0},{2,3},{3,2},{4,5},{5,4},{6,7},{7,6},{8,9},{9,8},{10,11... | collective-permute-start | bytes 2359304 | tf_op jit(solution)/shard_map/ppermute | solution.py:392

commit v7 on v6

--- a/solution.py
+++ b/solution.py
@@ -22,6 +22,23 @@
 def columns_of(rows):
     pad = jnp.zeros((128 - rows.shape[0], rows.shape[1]), rows.dtype)
     return jnp.concatenate([rows, pad], axis=0).T
+
+
+def earlier_rows(named):
+    seq_rows = named.shape[0]
+    row_a = lax.broadcasted_iota(jnp.int32, (seq_rows, seq_rows), 0)
+    row_b = lax.broadcasted_iota(jnp.int32, (seq_rows, seq_rows), 1)
+    below = jnp.where(row_b < row_a, 1.0, 0.0)
+    return jnp.dot(below, named, preferred_element_type=jnp.float32).astype(jnp.int32)
+
+
+def picked_rows(routes, core, slot):
+    seq_rows, top_k = routes.shape
+    experts = 2 * lax.broadcasted_iota(jnp.int32, (seq_rows, 64), 1) + core
+    named = jnp.zeros((seq_rows, 64), jnp.float32)
+    for route in range(top_k):
+        named = named + jnp.where(experts == routes[:, route : route + 1], 1.0, 0.0)
+    return jnp.where(earlier_rows(named) == slot, named, 0.0).astype(jnp.bfloat16)
 
 
 def mixer_kernel(
@@ -44,7 +61,6 @@
     down_hbm,
     partial_hbm,
     next_hbm,
-    dispatch_ref,
     mix_ref,
     packed_ref,
     tokens_v,
@@ -63,11 +79,15 @@
     next_v,
     out_weight_v,
     partial_v,
+    plain_v,
+    mixed_v,
     found_k,
     found_q,
     sems,
 ):
     seq_rows = tokens_hbm.shape[0]
+    core = lax.axis_index("ep") % 2
+    tp_index = lax.axis_index("tp")
     width, hidden = gate_hbm.shape
     half = seq_rows // 2
     wide_block = 2 * hidden
@@ -122,12 +142,7 @@
         hit = expert_iota == routes[:, route : route + 1]
         named = named + jnp.where(hit, 1.0, 0.0)
         mix = mix + jnp.where(hit, scale[:, route : route + 1], 0.0)
-    row_a = lax.broadcasted_iota(jnp.int32, (seq_rows, seq_rows), 0)
-    row_b = lax.broadcasted_iota(jnp.int32, (seq_rows, seq_rows), 1)
-    below = jnp.where(row_b < row_a, 1.0, 0.0)
-    earlier = jnp.dot(below, named, preferred_element_type=jnp.float32)
-    chosen = earlier.astype(jnp.int32)
-    dispatch_ref[...] = jnp.where(chosen == lax.axis_index("tp") % 2, named, 0.0).astype(jnp.bfloat16)
+    chosen = earlier_rows(named)
     loads[8].wait()
     query_raw = jnp.dot(normed, query_v[...], preferred_element_type=jnp.float32)
     loads[9].wait()
@@ -159,9 +174,24 @@
     head_out = rms_rows(readout, head_gain_v[...]).astype(jnp.bfloat16)
     loads[14].wait()
     partial = jnp.dot(head_out, out_weight_v[...], preferred_element_type=jnp.float32)
-    partial = partial.astype(jnp.bfloat16)
+    partial = partial.astype(jnp.bfloat16).astype(jnp.float32)
+    mixed = partial + jnp.where(tp_index == 0, tokens_v[...].astype(jnp.float32), 0.0)
+    lanes = width // 128
+    top_k = routes_hbm.shape[0]
+    for lane in range(lanes):
+        part = slice(lane * 128, (lane + 1) * 128)
+        plain_v[pl.ds(lane, seq_rows, stride=lanes), :] = partial[:, part]
+        mixed_v[pl.ds(lane, seq_rows, stride=lanes), :] = mixed[:, part]
+    plain_v[seq_rows * lanes :, :] = jnp.zeros((8, 128), jnp.float32)
+    mixed_v[seq_rows * lanes :, :] = jnp.zeros((8, 128), jnp.float32)
+    names = slice(seq_rows * lanes, seq_rows * lanes + top_k)
+    plain_v[names, :seq_rows] = routes_v[...].astype(jnp.float32)
+    mixed_v[names, :seq_rows] = routes_v[...].astype(jnp.float32)
+    plain = plain_v[...].astype(jnp.bfloat16)
+    mixed = mixed_v[...].astype(jnp.bfloat16)
+    group = partial_v.shape[0] // 2
     for copy_number in range(partial_v.shape[0]):
-        partial_v[copy_number] = partial
+        partial_v[copy_number] = jnp.where(core == copy_number // group, plain, mixed)
     store = pltpu.make_async_copy(partial_v, partial_hbm, sems.at[0])
     store.start()
     keep_rows = jnp.broadcast_to(keep, update.shape)
@@ -178,7 +208,7 @@
         )
         store.start()
         stores.append(store)
-    slots, experts = 2, dispatch_ref.shape[1]
+    slots, experts = 2, 128
     chunks = mix_ref.shape[0] // 64
     spread = slots * chunks * experts
     lane = lax.broadcasted_iota(jnp.int32, (experts, spread), 1)
@@ -206,77 +236,116 @@
     gathered_ref,
     tokens_ref,
     gain_ref,
-    dispatch_ref,
     residual_ref,
     input_ref,
     rows_ref,
+    sums_v,
+    tokens_v,
     wide_v,
 ):
-    mixed = jnp.sum(gathered_ref[...].astype(jnp.float32), axis=0)
-    mixed = mixed.astype(jnp.bfloat16).astype(jnp.float32)
-    residual = (tokens_ref[...].astype(jnp.float32) + mixed).astype(jnp.bfloat16)
-    inputs = rms_rows(residual.astype(jnp.float32), gain_ref[...]).astype(jnp.bfloat16)
-    residual_ref[...] = residual
-    input_ref[...] = inputs
-    experts = dispatch_ref.shape[1]
-    picked = lax.dot_general(
-        dispatch_ref[...], inputs, (((0,), (0,)), ((), ())), preferred_element_type=jnp.float32
-    )
-    lanes = inputs.shape[1] // 128
+    seq_rows, width = tokens_ref.shape
+    padded = tokens_v.shape[0]
+    lanes = width // 128
+    core = lax.axis_index("ep") % 2
+    slot = lax.axis_index("tp") % 2
+    group = gathered_ref.shape[0] // 2
+    sent = seq_rows * lanes
+    peers = rows_ref.shape[0] // (2 * lanes)
+    tokens_v[...] = jnp.zeros(tokens_v.shape, jnp.float32)
+    tokens_v[:seq_rows, :] = tokens_ref[...].astype(jnp.float32)
+    for place in range(2):
+        first = (core if place == 0 else 1 - core) * group
+        summed = jnp.sum(gathered_ref[pl.ds(first, group), :sent].astype(jnp.float32), axis=0)
+        sums_v[place, :sent] = summed
+        sums_v[place, sent:] = jnp.zeros((padded * lanes - sent, 128), jnp.float32)
+        total = jnp.concatenate(
+            [sums_v[place, pl.ds(lane, padded, stride=lanes), :] for lane in range(lanes)],
+            axis=1,
+        )
+        if place == 0:
+            total = tokens_v[...] + total.astype(jnp.bfloat16).astype(jnp.float32)
+        names = gathered_ref[first, sent:, :].astype(jnp.float32)
+        blank = jnp.zeros((128 - names.shape[0], 128), jnp.float32)
+        routes = jnp.concatenate([names, blank], axis=0).T[:padded, :6]
+        picks = picked_rows(routes.astype(jnp.int32), core, slot)
+        residual = total.astype(jnp.bfloat16)
+        inputs = rms_rows(residual.astype(jnp.float32), gain_ref[...]).astype(jnp.bfloat16)
+        if place == 0:
+            residual_ref[...] = residual[:seq_rows]
+            input_ref[...] = inputs[:seq_rows]
+        picked = lax.dot_general(
+            picks, inputs, (((0,), (0,)), ((), ())), preferred_element_type=jnp.float32
+        )
+        for lane in range(lanes):
+            wide_v[pl.ds(place * lanes + lane, peers, stride=2 * lanes), :] = picked[
+                :, lane * 128 : (lane + 1) * 128
+            ]
+    rows_ref[...] = wide_v[...].astype(jnp.bfloat16)
+
+
+def unpack_kernel(sent_ref, rows_ref, wide_v):
+    lanes = rows_ref.shape[1] // 128
+    experts = rows_ref.shape[0]
+    wide_v[...] = sent_ref[...].astype(jnp.float32)
     for lane in range(lanes):
-        wide_v[pl.ds(lane, experts, stride=lanes), :] = picked[:, lane * 128 : (lane + 1) * 128]
-    rows_ref[...] = wide_v[...].astype(jnp.bfloat16)
-
-
-def expert_kernel(
-    rows_ref,
-    own_ref,
-    other_ref,
-    shared_ref,
-    blocks_ref,
-    wide_v,
-    rows_v,
-):
-    lanes = 8
-    experts = rows_ref.shape[0] // lanes
-    width = lanes * 128
-    wide_v[...] = rows_ref[...].astype(jnp.float32)
-    for lane in range(lanes):
-        rows_v[:, lane * 128 : (lane + 1) * 128] = wide_v[
+        rows_ref[:, lane * 128 : (lane + 1) * 128] = wide_v[
             pl.ds(lane, experts, stride=lanes), :
         ].astype(jnp.bfloat16)
-    rows = rows_v[...]
+
+
+def expert_kernel(rows_ref, own_ref, other_ref, shared_ref, blocks_ref, total_v):
+    core = lax.axis_index("ep") % 2
+    experts, width = rows_ref.shape
+    rows = rows_ref[...]
     acts = []
     for pack_ref in (own_ref, other_ref):
         both = jnp.dot(rows, pack_ref[:width], preferred_element_type=jnp.float32)
         gate, up = both[:, :128], both[:, 128:]
         acts.append((gate / (1.0 + jnp.exp(-gate)) * up).astype(jnp.bfloat16))
     act = jnp.concatenate(acts, axis=1)
-    parts = blocks_ref.shape[0]
-    share = width // parts
-    for part in range(parts):
-        at = width + part * 128
-        down = jnp.concatenate([own_ref[at : at + 128], other_ref[at : at + 128]], axis=0)
+    group = blocks_ref.shape[0] // 2
+    share = width // group
+    peers = experts // 2
+    for part in range(group):
+        start = width + part * 128
+        down = jnp.concatenate([own_ref[start : start + 128], other_ref[start : start + 128]], axis=0)
         total = jnp.dot(act, down, preferred_element_type=jnp.float32)
-        blocks_ref[part, :experts, :] = total.astype(jnp.bfloat16)
-        blocks_ref[part, experts:, :] = shared_ref[:, part * share : (part + 1) * share]
+        for chunk in range(share // 128):
+            total_v[chunk] = total[:, chunk * 128 : (chunk + 1) * 128]
+        mine, theirs = [
+            jnp.concatenate(
+                [total_v[chunk, pl.ds(at, peers, stride=2), :] for chunk in range(share // 128)],
+                axis=1,
+            ).astype(jnp.bfloat16)
+            for at in range(2)
+        ]
+        shared = shared_ref[:, part * share : (part + 1) * share]
+        for target in range(2):
+            here = core == target
+            blocks_ref[target * group + part, :peers, :] = jnp.where(here, mine, theirs)
+            blocks_ref[target * group + part, peers:, :] = jnp.where(
+                here, shared, jnp.zeros_like(shared)
+            )
 
 
 def share_kernel(parts_ref, rows_ref, shared_ref, wide_v):
     share = parts_ref.shape[2]
     seq_rows = shared_ref.shape[0]
-    experts = parts_ref.shape[1] - seq_rows
-    quads = rows_ref.shape[0] // experts
+    peers = parts_ref.shape[1] - seq_rows
+    group = parts_ref.shape[0] // 2
     chunks = share // 128
-    for slot in range(2):
-        total = parts_ref[slot, :experts, :].astype(jnp.float32)
-        total += parts_ref[slot + 2, :experts, :].astype(jnp.float32)
-        for chunk in range(chunks):
-            wide_v[pl.ds(slot * chunks + chunk, experts, stride=quads), :] = total[
-                :, chunk * 128 : (chunk + 1) * 128
-            ]
+    stride = rows_ref.shape[0] // peers
+    for source in range(2):
+        for slot in range(2):
+            total = parts_ref[source * group + slot, :peers, :].astype(jnp.float32)
+            total += parts_ref[source * group + slot + 2, :peers, :].astype(jnp.float32)
+            for chunk in range(chunks):
+                at = (source * 2 + slot) * chunks + chunk
+                wide_v[pl.ds(at, peers, stride=stride), :] = total[
+                    :, chunk * 128 : (chunk + 1) * 128
+                ]
     rows_ref[...] = wide_v[...].astype(jnp.bfloat16)
-    shared = jnp.sum(parts_ref[:, experts:, :].astype(jnp.float32), axis=0)
+    shared = jnp.sum(parts_ref[:, peers:, :].astype(jnp.float32), axis=0)
     shared_ref[...] = shared.astype(jnp.bfloat16).astype(jnp.float32)
 
 
@@ -335,19 +404,25 @@
     share_width = model_width // tp_count
     hidden = expert_gate.shape[2]
     quads = 2 * (share_width // 128)
+    lanes = model_width // 128
+    sent_rows = seq_rows * lanes + 8
+    same_core = [[2 * p + k for p in range(ep_count // 2)] for k in range(2)]
+    chips = [
+        [(2 * p + k) * tp_count + t for k in range(2) for t in range(tp_count)]
+        for p in range(ep_count // 2)
+    ]
     f32, bf16 = jnp.float32, jnp.bfloat16
     state = delta_state.reshape(seq_rows, head_dim, head_dim)
-    partials, next_state, dispatch, mix, packed = pl.pallas_call(
+    partials, next_state, mix, packed = pl.pallas_call(
         mixer_kernel,
         out_shape=[
-            jax.ShapeDtypeStruct((tp_count, seq_rows, model_width), bf16),
+            jax.ShapeDtypeStruct((2 * tp_count, sent_rows, 128), bf16),
             jax.ShapeDtypeStruct(state.shape, f32),
-            pltpu.VMEM((seq_rows, ep_count), bf16),
             pltpu.VMEM((64 * (share_width // 128), ep_count * quads), bf16),
             pltpu.VMEM((3 * model_width // 2, 2 * hidden), bf16),
         ],
         in_specs=[anywhere()] * 17,
-        out_specs=[anywhere()] * 2 + [vmem()] * 3,
+        out_specs=[anywhere()] * 2 + [vmem()] * 2,
         scratch_shapes=[
             pltpu.VMEM((seq_rows, model_width), bf16),
             pltpu.VMEM((1, model_width), f32),
@@ -364,7 +439,9 @@
             pltpu.VMEM((seq_rows, head_dim, head_dim), f32),
             pltpu.VMEM((seq_rows, head_dim, head_dim), f32),
             pltpu.VMEM((head_dim, model_width), bf16),
-            pltpu.VMEM((tp_count, seq_rows, model_width), bf16),
+            pltpu.VMEM((2 * tp_count, sent_rows, 128), bf16),
+            pltpu.VMEM((sent_rows, 128), f32),
+            pltpu.VMEM((sent_rows, 128), f32),
             pltpu.VMEM((seq_rows, head_dim), f32),
             pltpu.VMEM((seq_rows, head_dim), f32),
             pltpu.SemaphoreType.DMA((17 + model_width // (2 * hidden),)),
@@ -388,9 +465,8 @@
         expert_up[0],
         expert_down[0],
     )
-    gathered = lax.all_to_all(partials, "tp", 0, 0, tiled=True)
+    gathered = lax.all_to_all(partials, ("ep", "tp"), 0, 0, axis_index_groups=chips, tiled=True)
     other = lax.ppermute(packed, "tp", [(i, i ^ 1) for i in range(tp_count)])
-    lanes = model_width // 128
     residual, expert_input, outgoing = pl.pallas_call(
         rows_kernel,
         out_shape=[
@@ -398,14 +474,17 @@
             pltpu.VMEM((seq_rows, model_width), bf16),
             pltpu.VMEM((ep_count * lanes, 128), bf16),
         ],
-        in_specs=[vmem()] * 4,
+        in_specs=[vmem()] * 3,
         out_specs=[vmem()] * 3,
-        scratch_shapes=[pltpu.VMEM((ep_count * lanes, 128), f32)],
+        scratch_shapes=[
+            pltpu.VMEM((2, 32 * lanes, 128), f32),
+            pltpu.VMEM((32, model_width), f32),
+            pltpu.VMEM((ep_count * lanes, 128), f32),
+        ],
     )(
         in_vmem(gathered),
         in_vmem(tokens),
         in_vmem(channel_gain.reshape(1, model_width)),
-        in_vmem(dispatch),
     )
     shared_act = (
         jax.nn.silu(jnp.dot(expert_input, shared_gate, preferred_element_type=f32))
@@ -413,23 +492,38 @@
     ).astype(bf16)
     shared_partial = jnp.dot(shared_act, shared_down, preferred_element_type=f32).astype(bf16)
     outgoing, shared_partial = lax.optimization_barrier((outgoing, shared_partial))
-    received = lax.all_to_all(outgoing.reshape(ep_count, lanes, 128), "ep", 0, 0, tiled=True)
+    received = lax.all_to_all(
+        outgoing.reshape(ep_count // 2, 2 * lanes, 128),
+        "ep",
+        0,
+        0,
+        axis_index_groups=same_core,
+        tiled=True,
+    )
+    rows = pl.pallas_call(
+        unpack_kernel,
+        out_shape=pltpu.VMEM((ep_count, model_width), bf16),
+        in_specs=[vmem()],
+        out_specs=vmem(),
+        scratch_shapes=[pltpu.VMEM((ep_count * lanes, 128), f32)],
+    )(in_vmem(received.reshape(ep_count * lanes, 128)))
     blocks = pl.pallas_call(
         expert_kernel,
-        out_shape=pltpu.VMEM((tp_count, ep_count + seq_rows, share_width), bf16),
+        out_shape=pltpu.VMEM((2 * tp_count, ep_count // 2 + seq_rows, share_width), bf16),
         in_specs=[vmem()] * 4,
         out_specs=vmem(),
         scratch_shapes=[
-            pltpu.VMEM((ep_count * lanes, 128), f32),
-            pltpu.VMEM((ep_count, model_width), bf16),
+            pltpu.VMEM((share_width // 128, ep_count, 128), f32),
         ],
     )(
-        in_vmem(received.reshape(ep_count * lanes, 128)),
+        in_vmem(rows),
         in_vmem(packed),
         in_vmem(other),
         in_vmem(shared_partial),
     )
-    parts = lax.all_to_all(blocks, "tp", 0, 0, tiled=True)
+    parts = lax.all_to_all(
+        blocks, ("ep", "tp"), 0, 0, axis_index_groups=chips, tiled=True
+    )
     expert_share, shared_out = pl.pallas_call(
         share_kernel,
         out_shape=[
@@ -440,7 +534,14 @@
         out_specs=[vmem()] * 2,
         scratch_shapes=[pltpu.VMEM((ep_count * quads, 128), f32)],
     )(in_vmem(parts))
-    returned = lax.all_to_all(expert_share.reshape(ep_count, quads, 128), "ep", 0, 0, tiled=True)
+    returned = lax.all_to_all(
+        expert_share.reshape(ep_count // 2, 2 * quads, 128),
+        "ep",
+        0,
+        0,
+        axis_index_groups=same_core,
+        tiled=True,
+    )
     layer_out = pl.pallas_call(
         final_kernel,
         out_shape=jax.ShapeDtypeStruct((seq_rows, share_width), bf16),

time: 81.1 us -> 80.1 us (0.988)
  blocking collectives: 62.3 us -> 53.2 us
  starting transfers between devices: 8.2 us -> 13.6 us
  waiting for transfers between devices: 1.81 us -> 3.82 us
    all_to_all x3, blocking collectives: 62.3 us -> 53.2 us  [the longest x1 25 us: per_device(): lax.all_to_all(outgoing.reshape(ep_count // 2, 2 * lanes, 128), 'ep', 0,...]
    all_to_all x1, starting transfers between devices: 4.84 us -> 10.3 us  [per_device(): lax.all_to_all(partials, ('ep', 'tp'), 0, 0, axis_index_groups=chips, til...]
    all_to_all x1, waiting for transfers between devices: 1.81 us -> 3.81 us  [per_device(): lax.all_to_all(partials, ('ep', 'tp'), 0, 0, axis_index_groups=chips, til...]
    pallas_call x2 -> x3, Pallas kernels: 4.73 us -> 4.9 us  [the longest x1 4.24 us: per_device(): pl.pallas_call(mixer_kernel, out_shape=[jax.ShapeDtypeStruct((2 * tp_coun...]
  transfers between devices with their start and end apart: 2 -> 2, of which waited for: 1 -> 1; matrix products, arithmetic and copies ran while one was open for 1% -> 1% of each run, Pallas kernels for 0% -> 1%
where the time goes in v7:
time: 80.1 us; the launch traced here: 79.7 us
  blocking collectives  53.2 us (66%)
  starting transfers between devices  13.6 us (17%)
  Pallas kernels  6.6 us (8%)
  waiting for transfers between devices  3.82 us (5%)
  between operations  2.09 us (3%)
    all_to_all x1, blocking collectives, per_device(): lax.all_to_all(outgoing.reshape(ep_count // 2, 2 * lanes, 128), 'ep', 0,...  25 us
    all_to_all x1, blocking collectives, per_device(): lax.all_to_all(expert_share.reshape(ep_count // 2, 2 * quads, 128), 'ep',...  15.4 us
    all_to_all x1, blocking collectives, per_device(): lax.all_to_all(blocks, ('ep', 'tp'), 0, 0, axis_index_groups=chips, tiled...  12.8 us
    all_to_all x1, starting transfers between devices, per_device(): lax.all_to_all(partials, ('ep', 'tp'), 0, 0, axis_index_groups=chips, til...  10.3 us
    pallas_call x1, Pallas kernels, per_device(): pl.pallas_call(mixer_kernel, out_shape=[jax.ShapeDtypeStruct((2 * tp_coun...  4.24 us
    all_to_all x1, waiting for transfers between devices, per_device(): lax.all_to_all(partials, ('ep', 'tp'), 0, 0, axis_index_groups=chips, til...  3.81 us
    ppermute x1, starting transfers between devices, per_device(): other = lax.ppermute(packed, 'tp', [(i, i ^ 1) for i in range(tp_count)])  3.25 us
  transfers between devices with their start and end apart: 2, of which 1 were waited for; matrix products, arithmetic and copies ran while one was open for 1% of the time, Pallas kernels for 1%

profile of v7, /device:TPU:1, one launch (start us, length us, event | category | flops | bytes accessed | tf_op | source)
XLA Modules:
  0.0 79.7 jit_solution(726141354817976823)
XLA Ops:
  0.6 0.0 copy-start
  2.0 0.0 copy-start.1
  2.0 0.0 copy-start.2
  2.0 0.0 copy-start.3
  2.0 4.2 %shard_map.212 = (bf16[8,152,128]{2,1,0:T(8,128)(2,1)}, f32[18,128,128]{2,1,0:T(8,128)}, bf16[128,512]{1,0:T(8,128)(2,1)S(1)}, bf16[1536,256]{1,0:T(8,128)(2,1)S(1)}) custom-call(bf16[18,1024]{1,0:T(8,128)(2,1)} %tokens_ref.1, f32[1,1024]{1,0:T(1,128)} %bitcast.32, bf16[1,1024]{1,0:T(2,128)(2,1)} %bitcast.33, bf16[1,1024]{1,0:T(2,128)(2,1)} %bitcast.34, ...), custom_call_target="tpu_custom_call" | custom-call | tf_op jit(solution)/shard_map/pallas_call | solution.py:416
  6.3 0.0 copy-start.4
  6.3 10.3 %all-to-all-start = ((bf16[8,152,128]{2,1,0:T(8,128)(2,1)}), bf16[8,152,128]{2,1,0:T(8,128)(2,1)S(1)}, u32[]{:S(2)}, u32[]{:S(2)}) async-start(bf16[8,152,128]{2,1,0:T(8,128)(2,1)} %get-tuple-element.13), calls=%async_computation | async-start | bytes 622592 | tf_op jit(solution)/shard_map/all_to_all | solution.py:468
  16.6 3.3 %collective-permute-start = (bf16[1536,256]{1,0:T(8,128)(2,1)S(1)}, bf16[1536,256]{1,0:T(8,128)(2,1)S(1)}, u32[]{:S(2)}, u32[]{:S(2)}) collective-permute-start(bf16[1536,256]{1,0:T(8,128)(2,1)S(1)} %get-tuple-element.17.own_ref), channel_id=1, source_target_pairs={{0,1},{1,0},{2,3},{3,2},{4,5},{5,4},{6,7},{7,6},{8,9},{9,8},{10,11... | collective-permute-start | bytes 2359304 | tf_op jit(solution)/shard_map/ppermute | solution.py:469
  19.9 3.8 %all-to-all-done.gathered_ref = bf16[8,152,128]{2,1,0:T(8,128)(2,1)S(1)} async-done(((bf16[8,152,128]{2,1,0:T(8,128)(2,1)}), bf16[8,152,128]{2,1,0:T(8,128)(2,1)S(1)}, u32[]{:S(2)}, u32[]{:S(2)}) %all-to-all-start) | async-done | bytes 311328 | tf_op jit(solution)/shard_map/all_to_all | solution.py:468
  23.7 0.0 copy-done.1
  23.7 0.0 copy-done.2
  23.7 0.8 %shard_map.213 = (bf16[18,1024]{1,0:T(8,128)(2,1)S(1)}, bf16[18,1024]{1,0:T(8,128)(2,1)S(1)}, bf16[1024,128]{1,0:T(8,128)(2,1)S(1)}) custom-call(bf16[8,152,128]{2,1,0:T(8,128)(2,1)S(1)} %all-to-all-done.gathered_ref, bf16[18,1024]{1,0:T(8,128)(2,1)S(1)} %copy-done.1, f32[1,1024]{1,0:T(1,128)S(1)} %bitcast.27), custom_call_target="tpu_custom_call" | custom-call | tf_op jit(solution)/shard_map/pallas_call | solution.py:470
  24.5 0.0 copy-done.3
  24.6 0.2 fusion.8
  24.7 0.0 copy-done
  24.7 0.3 convolution_convert_fusion.shared_ref
  25.0 25.0 %all_to_all.20 = bf16[64,16,128]{2,1,0:T(8,128)(2,1)S(1)} all-to-all(bf16[64,16,128]{2,1,0:T(8,128)(2,1)S(1)} %bitcast.25), channel_id=1, replica_groups={{0,8,16,24,32,40,48,56,64,72,80,88,96,104,112,120,128,136,144,152,160,1..., dimensions={0} | all-to-all | bytes 524288 | tf_op jit(solution)/shard_map/all_to_all | solution.py:495
  50.0 0.1 shard_map.214.rows_ref
  50.2 0.0 collective-permute-done.other_ref
  50.2 0.5 shard_map.215
  50.7 12.8 %all_to_all.21.parts_ref = bf16[8,82,256]{2,1,0:T(8,128)(2,1)S(1)} all-to-all(bf16[8,82,256]{2,1,0:T(8,128)(2,1)S(1)} %shard_map.215), channel_id=1, replica_groups={{0,1,2,3,4,5,6,7},{8,9,10,11,12,13,14,15},{16,17,18,19,20,21,22,23},{24..., dimensions={0} | all-to-all | bytes 671744 | tf_op jit(solution)/shard_map/all_to_all | solution.py:524
  63.5 0.1 shard_map.216
  63.6 15.4 %all_to_all.22 = bf16[64,8,128]{2,1,0:T(8,128)(2,1)S(1)} all-to-all(bf16[64,8,128]{2,1,0:T(8,128)(2,1)S(1)} %bitcast.26), channel_id=1, replica_groups={{0,8,16,24,32,40,48,56,64,72,80,88,96,104,112,120,128,136,144,152,160,1..., dimensions={0} | all-to-all | bytes 262144 | tf_op jit(solution)/shard_map/all_to_all | solution.py:537
  78.9 0.8 shard_map.217
  (1 shorter events, 0.0 us)
Async XLA Ops:
  0.6 24.1 %copy-start = (bf16[128,1024]{1,0:T(8,128)(2,1)S(1)}, bf16[128,1024]{1,0:T(8,128)(2,1)}, u32[]{:S(2)}) copy-start(bf16[128,1024]{1,0:T(8,128)(2,1)} %param.41) | copy-start | bytes 786436
  2.0 21.7 %copy-start.1 = (bf16[18,1024]{1,0:T(8,128)(2,1)S(1)}, bf16[18,1024]{1,0:T(8,128)(2,1)}, u32[]{:S(2)}) copy-start(bf16[18,1024]{1,0:T(8,128)(2,1)} %tokens_ref.1) | copy-start | bytes 110596
  2.0 21.7 %copy-start.2 = (f32[1024]{0:T(1024)S(1)}, f32[1024]{0:T(1024)}, u32[]{:S(2)}) copy-start(f32[1024]{0:T(1024)} %param.33) | copy-start | bytes 12292
  2.0 22.5 %copy-start.3 = (bf16[1024,128]{1,0:T(8,128)(2,1)S(1)}, bf16[1024,128]{1,0:T(8,128)(2,1)}, u32[]{:S(2)}) copy-start(bf16[1024,128]{1,0:T(8,128)(2,1)} %param.39) | copy-start | bytes 786436
  6.3 18.5 %copy-start.4 = (bf16[1024,128]{1,0:T(8,128)(2,1)S(1)}, bf16[1024,128]{1,0:T(8,128)(2,1)}, u32[]{:S(2)}) copy-start(bf16[1024,128]{1,0:T(8,128)(2,1)} %param.40) | copy-start | bytes 786436
  6.3 17.4 %all-to-all-start = ((bf16[8,152,128]{2,1,0:T(8,128)(2,1)}), bf16[8,152,128]{2,1,0:T(8,128)(2,1)S(1)}, u32[]{:S(2)}, u32[]{:S(2)}) async-start(bf16[8,152,128]{2,1,0:T(8,128)(2,1)} %get-tuple-element.13), calls=%async_computation | async-start | bytes 622592 | tf_op jit(solution)/shard_map/all_to_all | solution.py:468
  16.6 33.6 %collective-permute-start = (bf16[1536,256]{1,0:T(8,128)(2,1)S(1)}, bf16[1536,256]{1,0:T(8,128)(2,1)S(1)}, u32[]{:S(2)}, u32[]{:S(2)}) collective-permute-start(bf16[1536,256]{1,0:T(8,128)(2,1)S(1)} %get-tuple-element.17.own_ref), channel_id=1, source_target_pairs={{0,1},{1,0},{2,3},{3,2},{4,5},{5,4},{6,7},{7,6},{8,9},{9,8},{10,11... | collective-permute-start | bytes 2359304 | tf_op jit(solution)/shard_map/ppermute | solution.py:469

commit v8 on v7

--- a/solution.py
+++ b/solution.py
@@ -60,8 +60,9 @@
     up_hbm,
     down_hbm,
     partial_hbm,
-    next_hbm,
-    mix_ref,
+    key_unit_ref,
+    update_ref,
+    keep_ref,
     packed_ref,
     tokens_v,
     gain_v,
@@ -76,7 +77,6 @@
     key_v,
     value_v,
     state_v,
-    next_v,
     out_weight_v,
     partial_v,
     plain_v,
@@ -132,17 +132,6 @@
     biased = decay_logit + bias_v[0]
     softplus = jnp.maximum(biased, 0.0) + jnp.log1p(jnp.exp(-jnp.abs(biased)))
     keep = jnp.exp(-rate_v[0] * softplus)
-    routes = columns_of(routes_v[...].astype(jnp.float32))[:seq_rows].astype(jnp.int32)
-    weights = columns_of(weights_v[...])[:seq_rows]
-    scale = weights / jnp.sum(weights, axis=1, keepdims=True) * ROUTED_SCALE
-    expert_iota = lax.broadcasted_iota(jnp.int32, (seq_rows, 128), 1)
-    named = jnp.zeros((seq_rows, 128), jnp.float32)
-    mix = jnp.zeros((seq_rows, 128), jnp.float32)
-    for route in range(routes_hbm.shape[0]):
-        hit = expert_iota == routes[:, route : route + 1]
-        named = named + jnp.where(hit, 1.0, 0.0)
-        mix = mix + jnp.where(hit, scale[:, route : route + 1], 0.0)
-    chosen = earlier_rows(named)
     loads[8].wait()
     query_raw = jnp.dot(normed, query_v[...], preferred_element_type=jnp.float32)
     loads[9].wait()
@@ -194,20 +183,55 @@
         partial_v[copy_number] = jnp.where(core == copy_number // group, plain, mixed)
     store = pltpu.make_async_copy(partial_v, partial_hbm, sems.at[0])
     store.start()
-    keep_rows = jnp.broadcast_to(keep, update.shape)
-    stores = [store]
-    step = 3
-    for at in range(0, seq_rows, step):
-        for row in range(at, at + step):
-            next_v[row] = (
-                keep_rows[row : row + 1, :] * state_v[row]
-                + key_cols[:, row : row + 1] * update[row : row + 1, :]
-            )
-        store = pltpu.make_async_copy(
-            next_v.at[pl.ds(at, step)], next_hbm.at[pl.ds(at, step)], sems.at[1 + at // step]
+    key_unit_ref[...] = key_unit
+    update_ref[...] = update
+    keep_ref[...] = jnp.broadcast_to(keep, keep_ref.shape)
+    for copy in loads[15:]:
+        copy.wait()
+    store.wait()
+
+
+def state_kernel(
+    routes_ref,
+    weights_ref,
+    key_unit_ref,
+    update_ref,
+    keep_ref,
+    state_hbm,
+    next_hbm,
+    mix_ref,
+    state_v,
+    next_v,
+    sems,
+):
+    seq_rows = key_unit_ref.shape[0]
+    half = seq_rows // 2
+    spans = [(0, half), (half, seq_rows - half)]
+    loads = [
+        pltpu.make_async_copy(
+            state_hbm.at[pl.ds(at, size)], state_v.at[pl.ds(at, size)], sems.at[i]
         )
-        store.start()
-        stores.append(store)
+        for i, (at, size) in enumerate(spans)
+    ]
+    stores = [
+        pltpu.make_async_copy(
+            next_v.at[pl.ds(at, size)], next_hbm.at[pl.ds(at, size)], sems.at[2 + i]
+        )
+        for i, (at, size) in enumerate(spans)
+    ]
+    for copy in loads:
+        copy.start()
+    routes = columns_of(routes_ref[...].astype(jnp.float32))[:seq_rows].astype(jnp.int32)
+    weights = columns_of(weights_ref[...])[:seq_rows]
+    scale = weights / jnp.sum(weights, axis=1, keepdims=True) * ROUTED_SCALE
+    expert_iota = lax.broadcasted_iota(jnp.int32, (seq_rows, 128), 1)
+    named = jnp.zeros((seq_rows, 128), jnp.float32)
+    mix = jnp.zeros((seq_rows, 128), jnp.float32)
+    for route in range(routes_ref.shape[0]):
+        hit = expert_iota == routes[:, route : route + 1]
+        named = named + jnp.where(hit, 1.0, 0.0)
+        mix = mix + jnp.where(hit, scale[:, route : route + 1], 0.0)
+    chosen = earlier_rows(named)
     slots, experts = 2, 128
     chunks = mix_ref.shape[0] // 64
     spread = slots * chunks * experts
@@ -226,8 +250,15 @@
                 at = (part * chunks + chunk) * 32
                 kept = jnp.where(member == slot * chunks + chunk, grown, 0.0)
                 mix_ref[at : at + seq_rows, :] += kept.astype(jnp.bfloat16)
-    for copy in loads[15:]:
-        copy.wait()
+    key_cols = columns_of(key_unit_ref[...])
+    for part, (at, size) in enumerate(spans):
+        loads[part].wait()
+        for row in range(at, at + size):
+            next_v[row] = (
+                keep_ref[row : row + 1, :] * state_v[row]
+                + key_cols[:, row : row + 1] * update_ref[row : row + 1, :]
+            )
+        stores[part].start()
     for copy in stores:
         copy.wait()
 
@@ -413,16 +444,18 @@
     ]
     f32, bf16 = jnp.float32, jnp.bfloat16
     state = delta_state.reshape(seq_rows, head_dim, head_dim)
-    partials, next_state, mix, packed = pl.pallas_call(
+    small = pltpu.VMEM((seq_rows, head_dim), f32)
+    partials, key_unit, update, keep, packed = pl.pallas_call(
         mixer_kernel,
         out_shape=[
             jax.ShapeDtypeStruct((2 * tp_count, sent_rows, 128), bf16),
-            jax.ShapeDtypeStruct(state.shape, f32),
-            pltpu.VMEM((64 * (share_width // 128), ep_count * quads), bf16),
+            small,
+            small,
+            small,
             pltpu.VMEM((3 * model_width // 2, 2 * hidden), bf16),
         ],
         in_specs=[anywhere()] * 17,
-        out_specs=[anywhere()] * 2 + [vmem()] * 2,
+        out_specs=[anywhere()] + [vmem()] * 4,
         scratch_shapes=[
             pltpu.VMEM((seq_rows, model_width), bf16),
             pltpu.VMEM((1, model_width), f32),
@@ -436,7 +469,6 @@
             pltpu.VMEM((model_width, head_dim), bf16),
             pltpu.VMEM((model_width, head_dim), bf16),
             pltpu.VMEM((model_width, head_dim), bf16),
-            pltpu.VMEM((seq_rows, head_dim, head_dim), f32),
             pltpu.VMEM((seq_rows, head_dim, head_dim), f32),
             pltpu.VMEM((head_dim, model_width), bf16),
             pltpu.VMEM((2 * tp_count, sent_rows, 128), bf16),
@@ -465,7 +497,30 @@
         expert_up[0],
         expert_down[0],
     )
-    gathered = lax.all_to_all(partials, ("ep", "tp"), 0, 0, axis_index_groups=chips, tiled=True)
+    gathered = lax.all_to_all(
+        partials, ("ep", "tp"), 0, 0, axis_index_groups=chips, tiled=True
+    )
+    next_state, mix = pl.pallas_call(
+        state_kernel,
+        out_shape=[
+            jax.ShapeDtypeStruct(state.shape, f32),
+            pltpu.VMEM((64 * (share_width // 128), ep_count * quads), bf16),
+        ],
+        in_specs=[vmem()] * 5 + [anywhere()],
+        out_specs=[anywhere(), vmem()],
+        scratch_shapes=[
+            pltpu.VMEM(state.shape, f32),
+            pltpu.VMEM(state.shape, f32),
+            pltpu.SemaphoreType.DMA((4,)),
+        ],
+    )(
+        in_vmem(routes.T),
+        in_vmem(route_weights.T),
+        in_vmem(key_unit),
+        in_vmem(update),
+        in_vmem(keep),
+        state,
+    )
     other = lax.ppermute(packed, "tp", [(i, i ^ 1) for i in range(tp_count)])
     residual, expert_input, outgoing = pl.pallas_call(
         rows_kernel,
@@ -481,11 +536,7 @@
             pltpu.VMEM((32, model_width), f32),
             pltpu.VMEM((ep_count * lanes, 128), f32),
         ],
-    )(
-        in_vmem(gathered),
-        in_vmem(tokens),
-        in_vmem(channel_gain.reshape(1, model_width)),
-    )
+    )(in_vmem(gathered), in_vmem(tokens), in_vmem(channel_gain.reshape(1, model_width)))
     shared_act = (
         jax.nn.silu(jnp.dot(expert_input, shared_gate, preferred_element_type=f32))
         * jnp.dot(expert_input, shared_up, preferred_element_type=f32)

time: 80.1 us -> 81.2 us (1.014)
  blocking collectives: 53.2 us -> 37.8 us
  waiting for transfers between devices: 3.82 us -> 13 us
  starting transfers between devices: 13.6 us -> 18.2 us
  Pallas kernels: 6.6 us -> 9.13 us
    all_to_all x1 -> x0, blocking collectives: 15.4 us -> none  [per_device(): lax.all_to_all(expert_share.reshape(ep_count // 2, 2 * quads, 128), 'ep',...]
    all_to_all x0 -> x1, waiting for transfers between devices: none -> 9.19 us  [per_device(): lax.all_to_all(expert_share.reshape(ep_count // 2, 2 * quads, 128), 'ep',...]
    all_to_all x0 -> x1, starting transfers between devices: none -> 4.6 us  [per_device(): lax.all_to_all(expert_share.reshape(ep_count // 2, 2 * quads, 128), 'ep',...]
    pallas_call x0 -> x1, Pallas kernels: none -> 2.39 us  [per_device(): pl.pallas_call(state_kernel, out_shape=[jax.ShapeDtypeStruct(state.shape,...]
  transfers between devices with their start and end apart: 2 -> 3, of which waited for: 1 -> 2; matrix products, arithmetic and copies ran while one was open for 1% -> 1% of each run, Pallas kernels for 1% -> 4%
where the time goes in v8:
time: 81.2 us; the launch traced here: 80.7 us
  blocking collectives  37.8 us (47%)
  starting transfers between devices  18.2 us (22%)
  waiting for transfers between devices  13 us (16%)
  Pallas kernels  9.13 us (11%)
  between operations  2.13 us (3%)
    all_to_all x1, blocking collectives, per_device(): lax.all_to_all(outgoing.reshape(ep_count // 2, 2 * lanes, 128), 'ep', 0,...  25 us
    all_to_all x1, blocking collectives, per_device(): lax.all_to_all(blocks, ('ep', 'tp'), 0, 0, axis_index_groups=chips, tiled...  12.8 us
    all_to_all x1, starting transfers between devices, per_device(): lax.all_to_all(partials, ('ep', 'tp'), 0, 0, axis_index_groups=chips, til...  10.3 us
    all_to_all x1, waiting for transfers between devices, per_device(): lax.all_to_all(expert_share.reshape(ep_count // 2, 2 * quads, 128), 'ep',...  9.19 us
    all_to_all x1, starting transfers between devices, per_device(): lax.all_to_all(expert_share.reshape(ep_count // 2, 2 * quads, 128), 'ep',...  4.6 us
    all_to_all x1, waiting for transfers between devices, per_device(): lax.all_to_all(partials, ('ep', 'tp'), 0, 0, axis_index_groups=chips, til...  3.81 us
    pallas_call x1, Pallas kernels, per_device(): pl.pallas_call(mixer_kernel, out_shape=[jax.ShapeDtypeStruct((2 * tp_coun...  3.73 us
    ppermute x1, starting transfers between devices, per_device(): other = lax.ppermute(packed, 'tp', [(i, i ^ 1) for i in range(tp_count)])  3.25 us
  transfers between devices with their start and end apart: 3, of which 2 were waited for; matrix products, arithmetic and copies ran while one was open for 1% of the time, Pallas kernels for 4%

profile of v8, /device:TPU:1, one launch (start us, length us, event | category | flops | bytes accessed | tf_op | source)
XLA Modules:
  0.0 80.7 jit_solution(6891692205757896247)
XLA Ops:
  0.6 0.0 copy-start
  2.0 0.0 copy-start.1
  2.0 0.0 copy-start.4
  2.0 0.0 copy-start.5
  2.0 3.7 %shard_map.212 = (bf16[8,152,128]{2,1,0:T(8,128)(2,1)}, f32[18,128]{1,0:T(8,128)S(1)}, f32[18,128]{1,0:T(8,128)S(1)}, f32[18,128]{1,0:T(8,128)S(1)}, bf16[1536,256]{1,0:T(8,128)(2,1)S(1)}) custom-call(bf16[18,1024]{1,0:T(8,128)(2,1)} %tokens_ref.1, f32[1,1024]{1,0:T(1,128)} %bitcast.36, bf16[1,1024]{1,0:T(2,128)(2,1)} %bitcast.37, bf16[1,1024]{1,0:T(2,128)(2,1)} %bitcast.38, ...), custom_call_target="tpu_custom_call" | custom-call | tf_op jit(solution)/shard_map/pallas_call | solution.py:448
  5.7 0.0 copy-start.6
  5.8 10.3 %all-to-all-start = ((bf16[8,152,128]{2,1,0:T(8,128)(2,1)}), bf16[8,152,128]{2,1,0:T(8,128)(2,1)S(1)}, u32[]{:S(2)}, u32[]{:S(2)}) async-start(bf16[8,152,128]{2,1,0:T(8,128)(2,1)} %get-tuple-element.16), calls=%async_computation | async-start | bytes 622592 | tf_op jit(solution)/shard_map/all_to_all | solution.py:500
  16.1 3.3 %collective-permute-start = (bf16[1536,256]{1,0:T(8,128)(2,1)S(1)}, bf16[1536,256]{1,0:T(8,128)(2,1)S(1)}, u32[]{:S(2)}, u32[]{:S(2)}) collective-permute-start(bf16[1536,256]{1,0:T(8,128)(2,1)S(1)} %get-tuple-element.20.own_ref), channel_id=1, source_target_pairs={{0,1},{1,0},{2,3},{3,2},{4,5},{5,4},{6,7},{7,6},{8,9},{9,8},{10,11... | collective-permute-start | bytes 2359304 | tf_op jit(solution)/shard_map/ppermute | solution.py:524
  19.4 3.8 %all-to-all-done.gathered_ref = bf16[8,152,128]{2,1,0:T(8,128)(2,1)S(1)} async-done(((bf16[8,152,128]{2,1,0:T(8,128)(2,1)}), bf16[8,152,128]{2,1,0:T(8,128)(2,1)S(1)}, u32[]{:S(2)}, u32[]{:S(2)}) %all-to-all-start) | async-done | bytes 311328 | tf_op jit(solution)/shard_map/all_to_all | solution.py:500
  23.2 0.8 %shard_map.213 = (bf16[18,1024]{1,0:T(8,128)(2,1)S(1)}, bf16[18,1024]{1,0:T(8,128)(2,1)S(1)}, bf16[1024,128]{1,0:T(8,128)(2,1)S(1)}) custom-call(bf16[8,152,128]{2,1,0:T(8,128)(2,1)S(1)} %all-to-all-done.gathered_ref, bf16[18,1024]{1,0:T(8,128)(2,1)S(1)} %copy-done.1, f32[1,1024]{1,0:T(1,128)S(1)} %bitcast.30), custom_call_target="tpu_custom_call" | custom-call | tf_op jit(solution)/shard_map/pallas_call | solution.py:525
  24.0 0.2 fusion.8
  24.2 0.3 convolution_convert_fusion.shared_ref
  24.5 25.0 %all_to_all.20 = bf16[64,16,128]{2,1,0:T(8,128)(2,1)S(1)} all-to-all(bf16[64,16,128]{2,1,0:T(8,128)(2,1)S(1)} %bitcast.25), channel_id=1, replica_groups={{0,8,16,24,32,40,48,56,64,72,80,88,96,104,112,120,128,136,144,152,160,1..., dimensions={0} | all-to-all | bytes 524288 | tf_op jit(solution)/shard_map/all_to_all | solution.py:546
  49.5 0.1 shard_map.214.rows_ref
  49.7 0.0 collective-permute-done.other_ref
  49.7 0.5 shard_map.215
  50.2 0.0 copy-start.2
  50.2 0.0 copy-start.3
  50.2 12.8 %all_to_all.21.parts_ref = bf16[8,82,256]{2,1,0:T(8,128)(2,1)S(1)} all-to-all(bf16[8,82,256]{2,1,0:T(8,128)(2,1)S(1)} %shard_map.215), channel_id=1, replica_groups={{0,1,2,3,4,5,6,7},{8,9,10,11,12,13,14,15},{16,17,18,19,20,21,22,23},{24..., dimensions={0} | all-to-all | bytes 671744 | tf_op jit(solution)/shard_map/all_to_all | solution.py:575
  63.0 0.7 shard_map.216
  63.7 4.6 %all-to-all-start.3 = ((bf16[64,8,128]{2,1,0:T(8,128)(2,1)}), bf16[64,8,128]{2,1,0:T(8,128)(2,1)S(1)}, u32[]{:S(2)}, u32[]{:S(2)}) async-start(bf16[64,8,128]{2,1,0:T(8,128)(2,1)} %bitcast.13), calls=%async_computation.3 | async-start | bytes 262144 | tf_op jit(solution)/shard_map/all_to_all | solution.py:588
  68.4 2.4 %shard_map.217 = (f32[18,128,128]{2,1,0:T(8,128)}, bf16[128,512]{1,0:T(8,128)(2,1)S(1)}) custom-call(s32[6,18]{1,0:T(8,128)S(1)} %bitcast.27, f32[6,18]{1,0:T(8,128)S(1)} %bitcast.29, f32[18,128]{1,0:T(8,128)S(1)} %get-tuple-element.23.key_unit_ref, f32[18,128]{1,0:T(8,128)S(1)} %get-tuple-element.24.update_ref, f32[18,128]{1,0:T(8,128)S(1)} %get-tuple-element.25.keep_ref, ...), custom_call_target="tpu_custom_call" | custom-call | tf_op jit(solution)/shard_map/pallas_call | solution.py:503
  70.8 9.2 %all-to-all-done.3 = bf16[64,8,128]{2,1,0:T(8,128)(2,1)S(1)} async-done(((bf16[64,8,128]{2,1,0:T(8,128)(2,1)}), bf16[64,8,128]{2,1,0:T(8,128)(2,1)S(1)}, u32[]{:S(2)}, u32[]{:S(2)}) %all-to-all-start.3) | async-done | bytes 131104 | tf_op jit(solution)/shard_map/all_to_all | solution.py:588
  80.0 0.8 shard_map.218
  (7 shorter events, 0.0 us)
Async XLA Ops:
  0.6 23.6 %copy-start = (bf16[128,1024]{1,0:T(8,128)(2,1)S(1)}, bf16[128,1024]{1,0:T(8,128)(2,1)}, u32[]{:S(2)}) copy-start(bf16[128,1024]{1,0:T(8,128)(2,1)} %param.41) | copy-start | bytes 786436
  2.0 21.2 %copy-start.1 = (bf16[18,1024]{1,0:T(8,128)(2,1)S(1)}, bf16[18,1024]{1,0:T(8,128)(2,1)}, u32[]{:S(2)}) copy-start(bf16[18,1024]{1,0:T(8,128)(2,1)} %tokens_ref.1) | copy-start | bytes 110596
  2.0 21.2 %copy-start.4 = (f32[1024]{0:T(1024)S(1)}, f32[1024]{0:T(1024)}, u32[]{:S(2)}) copy-start(f32[1024]{0:T(1024)} %param.33) | copy-start | bytes 12292
  2.0 22.0 %copy-start.5 = (bf16[1024,128]{1,0:T(8,128)(2,1)S(1)}, bf16[1024,128]{1,0:T(8,128)(2,1)}, u32[]{:S(2)}) copy-start(bf16[1024,128]{1,0:T(8,128)(2,1)} %param.39) | copy-start | bytes 786436
  5.7 18.5 %copy-start.6 = (bf16[1024,128]{1,0:T(8,128)(2,1)S(1)}, bf16[1024,128]{1,0:T(8,128)(2,1)}, u32[]{:S(2)}) copy-start(bf16[1024,128]{1,0:T(8,128)(2,1)} %param.40) | copy-start | bytes 786436
  5.8 17.4 %all-to-all-start = ((bf16[8,152,128]{2,1,0:T(8,128)(2,1)}), bf16[8,152,128]{2,1,0:T(8,128)(2,1)S(1)}, u32[]{:S(2)}, u32[]{:S(2)}) async-start(bf16[8,152,128]{2,1,0:T(8,128)(2,1)} %get-tuple-element.16), calls=%async_computation | async-start | bytes 622592 | tf_op jit(solution)/shard_map/all_to_all | solution.py:500
  16.1 33.6 %collective-permute-start = (bf16[1536,256]{1,0:T(8,128)(2,1)S(1)}, bf16[1536,256]{1,0:T(8,128)(2,1)S(1)}, u32[]{:S(2)}, u32[]{:S(2)}) collective-permute-start(bf16[1536,256]{1,0:T(8,128)(2,1)S(1)} %get-tuple-element.20.own_ref), channel_id=1, source_target_pairs={{0,1},{1,0},{2,3},{3,2},{4,5},{5,4},{6,7},{7,6},{8,9},{9,8},{10,11... | collective-permute-start | bytes 2359304 | tf_op jit(solution)/shard_map/ppermute | solution.py:524
  50.2 18.2 %copy-start.2 = (s32[18,6]{0,1:T(8,128)S(1)}, s32[18,6]{0,1:T(8,128)}, u32[]{:S(2)}) copy-start(s32[18,6]{0,1:T(8,128)} %param.34) | copy-start | bytes 1300
  50.2 18.2 %copy-start.3 = (f32[18,6]{0,1:T(8,128)S(1)}, f32[18,6]{0,1:T(8,128)}, u32[]{:S(2)}) copy-start(f32[18,6]{0,1:T(8,128)} %param.35) | copy-start | bytes 1300
  63.7 16.2 %all-to-all-start.3 = ((bf16[64,8,128]{2,1,0:T(8,128)(2,1)}), bf16[64,8,128]{2,1,0:T(8,128)(2,1)S(1)}, u32[]{:S(2)}, u32[]{:S(2)}) async-start(bf16[64,8,128]{2,1,0:T(8,128)(2,1)} %bitcast.13), calls=%async_computation.3 | async-start | bytes 262144 | tf_op jit(solution)/shard_map/all_to_all | solution.py:588

commit v9 on v8

--- a/solution.py
+++ b/solution.py
@@ -267,8 +267,11 @@
     gathered_ref,
     tokens_ref,
     gain_ref,
+    shared_gate_ref,
+    shared_up_ref,
+    shared_down_ref,
     residual_ref,
-    input_ref,
+    shared_ref,
     rows_ref,
     sums_v,
     tokens_v,
@@ -303,7 +306,11 @@
         inputs = rms_rows(residual.astype(jnp.float32), gain_ref[...]).astype(jnp.bfloat16)
         if place == 0:
             residual_ref[...] = residual[:seq_rows]
-            input_ref[...] = inputs[:seq_rows]
+            gate = jnp.dot(inputs, shared_gate_ref[...], preferred_element_type=jnp.float32)
+            up = jnp.dot(inputs, shared_up_ref[...], preferred_element_type=jnp.float32)
+            act = (gate / (1.0 + jnp.exp(-gate)) * up).astype(jnp.bfloat16)
+            shared = jnp.dot(act, shared_down_ref[...], preferred_element_type=jnp.float32)
+            shared_ref[...] = shared.astype(jnp.bfloat16)[:seq_rows]
         picked = lax.dot_general(
             picks, inputs, (((0,), (0,)), ((), ())), preferred_element_type=jnp.float32
         )
@@ -497,9 +504,7 @@
         expert_up[0],
         expert_down[0],
     )
-    gathered = lax.all_to_all(
-        partials, ("ep", "tp"), 0, 0, axis_index_groups=chips, tiled=True
-    )
+    gathered = lax.all_to_all(partials, ("ep", "tp"), 0, 0, axis_index_groups=chips, tiled=True)
     next_state, mix = pl.pallas_call(
         state_kernel,
         out_shape=[
@@ -522,27 +527,28 @@
         state,
     )
     other = lax.ppermute(packed, "tp", [(i, i ^ 1) for i in range(tp_count)])
-    residual, expert_input, outgoing = pl.pallas_call(
+    residual, shared_partial, outgoing = pl.pallas_call(
         rows_kernel,
         out_shape=[
             pltpu.VMEM((seq_rows, model_width), bf16),
             pltpu.VMEM((seq_rows, model_width), bf16),
             pltpu.VMEM((ep_count * lanes, 128), bf16),
         ],
-        in_specs=[vmem()] * 3,
+        in_specs=[vmem()] * 6,
         out_specs=[vmem()] * 3,
         scratch_shapes=[
             pltpu.VMEM((2, 32 * lanes, 128), f32),
             pltpu.VMEM((32, model_width), f32),
             pltpu.VMEM((ep_count * lanes, 128), f32),
         ],
-    )(in_vmem(gathered), in_vmem(tokens), in_vmem(channel_gain.reshape(1, model_width)))
-    shared_act = (
-        jax.nn.silu(jnp.dot(expert_input, shared_gate, preferred_element_type=f32))
-        * jnp.dot(expert_input, shared_up, preferred_element_type=f32)
-    ).astype(bf16)
-    shared_partial = jnp.dot(shared_act, shared_down, preferred_element_type=f32).astype(bf16)
-    outgoing, shared_partial = lax.optimization_barrier((outgoing, shared_partial))
+    )(
+        in_vmem(gathered),
+        in_vmem(tokens),
+        in_vmem(channel_gain.reshape(1, model_width)),
+        in_vmem(shared_gate),
+        in_vmem(shared_up),
+        in_vmem(shared_down),
+    )
     received = lax.all_to_all(
         outgoing.reshape(ep_count // 2, 2 * lanes, 128),
         "ep",

time: 81.2 us -> 81.8 us (level)
  Pallas kernels: 9.13 us -> 10.4 us
    pallas_call x1, Pallas kernels: 0.52 us -> 1.67 us  [per_device(): pl.pallas_call(expert_kernel, out_shape=pltpu.VMEM((2 * tp_count, ep_coun...]
  transfers between devices with their start and end apart: 3 -> 3, of which waited for: 2 -> 2; matrix products, arithmetic and copies ran while one was open for 1% -> 0% of each run, Pallas kernels for 4% -> 4%
where the time goes in v9:
time: 81.8 us; the launch traced here: 81.4 us
  blocking collectives  37.8 us (46%)
  starting transfers between devices  18.1 us (22%)
  waiting for transfers between devices  13 us (16%)
  Pallas kernels  10.4 us (13%)
  between operations  2.08 us (3%)
    all_to_all x1, blocking collectives, per_device(): lax.all_to_all(outgoing.reshape(ep_count // 2, 2 * lanes, 128), 'ep', 0,...  25 us
    all_to_all x1, blocking collectives, per_device(): lax.all_to_all(blocks, ('ep', 'tp'), 0, 0, axis_index_groups=chips, tiled...  12.8 us
    all_to_all x1, starting transfers between devices, per_device(): lax.all_to_all(partials, ('ep', 'tp'), 0, 0, axis_index_groups=chips, til...  10.2 us
    all_to_all x1, waiting for transfers between devices, per_device(): lax.all_to_all(expert_share.reshape(ep_count // 2, 2 * quads, 128), 'ep',...  9.19 us
    all_to_all x1, starting transfers between devices, per_device(): lax.all_to_all(expert_share.reshape(ep_count // 2, 2 * quads, 128), 'ep',...  4.6 us
    all_to_all x1, waiting for transfers between devices, per_device(): lax.all_to_all(partials, ('ep', 'tp'), 0, 0, axis_index_groups=chips, til...  3.81 us
    pallas_call x1, Pallas kernels, per_device(): pl.pallas_call(mixer_kernel, out_shape=[jax.ShapeDtypeStruct((2 * tp_coun...  3.73 us
    ppermute x1, starting transfers between devices, per_device(): other = lax.ppermute(packed, 'tp', [(i, i ^ 1) for i in range(tp_count)])  3.26 us
  transfers between devices with their start and end apart: 3, of which 2 were waited for; matrix products, arithmetic and copies ran while one was open for 0% of the time, Pallas kernels for 4%

profile of v9, /device:TPU:1, one launch (start us, length us, event | category | flops | bytes accessed | tf_op | source)
XLA Modules:
  0.0 81.4 jit_solution(11917780232745158845)
XLA Ops:
  1.9 0.0 copy-start
  1.9 0.0 copy-start.1
  1.9 0.0 copy-start.2
  2.0 0.0 copy-start.3
  2.0 0.0 copy-start.6
  2.0 3.7 %shard_map.212 = (bf16[8,152,128]{2,1,0:T(8,128)(2,1)}, f32[18,128]{1,0:T(8,128)S(1)}, f32[18,128]{1,0:T(8,128)S(1)}, f32[18,128]{1,0:T(8,128)S(1)}, bf16[1536,256]{1,0:T(8,128)(2,1)S(1)}) custom-call(bf16[18,1024]{1,0:T(8,128)(2,1)} %tokens_ref.1, f32[1,1024]{1,0:T(1,128)} %bitcast.31, bf16[1,1024]{1,0:T(2,128)(2,1)} %bitcast.32, bf16[1,1024]{1,0:T(2,128)(2,1)} %bitcast.33, ...), custom_call_target="tpu_custom_call" | custom-call | tf_op jit(solution)/shard_map/pallas_call | solution.py:455
  5.7 10.2 %all-to-all-start = ((bf16[8,152,128]{2,1,0:T(8,128)(2,1)}), bf16[8,152,128]{2,1,0:T(8,128)(2,1)S(1)}, u32[]{:S(2)}, u32[]{:S(2)}) async-start(bf16[8,152,128]{2,1,0:T(8,128)(2,1)} %get-tuple-element.14), calls=%async_computation | async-start | bytes 622592 | tf_op jit(solution)/shard_map/all_to_all | solution.py:507
  15.9 3.3 %collective-permute-start = (bf16[1536,256]{1,0:T(8,128)(2,1)S(1)}, bf16[1536,256]{1,0:T(8,128)(2,1)}, u32[]{:S(2)}, u32[]{:S(2)}) collective-permute-start(bf16[1536,256]{1,0:T(8,128)(2,1)S(1)} %get-tuple-element.16.own_ref), channel_id=1, source_target_pairs={{0,1},{1,0},{2,3},{3,2},{4,5},{5,4},{6,7},{7,6},{8,9},{9,8},{10,11... | collective-permute-start | bytes 2359304 | tf_op jit(solution)/shard_map/ppermute | solution.py:529
  19.2 3.8 %all-to-all-done.gathered_ref = bf16[8,152,128]{2,1,0:T(8,128)(2,1)S(1)} async-done(((bf16[8,152,128]{2,1,0:T(8,128)(2,1)}), bf16[8,152,128]{2,1,0:T(8,128)(2,1)S(1)}, u32[]{:S(2)}, u32[]{:S(2)}) %all-to-all-start) | async-done | bytes 311328 | tf_op jit(solution)/shard_map/all_to_all | solution.py:507
  23.0 0.0 copy-done
  23.0 0.0 copy-done.1
  23.0 1.0 %shard_map.213 = (bf16[18,1024]{1,0:T(8,128)(2,1)S(1)}, bf16[18,1024]{1,0:T(8,128)(2,1)S(1)}, bf16[1024,128]{1,0:T(8,128)(2,1)S(1)}) custom-call(bf16[8,152,128]{2,1,0:T(8,128)(2,1)S(1)} %all-to-all-done.gathered_ref, bf16[18,1024]{1,0:T(8,128)(2,1)S(1)} %copy-done.3, f32[1,1024]{1,0:T(1,128)S(1)} %bitcast.25, bf16[1024,128]{1,0:T(8,128)(2,1)S(1)} %copy-done, ...), custom_call_target="tpu_custom_call" | custom-call | tf_op jit(solution)/shard_map/pallas_call | solution.py:530
  24.0 25.0 %all_to_all.20 = bf16[64,16,128]{2,1,0:T(8,128)(2,1)S(1)} all-to-all(bf16[64,16,128]{2,1,0:T(8,128)(2,1)S(1)} %bitcast.20), channel_id=1, replica_groups={{0,8,16,24,32,40,48,56,64,72,80,88,96,104,112,120,128,136,144,152,160,1..., dimensions={0} | all-to-all | bytes 524288 | tf_op jit(solution)/shard_map/all_to_all | solution.py:552
  49.0 0.1 shard_map.214.rows_ref
  49.1 0.0 collective-permute-done.other_ref
  49.2 1.7 %shard_map.215 = bf16[8,82,256]{2,1,0:T(8,128)(2,1)S(1)} custom-call(bf16[128,1024]{1,0:T(8,128)(2,1)S(1)} %shard_map.214.rows_ref, bf16[1536,256]{1,0:T(8,128)(2,1)S(1)} %get-tuple-element.16.own_ref, bf16[1536,256]{1,0:T(8,128)(2,1)} %collective-permute-done.other_ref, bf16[18,1024]{1,0:T(8,128)(2,1)S(1)} %get-tuple-element.17.shared_ref), custom_call_target="tpu_custom_call" | custom-call | tf_op jit(solution)/shard_map/pallas_call | solution.py:567
  50.8 0.0 copy-start.4
  50.8 0.0 copy-start.5
  50.9 12.8 %all_to_all.21.parts_ref = bf16[8,82,256]{2,1,0:T(8,128)(2,1)S(1)} all-to-all(bf16[8,82,256]{2,1,0:T(8,128)(2,1)S(1)} %shard_map.215), channel_id=1, replica_groups={{0,1,2,3,4,5,6,7},{8,9,10,11,12,13,14,15},{16,17,18,19,20,21,22,23},{24..., dimensions={0} | all-to-all | bytes 671744 | tf_op jit(solution)/shard_map/all_to_all | solution.py:581
  63.7 0.7 shard_map.216
  64.4 4.6 %all-to-all-start.3 = ((bf16[64,8,128]{2,1,0:T(8,128)(2,1)}), bf16[64,8,128]{2,1,0:T(8,128)(2,1)S(1)}, u32[]{:S(2)}, u32[]{:S(2)}) async-start(bf16[64,8,128]{2,1,0:T(8,128)(2,1)} %bitcast.13), calls=%async_computation.3 | async-start | bytes 262144 | tf_op jit(solution)/shard_map/all_to_all | solution.py:594
  69.0 2.4 %shard_map.217 = (f32[18,128,128]{2,1,0:T(8,128)}, bf16[128,512]{1,0:T(8,128)(2,1)S(1)}) custom-call(s32[6,18]{1,0:T(8,128)S(1)} %bitcast.22, f32[6,18]{1,0:T(8,128)S(1)} %bitcast.24, f32[18,128]{1,0:T(8,128)S(1)} %get-tuple-element.19.key_unit_ref, f32[18,128]{1,0:T(8,128)S(1)} %get-tuple-element.20.update_ref, f32[18,128]{1,0:T(8,128)S(1)} %get-tuple-element.21.keep_ref, ...), custom_call_target="tpu_custom_call" | custom-call | tf_op jit(solution)/shard_map/pallas_call | solution.py:508
  71.4 9.2 %all-to-all-done.3 = bf16[64,8,128]{2,1,0:T(8,128)(2,1)S(1)} async-done(((bf16[64,8,128]{2,1,0:T(8,128)(2,1)}), bf16[64,8,128]{2,1,0:T(8,128)(2,1)S(1)}, u32[]{:S(2)}, u32[]{:S(2)}) %all-to-all-start.3) | async-done | bytes 131104 | tf_op jit(solution)/shard_map/all_to_all | solution.py:594
  80.6 0.8 shard_map.218
  (5 shorter events, 0.0 us)
Async XLA Ops:
  1.9 21.1 %copy-start = (bf16[1024,128]{1,0:T(8,128)(2,1)S(1)}, bf16[1024,128]{1,0:T(8,128)(2,1)}, u32[]{:S(2)}) copy-start(bf16[1024,128]{1,0:T(8,128)(2,1)} %shared_gate_ref.1) | copy-start | bytes 786436
  1.9 21.1 %copy-start.1 = (bf16[1024,128]{1,0:T(8,128)(2,1)S(1)}, bf16[1024,128]{1,0:T(8,128)(2,1)}, u32[]{:S(2)}) copy-start(bf16[1024,128]{1,0:T(8,128)(2,1)} %shared_up_ref.1) | copy-start | bytes 786436
  1.9 21.1 %copy-start.2 = (bf16[128,1024]{1,0:T(8,128)(2,1)S(1)}, bf16[128,1024]{1,0:T(8,128)(2,1)}, u32[]{:S(2)}) copy-start(bf16[128,1024]{1,0:T(8,128)(2,1)} %shared_down_ref.1) | copy-start | bytes 786436
  2.0 21.0 %copy-start.3 = (bf16[18,1024]{1,0:T(8,128)(2,1)S(1)}, bf16[18,1024]{1,0:T(8,128)(2,1)}, u32[]{:S(2)}) copy-start(bf16[18,1024]{1,0:T(8,128)(2,1)} %tokens_ref.1) | copy-start | bytes 110596
  2.0 21.0 %copy-start.6 = (f32[1024]{0:T(1024)S(1)}, f32[1024]{0:T(1024)}, u32[]{:S(2)}) copy-start(f32[1024]{0:T(1024)} %param.33) | copy-start | bytes 12292
  5.7 17.3 %all-to-all-start = ((bf16[8,152,128]{2,1,0:T(8,128)(2,1)}), bf16[8,152,128]{2,1,0:T(8,128)(2,1)S(1)}, u32[]{:S(2)}, u32[]{:S(2)}) async-start(bf16[8,152,128]{2,1,0:T(8,128)(2,1)} %get-tuple-element.14), calls=%async_computation | async-start | bytes 622592 | tf_op jit(solution)/shard_map/all_to_all | solution.py:507
  15.9 33.2 %collective-permute-start = (bf16[1536,256]{1,0:T(8,128)(2,1)S(1)}, bf16[1536,256]{1,0:T(8,128)(2,1)}, u32[]{:S(2)}, u32[]{:S(2)}) collective-permute-start(bf16[1536,256]{1,0:T(8,128)(2,1)S(1)} %get-tuple-element.16.own_ref), channel_id=1, source_target_pairs={{0,1},{1,0},{2,3},{3,2},{4,5},{5,4},{6,7},{7,6},{8,9},{9,8},{10,11... | collective-permute-start | bytes 2359304 | tf_op jit(solution)/shard_map/ppermute | solution.py:529
  50.8 18.2 %copy-start.4 = (s32[18,6]{0,1:T(8,128)S(1)}, s32[18,6]{0,1:T(8,128)}, u32[]{:S(2)}) copy-start(s32[18,6]{0,1:T(8,128)} %param.34) | copy-start | bytes 1300
  50.8 18.2 %copy-start.5 = (f32[18,6]{0,1:T(8,128)S(1)}, f32[18,6]{0,1:T(8,128)}, u32[]{:S(2)}) copy-start(f32[18,6]{0,1:T(8,128)} %param.35) | copy-start | bytes 1300
  64.4 16.2 %all-to-all-start.3 = ((bf16[64,8,128]{2,1,0:T(8,128)(2,1)}), bf16[64,8,128]{2,1,0:T(8,128)(2,1)S(1)}, u32[]{:S(2)}, u32[]{:S(2)}) async-start(bf16[64,8,128]{2,1,0:T(8,128)(2,1)} %bitcast.13), calls=%async_computation.3 | async-start | bytes 262144 | tf_op jit(solution)/shard_map/all_to_all | solution.py:594
